TPU v7x, 512 devices: a whole 4x8x8 slice. The times are simulated.
512 devices in a mesh: sp: 32 (over z, x), dp: 16 (over y, core).
Axes of the slice: x: 4, y: 8, z: 8, core: 2. Of those that a mesh axis runs over, the one named last changes fastest.
Arguments:
- inputs: bfloat16 [16, 4096, 2048], P('dp', 'sp'), may hold values from -6 to 6
- w_key: bfloat16 [2048, 256], P('dp')
- w_value: bfloat16 [2048, 256], P('dp'), may hold values from -0.125 to 0.125
- queries: bfloat16 [16, 4096, 2048], P('dp', 'sp')
- cotangent: bfloat16 [16, 4096, 2048], P('dp', 'sp'), may hold values from -6 to 6
- cum_gate: float32 [16, 32, 4096], P('dp', 'sp'), as said below
Outputs:
- grad_input: bfloat16 [16, 4096, 2048], P('dp', 'sp')
- grad_queries: bfloat16 [16, 4096, 2048], P('dp', 'sp')
- grad_cum: float32 [16, 32, 4096], P('dp', 'sp')
- grad_w_key: float32 [2048, 256], P('dp')
- grad_w_value: float32 [2048, 256], P('dp')
Inputs may be any that keep to these rules, and one draw needn't show every extreme that they name: Along each sequence cum_gate never rises, and it is at most zero.
All inputs are finite; a program needn't handle non-finite values.
Results may differ from a plain program's by a relative error of at most 0.023.
Values may be sent and summed in bfloat16 or wider, within the bound.
No kernel may reach another device: no remote copies, remote signals or barrier semaphores. Data moves between devices by JAX's collectives and lax.ppermute only.
A program may use at most 128 MiB of HBM per device.

v0:
```python
import functools

import jax
import jax.numpy as jnp
from jax import lax
from jax.sharding import Mesh
from jax.sharding import PartitionSpec as P

HD = 64
BLOCKS = 16
SP = ("sp_0", "sp_1")


def side_by_side(arrays, axis, dim, along):
    widths = [a.shape[along] for a in arrays]
    both = jnp.concatenate(arrays, axis=along)
    result = lax.all_gather(both, axis, axis=dim, tiled=True)
    return tuple(jnp.split(result, [sum(widths[:k]) for k in range(1, len(widths))], axis=along))


def sent_together(arrays, axis, split_dim, concat_dim, along):
    widths = [a.shape[along] for a in arrays]
    both = jnp.concatenate(arrays, axis=along)
    result = lax.all_to_all(both, axis, split_axis=split_dim, concat_axis=concat_dim, tiled=True)
    return tuple(jnp.split(result, [sum(widths[:k]) for k in range(1, len(widths))], axis=along))


def over_axes(x, axes):
    return functools.reduce(lax.psum, axes, x)


def attend_sequence(query_seq, key_seq, value_seq, grad_seq, cum_seq):
    seq_length = query_seq.shape[0]
    block_rows = seq_length // BLOCKS
    score_scale = HD ** (-0.5)
    key_parts = []
    value_parts = []
    column_parts = []
    row_parts = []
    query_blocks = []
    for block_index in range(BLOCKS):
        row_low = block_index * block_rows
        row_high = row_low + block_rows
        query_block = query_seq[row_low:row_high]
        grad_block = grad_seq[row_low:row_high]
        key_prefix = key_seq[:row_high]
        value_prefix = value_seq[:row_high]
        scores = (
            jnp.einsum("thd,shd->hts", query_block, key_prefix, preferred_element_type=jnp.float32)
            * score_scale
        )
        scores = scores + cum_seq[:, row_low:row_high, None] - cum_seq[:, None, :row_high]
        later = jnp.arange(row_high)[None, :] > (row_low + jnp.arange(block_rows))[:, None]
        scores = jnp.where(later[None], -jnp.inf, scores)
        row_max = jnp.max(scores, axis=2, keepdims=True)
        exp_scores = jnp.exp(scores - row_max)
        probs = exp_scores / jnp.sum(exp_scores, axis=2, keepdims=True)
        probs_low = probs.astype(jnp.bfloat16)
        outputs = jnp.einsum(
            "hts,shd->thd", probs_low, value_prefix, preferred_element_type=jnp.float32
        )
        row_dot = jnp.sum(grad_block.astype(jnp.float32) * outputs, axis=2).T
        grad_probs = jnp.einsum(
            "thd,shd->hts", grad_block, value_prefix, preferred_element_type=jnp.float32
        )
        grad_scores = probs * (grad_probs - row_dot[:, :, None])
        grad_low = grad_scores.astype(jnp.bfloat16)
        row_parts.append(jnp.sum(grad_scores, axis=2))
        column_parts.append(jnp.sum(grad_scores, axis=1))
        query_grad = jnp.einsum(
            "hts,shd->thd", grad_low, key_prefix, preferred_element_type=jnp.float32
        )
        query_blocks.append((query_grad * score_scale).astype(jnp.bfloat16))
        key_parts.append(
            jnp.einsum("hts,thd->shd", grad_low, query_block, preferred_element_type=jnp.float32)
        )
        value_parts.append(
            jnp.einsum("hts,thd->shd", probs_low, grad_block, preferred_element_type=jnp.float32)
        )
    grad_keys_rows = []
    grad_values_rows = []
    column_rows = []
    for block_index in range(BLOCKS):
        row_low = block_index * block_rows
        row_high = row_low + block_rows
        key_total = key_parts[block_index][row_low:row_high]
        value_total = value_parts[block_index][row_low:row_high]
        column_total = column_parts[block_index][:, row_low:row_high]
        for later_index in range(block_index + 1, BLOCKS):
            key_total = key_total + key_parts[later_index][row_low:row_high]
            value_total = value_total + value_parts[later_index][row_low:row_high]
            column_total = column_total + column_parts[later_index][:, row_low:row_high]
        grad_keys_rows.append(key_total)
        grad_values_rows.append(value_total)
        column_rows.append(column_total)
    grad_keys = jnp.concatenate(grad_keys_rows, axis=0)
    grad_values = jnp.concatenate(grad_values_rows, axis=0)
    grad_cum = jnp.concatenate(row_parts, axis=1) - jnp.concatenate(column_rows, axis=1)
    grad_queries = jnp.concatenate(query_blocks, axis=0)
    key_terms = (grad_keys * score_scale).astype(jnp.bfloat16)
    return (grad_queries, key_terms, grad_values.astype(jnp.bfloat16), grad_cum)


def per_device(inputs, w_key, w_value, queries, cotangent, cum_gate):
    seq_count, positions, feature_count = inputs.shape
    flat_rows = inputs.reshape(seq_count * positions, feature_count)
    kv_width = w_key.shape[1]
    kv_heads = kv_width // HD
    query_width = queries.shape[2]
    group_size = query_width // HD // kv_heads
    key_whole, value_whole = side_by_side((w_key, w_value), "dp", 0, 1)
    key_proj = jnp.dot(flat_rows, key_whole, preferred_element_type=jnp.float32)
    value_proj = jnp.dot(flat_rows, value_whole, preferred_element_type=jnp.float32)

    def spread(projected):
        split_heads = projected.astype(jnp.bfloat16).reshape(seq_count, positions, kv_heads, HD)
        return jnp.repeat(split_heads, group_size, axis=2).reshape(
            seq_count, positions, query_width
        )

    head_queries, head_keys, head_values, head_grads = sent_together(
        (queries, spread(key_proj), spread(value_proj), cotangent), SP, 2, 1, 0
    )
    seq_length = head_queries.shape[1]
    head_count = head_queries.shape[2] // HD
    head_shape = (seq_count, seq_length, head_count, HD)
    query_four = head_queries.reshape(head_shape)
    key_four = head_keys.reshape(head_shape)
    value_four = head_values.reshape(head_shape)
    grad_four = head_grads.reshape(head_shape)
    results = [
        attend_sequence(query_four[0], key_four[0], value_four[0], grad_four[0], cum_gate[0])
    ]
    flat_shape = (seq_count, seq_length, head_count * HD)
    query_heads = jnp.stack([result[0] for result in results]).reshape(flat_shape)
    key_heads = jnp.stack([result[1] for result in results]).reshape(flat_shape)
    value_heads = jnp.stack([result[2] for result in results]).reshape(flat_shape)
    grad_cum = jnp.stack([result[3] for result in results])
    grad_queries, key_terms, value_terms = sent_together(
        (query_heads, key_heads, value_heads), SP, 1, 2, 0
    )

    def group_sum(terms):
        grouped = terms.reshape(seq_count * positions, kv_heads, group_size, HD).astype(jnp.float32)
        return (
            jnp.sum(grouped, axis=2).astype(jnp.bfloat16).reshape(seq_count * positions, kv_width)
        )

    grad_keys = group_sum(key_terms)
    grad_values = group_sum(value_terms)
    contract = (((1,), (1,)), ((), ()))
    back = lax.dot_general(
        grad_keys, key_whole, contract, preferred_element_type=jnp.float32
    ) + lax.dot_general(grad_values, value_whole, contract, preferred_element_type=jnp.float32)
    grad_input = back.astype(jnp.bfloat16).reshape(seq_count, positions, feature_count)
    grad_both = jnp.concatenate((grad_keys, grad_values), axis=1)
    token_contract = (((0,), (0,)), ((), ()))
    shares = lax.psum_scatter(
        lax.dot_general(
            flat_rows, grad_both, token_contract, preferred_element_type=jnp.float32
        ).astype(jnp.bfloat16),
        "dp",
        scatter_dimension=0,
        tiled=True,
    )
    summed = over_axes(shares, SP).astype(jnp.float32)
    return (grad_input, grad_queries, grad_cum, summed[:, :kv_width], summed[:, kv_width:])


def solution(mesh):
    split = Mesh(mesh.devices.reshape(8, 4, mesh.shape["dp"]), ("sp_0", "sp_1", "dp"))
    in_specs = (
        P("dp", SP, None),
        P("dp", None),
        P("dp", None),
        P("dp", SP, None),
        P("dp", SP, None),
        P("dp", SP, None),
    )
    out_specs = (
        P("dp", SP, None),
        P("dp", SP, None),
        P("dp", SP, None),
        P("dp", None),
        P("dp", None),
    )
    return jax.shard_map(
        per_device, mesh=split, in_specs=in_specs, out_specs=out_specs, check_vma=False
    )
```

profile of v0, /device:TPU:24, one launch (start us, length us, event | category | flops | bytes accessed | tf_op | source)
XLA Modules:
  0.0 570.7 jit_solution(13045218731493942836)
XLA Ops:
  7.2 1.6 pad_maximum_fusion.2
  8.8 1.3 copy.328
  10.2 1.3 copy.329
  11.5 45.4 %all-gather.2.cloned.1.call-done = bf16[2048,512]{1,0:T(8,128)(2,1)} async-done(((bf16[128,512]{1,0:T(8,128)(2,1)}), bf16[2048,512]{1,0:T(8,128)(2,1)}) %all-gather.2.cloned.1.call-update) | async-done | bytes 2097168 | tf_op jit(solution)/shard_map/all_gather | solution.py:17
  56.8 1.7 convolution_convert_fusion.1
  58.6 1.7 convolution_convert_fusion.2
  60.8 10.8 %copy.330 = bf16[4,128,2048]{1,0,2:T(4,128)(2,1)} copy(bf16[4,128,2048]{1,2,0:T(8,128)(2,1)S(1)} %pad_maximum_fusion) | data formatting | bytes 4194304 | tf_op jit(solution)/shard_map/concatenate | solution.py:23
  71.6 10.3 %all-to-all-start = ((bf16[4,128,2048]{1,0,2:T(4,128)(2,1)}), bf16[4,128,2048]{1,0,2:T(4,128)(2,1)S(1)}, u32[]{:S(2)}, u32[]{:S(2)}) async-start(bf16[4,128,2048]{1,0,2:T(4,128)(2,1)} %copy.330), calls=%async_computation | async-start | bytes 4194304 | tf_op jit(solution)/shard_map/all_to_all | solution.py:24
  99.4 32.8 %all-to-all-done = bf16[4,128,2048]{1,0,2:T(4,128)(2,1)S(1)} async-done(((bf16[4,128,2048]{1,0,2:T(4,128)(2,1)}), bf16[4,128,2048]{1,0,2:T(4,128)(2,1)S(1)}, u32[]{:S(2)}, u32[]{:S(2)}) %all-to-all-start) | async-done | bytes 2097184 | tf_op jit(solution)/shard_map/all_to_all | solution.py:24
  181.5 1.5 reshape.2810
  183.0 1.5 copy.342
  184.5 1.5 reshape.2811
  186.1 1.2 fusion.647
  187.5 1.8 convolution_bitcast_fusion.28
  189.9 1.5 fusion.610
  192.1 1.5 reshape.2812
  193.6 1.7 convolution_bitcast_fusion.26
  195.2 1.2 fusion.161
  196.4 2.6 fusion.609
  199.1 1.7 convolution_bitcast_fusion.24
  200.8 1.2 fusion.168
  220.2 1.9 fusion.611
  223.0 1.2 fusion.205
  241.5 1.2 fusion.604
  247.1 1.3 fusion.603
  253.0 1.3 fusion.602
  259.2 1.6 fusion.601
  265.9 1.4 fusion.600
  272.7 1.6 fusion.599
  275.4 1.3 fusion.635
  280.2 1.7 fusion.598
  283.1 1.3 fusion.634
  287.5 1.6 fusion.597
  290.4 1.4 fusion.633
  295.1 1.4 fusion.596
  300.6 4.7 copy.413
  305.4 7.2 %reshape.2838 = bf16[32,2,12288]{2,1,0:T(2,128)(2,1)} reshape(bf16[4096,3,64]{2,1,0:T(4,128)(2,1)} %bitcast.1465) | data formatting | bytes 3145728
  312.7 5.4 all-to-all-start.1
  318.3 38.9 %all-to-all-done.1 = bf16[32,2,12288]{2,1,0:T(2,128)(2,1)S(1)} async-done(((bf16[32,2,12288]{2,1,0:T(2,128)(2,1)}), bf16[32,2,12288]{2,1,0:T(2,128)(2,1)S(1)}, u32[]{:S(2)}, u32[]{:S(2)}) %all-to-all-start.1) | async-done | bytes 1572896 | tf_op jit(solution)/shard_map/all_to_all | solution.py:24
  357.2 4.8 reshape.2839
  361.9 4.3 copy.422
  368.1 2.5 copy.423
  372.7 52.2 %reduce-scatter.4.cloned.1.call-done = bf16[128,512]{1,0:T(8,128)(2,1)} async-done(((bf16[2048,512]{1,0:T(8,128)(2,1)}), bf16[128,512]{1,0:T(8,128)(2,1)}) %reduce-scatter.4.cloned.1.call-update) | async-done | bytes 131088
  424.9 1.7 copy.424
  426.6 1.7 fusion.218
  430.6 78.3 %all-reduce.3.cloned.1.call-done = bf16[128,512]{0,1:T(8,128)(2,1)} async-done(((bf16[128,512]{0,1:T(8,128)(2,1)}), bf16[128,512]{0,1:T(8,128)(2,1)}) %all-reduce.3.cloned.1.call-update) | async-done | bytes 131088 | tf_op jit(solution)/shard_map/psum | solution.py:29
  508.9 2.5 fusion.62
  511.4 49.9 %all-reduce.5.cloned.1.call-done = bf16[128,512]{0,1:T(8,128)(2,1)} async-done(((bf16[128,512]{0,1:T(8,128)(2,1)}), bf16[128,512]{0,1:T(8,128)(2,1)}) %all-reduce.5.cloned.1.call-update) | async-done | bytes 131088 | tf_op jit(solution)/shard_map/psum | solution.py:29
  (671 shorter events, 153.9 us)
Async XLA Ops:
  7.2 49.7 %copy-start = (bf16[1,128,2048]{2,1,0:T(8,128)(2,1)S(1)}, bf16[1,128,2048]{2,1,0:T(8,128)(2,1)}, u32[]{:S(2)}) copy-start(bf16[1,128,2048]{2,1,0:T(8,128)(2,1)} %param.6) | copy-start | bytes 1572868
  7.2 49.7 %all-gather.2.cloned.1.call-start = ((), (), s32[]{:S(2)}) async-start(), calls=%async_computation.3 | async-start | bytes 2228224 | tf_op jit(solution)/shard_map/all_gather | solution.py:17
  71.6 10.3 %copy-start.22 = (f32[1,1,4096]{2,1,0:T(1,128)S(1)}, f32[1,1,4096]{2,1,0:T(1,128)}, u32[]{:S(2)}) copy-start(f32[1,1,4096]{2,1,0:T(1,128)} %param.11) | copy-start | bytes 49156
  71.6 60.7 %all-to-all-start = ((bf16[4,128,2048]{1,0,2:T(4,128)(2,1)}), bf16[4,128,2048]{1,0,2:T(4,128)(2,1)S(1)}, u32[]{:S(2)}, u32[]{:S(2)}) async-start(bf16[4,128,2048]{1,0,2:T(4,128)(2,1)} %copy.330), calls=%async_computation | async-start | bytes 4194304 | tf_op jit(solution)/shard_map/all_to_all | solution.py:24
  135.1 11.7 %copy-start.148 = (f32[1,256]{1,0:T(1,128)S(1)}, f32[1,256]{1,0:T(1,128)}, u32[]{:S(2)}) copy-start(f32[1,256]{1,0:T(1,128)} %get-tuple-element.166) | copy-start | bytes 3076
  137.2 31.4 %copy-start.33 = (bf16[1,6,128,64]{2,1,3,0:T(8,128)(2,1)}, bf16[1,6,128,64]{2,1,3,0:T(8,128)(2,1)S(1)}, u32[]{:S(2)}) copy-start(bf16[1,6,128,64]{2,1,3,0:T(8,128)(2,1)S(1)} %copy.343) | copy-start | bytes 294916
  138.1 39.4 %copy-start.31 = (bf16[1,8,128,64]{2,1,3,0:T(8,128)(2,1)}, bf16[1,8,128,64]{2,1,3,0:T(8,128)(2,1)S(1)}, u32[]{:S(2)}) copy-start(bf16[1,8,128,64]{2,1,3,0:T(8,128)(2,1)S(1)} %copy.348) | copy-start | bytes 393220
  145.3 32.2 %copy-start.83 = (bf16[1,2,128,64]{2,1,3,0:T(2,128)(2,1)}, bf16[1,2,128,64]{2,1,3,0:T(2,128)(2,1)S(1)}, u32[]{:S(2)}) copy-start(bf16[1,2,128,64]{2,1,3,0:T(2,128)(2,1)S(1)} %copy.349) | copy-start | bytes 98308
  146.0 22.6 %copy-start.84 = (bf16[1,2,128,64]{2,1,3,0:T(2,128)(2,1)}, bf16[1,2,128,64]{2,1,3,0:T(2,128)(2,1)S(1)}, u32[]{:S(2)}) copy-start(bf16[1,2,128,64]{2,1,3,0:T(2,128)(2,1)S(1)} %copy.344) | copy-start | bytes 98308
  146.7 5.9 %copy-start.76 = (bf16[1,2,128,64]{2,1,3,0:T(2,128)(2,1)}, bf16[1,2,128,64]{2,1,3,0:T(2,128)(2,1)S(1)}, u32[]{:S(2)}) copy-start(bf16[1,2,128,64]{2,1,3,0:T(2,128)(2,1)S(1)} %copy.333) | copy-start | bytes 98308
  146.7 5.8 %copy-start.86 = (bf16[1,2,128,64]{2,1,3,0:T(2,128)(2,1)}, bf16[1,2,128,64]{2,1,3,0:T(2,128)(2,1)S(1)}, u32[]{:S(2)}) copy-start(bf16[1,2,128,64]{2,1,3,0:T(2,128)(2,1)S(1)} %copy.332) | copy-start | bytes 98308
  147.0 6.8 %copy-start.23 = (f32[256,256]{0,1:T(8,128)}, f32[256,256]{0,1:T(8,128)S(1)}, u32[]{:S(2)}) copy-start(f32[256,256]{0,1:T(8,128)S(1)} %get-tuple-element.168) | copy-start | bytes 786436
  147.0 6.8 %copy-start.117 = (f32[256]{0:T(256)}, f32[256]{0:T(256)S(1)}, u32[]{:S(2)}) copy-start(f32[256]{0:T(256)S(1)} %get-tuple-element.167) | copy-start | bytes 3076
  147.1 9.3 %copy-start.118 = (f32[256]{0:T(256)}, f32[256]{0:T(256)S(1)}, u32[]{:S(2)}) copy-start(f32[256]{0:T(256)S(1)} %fusion.339) | copy-start | bytes 3076
  153.2 15.4 %copy-start.126 = (f32[768]{0:T(1024)S(1)}, f32[768]{0:T(1024)}, u32[]{:S(2)}) copy-start(f32[768]{0:T(1024)} %slice_reduce_fusion.9) | copy-start | bytes 9220
  153.2 15.4 %copy-start.147 = (f32[1,256]{1,0:T(1,128)S(1)}, f32[1,256]{1,0:T(1,128)}, u32[]{:S(2)}) copy-start(f32[1,256]{1,0:T(1,128)} %get-tuple-element.165) | copy-start | bytes 3076
  153.2 15.4 %copy-start.164 = (s32[256]{0:T(256)S(1)}, s32[256]{0:T(256)}, u32[]{:S(2)}) copy-start(s32[256]{0:T(256)} %iota_add_fusion.13) | copy-start | bytes 3076
  193.6 5.4 copy-start.62
  199.1 4.0 copy-start.61
  203.1 11.7 %copy-start.60 = (f32[1,2,128,64]{2,3,1,0:T(8,128)S(1)}, f32[1,2,128,64]{2,3,1,0:T(8,128)}, u32[]{:S(2)}) copy-start(f32[1,2,128,64]{2,3,1,0:T(8,128)} %get-tuple-element.82) | copy-start | bytes 196612
  203.1 12.5 %copy-start.59 = (f32[1,2,128,64]{2,3,1,0:T(8,128)S(1)}, f32[1,2,128,64]{2,3,1,0:T(8,128)}, u32[]{:S(2)}) copy-start(f32[1,2,128,64]{2,3,1,0:T(8,128)} %get-tuple-element.83) | copy-start | bytes 196612
  203.1 13.2 %copy-start.58 = (f32[1,2,128,64]{2,3,1,0:T(8,128)S(1)}, f32[1,2,128,64]{2,3,1,0:T(8,128)}, u32[]{:S(2)}) copy-start(f32[1,2,128,64]{2,3,1,0:T(8,128)} %get-tuple-element.84) | copy-start | bytes 196612
  203.1 13.9 %copy-start.57 = (f32[1,2,128,64]{2,3,1,0:T(8,128)S(1)}, f32[1,2,128,64]{2,3,1,0:T(8,128)}, u32[]{:S(2)}) copy-start(f32[1,2,128,64]{2,3,1,0:T(8,128)} %get-tuple-element.85) | copy-start | bytes 196612
  203.1 14.6 %copy-start.24 = (bf16[256,512]{1,0:T(8,128)(2,1)S(1)}, bf16[256,512]{1,0:T(8,128)(2,1)}, u32[]{:S(2)}) copy-start(bf16[256,512]{1,0:T(8,128)(2,1)} %get-tuple-element.200) | copy-start | bytes 786436
  203.1 14.6 %copy-start.87 = (bf16[1,2,128,64]{2,1,3,0:T(2,128)(2,1)S(1)}, bf16[1,2,128,64]{2,1,3,0:T(2,128)(2,1)}, u32[]{:S(2)}) copy-start(bf16[1,2,128,64]{2,1,3,0:T(2,128)(2,1)} %copy.339) | copy-start | bytes 98308
  203.1 14.8 %copy-start.4 = (bf16[256,768]{1,0:T(8,128)(2,1)S(1)}, bf16[256,768]{1,0:T(8,128)(2,1)}, u32[]{:S(2)}) copy-start(bf16[256,768]{1,0:T(8,128)(2,1)} %get-tuple-element.201) | copy-start | bytes 1179652
  203.1 14.8 %copy-start.85 = (bf16[1,2,128,64]{2,1,3,0:T(2,128)(2,1)S(1)}, bf16[1,2,128,64]{2,1,3,0:T(2,128)(2,1)}, u32[]{:S(2)}) copy-start(bf16[1,2,128,64]{2,1,3,0:T(2,128)(2,1)} %copy-done.84) | copy-start | bytes 98308
  217.7 6.5 %copy-start.34 = (bf16[1,6,128,64]{2,1,3,0:T(8,128)(2,1)S(1)}, bf16[1,6,128,64]{2,1,3,0:T(8,128)(2,1)}, u32[]{:S(2)}) copy-start(bf16[1,6,128,64]{2,1,3,0:T(8,128)(2,1)} %copy-done.33) | copy-start | bytes 294916
  217.9 6.6 %copy-start.32 = (bf16[1,8,128,64]{2,1,3,0:T(8,128)(2,1)S(1)}, bf16[1,8,128,64]{2,1,3,0:T(8,128)(2,1)}, u32[]{:S(2)}) copy-start(bf16[1,8,128,64]{2,1,3,0:T(8,128)(2,1)} %copy-done.31) | copy-start | bytes 393220
  218.1 6.7 %copy-start.10 = (bf16[1,32,128,64]{2,3,1,0:T(8,128)(2,1)S(1)}, bf16[1,32,128,64]{2,3,1,0:T(8,128)(2,1)}, u32[]{:S(2)}) copy-start(bf16[1,32,128,64]{2,3,1,0:T(8,128)(2,1)} %get-tuple-element.117) | copy-start | bytes 1572868
  220.2 5.0 copy-start.30
  220.2 5.0 copy-start.81
  220.2 5.0 copy-start.114
  220.2 5.0 copy-start.145
  220.2 5.0 copy-start.162
  312.6 5.5 copy-start.150
  312.6 5.5 copy-start.149
  312.6 5.5 copy-start.119
  312.6 5.5 copy-start.128
  312.6 5.6 copy-start.115
  312.6 5.6 copy-start.120
  312.6 5.6 copy-start.116
  312.7 5.6 copy-start.121
  312.7 5.6 copy-start.129
  312.7 44.5 %all-to-all-start.1 = ((bf16[32,2,12288]{2,1,0:T(2,128)(2,1)}), bf16[32,2,12288]{2,1,0:T(2,128)(2,1)S(1)}, u32[]{:S(2)}, u32[]{:S(2)}) async-start(bf16[32,2,12288]{2,1,0:T(2,128)(2,1)} %reshape.2838), calls=%async_computation.1 | async-start | bytes 3145728 | tf_op jit(solution)/shard_map/all_to_all | solution.py:24
  318.0 106.8 %reduce-scatter.4.cloned.1.call-start = ((), (), s32[]{:S(2)}) async-start(), calls=%async_computation.6 | async-start | bytes 2228224
  370.9 138.0 %all-reduce.3.cloned.1.call-start = ((), (), s32[]{:S(2)}) async-start(), calls=%async_computation.4 | async-start | bytes 262144 | tf_op jit(solution)/shard_map/psum | solution.py:29
  426.6 134.7 %all-reduce.5.cloned.1.call-start = ((), (), s32[]{:S(2)}) async-start(), calls=%async_computation.5 | async-start | bytes 262144 | tf_op jit(solution)/shard_map/psum | solution.py:29
  (123 other events, 149.7 us)
Sparse Core Ops, SparseCore 0:
  10.7 46.1 all-gather.1
  371.0 53.8 reduce-scatter.3
  427.8 81.0 all-reduce.2
  511.1 50.2 all-reduce.4
where the time goes:
time: 579 us; the launch traced here: 571 us
  waiting for transfers between devices  298 us (51%)
  local copies, waits for them, and re-layouts  129 us (22%)
  matrix products  82 us (14%)
  other arithmetic  29.7 us (5%)
  between operations  16.7 us (3%)
  starting transfers between devices  15.8 us (3%)
    psum x2, waiting for transfers between devices, over_axes(): return functools.reduce(lax.psum, axes, x)  128 us
    all_to_all x2, waiting for transfers between devices, sent_together(): lax.all_to_all(both, axis, split_axis=split_dim, concat_axis=concat_dim,...  71.7 us
    unnamed x5, waiting for transfers between devices  52.3 us
    all_gather x1, waiting for transfers between devices, side_by_side(): result = lax.all_gather(both, axis, axis=dim, tiled=True)  45.4 us
    unnamed x354, local copies, waits for them, and re-layouts  30 us
    dot_general x16, matrix products, attend_sequence(): jnp.einsum('thd,shd->hts', grad_block, value_prefix, preferred_element_ty...  23.5 us
    convert_element_type x32, local copies, waits for them, and re-layouts, attend_sequence(): row_dot = jnp.sum(grad_block.astype(jnp.float32) * outputs, axis=2).T  22 us
    all_to_all x2, starting transfers between devices, sent_together(): lax.all_to_all(both, axis, split_axis=split_dim, concat_axis=concat_dim,...  15.7 us
  transfers between devices with their start and end apart: 6, of which 6 were waited for; matrix products, arithmetic and copies ran while one was open for 5% of the time, Pallas kernels for 0%

commit v1 on v0

v1 whole, which is shorter than its diff:
```python
import functools

import jax
import jax.numpy as jnp
from jax import lax
from jax.experimental import pallas as pl
from jax.experimental.pallas import tpu as pltpu
from jax.sharding import Mesh
from jax.sharding import PartitionSpec as P


HD = 64
LANES = 128
LOG2E = 1.4426950408889634
BLOCK = 512
ONES = HD + 16
SP = ("zg", "zp", "x")
GROUP = ("zp", "x")
bf16 = jnp.bfloat16
f32 = jnp.float32
VMEM = pltpu.VMEM


def dot(a, b, ca, cb):
    return lax.dot_general(a, b, (((ca,), (cb,)), ((), ())), preferred_element_type=f32)


def low_half(rows):
    return lax.broadcasted_iota(jnp.int32, (rows, LANES), 1) < HD


def merge_pair(a, b):
    low = low_half(a.shape[0])
    return jnp.where(low, a, pltpu.roll(b, HD, 1)), jnp.where(low, pltpu.roll(a, HD, 1), b)


def pieces(value):
    first = value.astype(bf16).astype(f32)
    rest = value - first
    second = rest.astype(bf16).astype(f32)
    third = (rest - second).astype(bf16).astype(f32)
    return first, second, third


def call(kernel, out_shapes, *args, scratch=(), vmem=60):
    many = isinstance(out_shapes, tuple)
    specs = pl.BlockSpec(memory_space=VMEM)
    return pl.pallas_call(
        kernel,
        out_shape=out_shapes,
        in_specs=[
            pl.BlockSpec(memory_space=pltpu.SMEM) if arg.dtype == jnp.int32 else specs
            for arg in args
        ],
        out_specs=(specs,) * len(out_shapes) if many else specs,
        scratch_shapes=scratch,
        compiler_params=pltpu.CompilerParams(vmem_limit_bytes=vmem * 1024 * 1024),
    )(*args)


def shape(dims, dtype=bf16):
    return jax.ShapeDtypeStruct(dims, dtype)


def pack_weights_kernel(key_ref, value_ref, out_ref):
    for pair in range(key_ref.shape[1] // LANES):
        at = slice(pair * LANES, (pair + 1) * LANES)
        first, second = merge_pair(key_ref[:, at].astype(f32), value_ref[:, at].astype(f32))
        out_ref[:, 2 * pair * LANES : (2 * pair + 1) * LANES] = first.astype(bf16)
        out_ref[:, (2 * pair + 1) * LANES : (2 * pair + 2) * LANES] = second.astype(bf16)


def pack_queries_kernel(query_ref, grad_ref, out_ref):
    for pair in range(query_ref.shape[1] // LANES):
        at = slice(pair * LANES, (pair + 1) * LANES)
        first, second = merge_pair(query_ref[:, at].astype(f32), grad_ref[:, at].astype(f32))
        out_ref[2 * pair] = first.astype(bf16)
        out_ref[2 * pair + 1] = second.astype(bf16)


def project_kernel(rows_ref, weight_ref, out_ref, *, group):
    projected = dot(rows_ref[...], weight_ref[...], 1, 0).astype(bf16)
    for head in range(out_ref.shape[0]):
        g = head // group
        out_ref[head] = projected[:, g * LANES : (g + 1) * LANES]


def attend_kernel(
    x_ref, kv_ref, cum_ref, dq_ref, dkv_ref, gcum_ref,
    qa_ref, ka_ref, kn_ref, s_ref, dp_ref, xt_ref, dkt_ref, dvt_ref, rows_ref, acc_ref,
    *, blk, seq, members,
):
    count = seq // blk
    scale = HD**-0.5
    lane = lax.broadcasted_iota(jnp.int32, (blk, LANES), 1)
    low = lane < HD
    row_id = lax.broadcasted_iota(jnp.int32, (LANES, blk), 0)

    def prepare(i, _):
        at = pl.ds(pl.multiple_of(i * blk, blk), blk)
        x = x_ref[at, :].astype(f32)
        kv = kv_ref[at, :].astype(f32)
        c1, c2, c3 = pieces(jnp.broadcast_to(cum_ref[:, at] * LOG2E, (LANES, blk)))
        one = jnp.ones_like(c1)

        def extra(values):
            total = jnp.zeros_like(c1)
            for k, value in enumerate(values):
                total = jnp.where(row_id == HD + k, value, total)
            return total.T

        q1, q2, q3 = pieces(x * (LOG2E * scale))
        qa_ref[at, 0:LANES] = jnp.where(low, q1, pltpu.roll(q2, HD, 1)).astype(bf16)
        qa_ref[at, LANES:] = jnp.where(low, q3, extra((c1, c2, c3, one, one, one))).astype(bf16)
        ka_ref[at, 0:LANES] = jnp.where(low, kv, pltpu.roll(kv, HD, 1)).astype(bf16)
        ka_ref[at, LANES:] = jnp.where(low, kv, extra((one, one, one, -c1, -c2, -c3))).astype(bf16)
        kn_ref[at, :] = jnp.where(low, kv, jnp.where(lane == HD, 1.0, 0.0)).astype(bf16)
        xt = x.T
        ones_row = jnp.where(row_id == HD, 1.0, 0.0)
        xt_ref[0:ONES, at] = jnp.where(row_id < HD, xt, ones_row)[0:ONES].astype(bf16)
        xt_ref[ONES:, at] = xt[HD:].astype(bf16)
        dkt_ref[:, at] = jnp.zeros((ONES, blk), f32)
        dvt_ref[:, at] = jnp.zeros((HD, blk), f32)
        return 0

    lax.fori_loop(0, count, prepare, 0)

    def fold(block, op):
        result = block[:, 0:LANES]
        for k in range(1, blk // LANES):
            result = op(result, block[:, k * LANES : (k + 1) * LANES])
        return result

    def query_block(i, _):
        rows = pl.ds(pl.multiple_of(i * blk, blk), blk)
        qa = qa_ref[rows, :]
        x = x_ref[rows, :]
        grad = jnp.where(low, jnp.zeros_like(x), x)

        def score(j):
            at = pl.ds(pl.multiple_of(j * blk, blk), blk)
            scores = dot(qa, ka_ref[at, :], 1, 1)
            dp_ref[:, at] = dot(grad, kv_ref[at, :], 1, 1)
            return scores, at

        def full_block(j, best):
            scores, at = score(j)
            s_ref[:, at] = scores
            return jnp.maximum(best, fold(scores, jnp.maximum))

        scores, at = score(i)
        sub = lax.broadcasted_iota(jnp.int32, (blk, blk), 0)
        col = lax.broadcasted_iota(jnp.int32, (blk, blk), 1)
        scores = jnp.where(col <= sub, scores, -jnp.inf)
        s_ref[:, at] = scores
        best = lax.fori_loop(0, i, full_block, fold(scores, jnp.maximum))
        best = jnp.max(best, axis=1, keepdims=True)

        def exponentials(j, carry):
            total, weighted = carry
            at = pl.ds(pl.multiple_of(j * blk, blk), blk)
            e = jnp.exp2(s_ref[:, at] - best)
            s_ref[:, at] = e
            return total + fold(e, jnp.add), weighted + fold(e * dp_ref[:, at], jnp.add)

        zero = jnp.zeros((blk, LANES), f32)
        total, weighted = lax.fori_loop(0, i + 1, exponentials, (zero, zero))
        inverse = 1.0 / jnp.sum(total, axis=1, keepdims=True)
        row_dot = jnp.sum(weighted, axis=1, keepdims=True) * inverse
        acc_ref[...] = zero

        def gradients(j, _):
            at = pl.ds(pl.multiple_of(j * blk, blk), blk)
            probs = s_ref[:, at] * inverse
            grad_low = (probs * (dp_ref[:, at] - row_dot)).astype(bf16)
            probs_low = probs.astype(bf16)
            acc_ref[...] += dot(grad_low, kn_ref[at, :], 1, 0)
            dkt_ref[:, at] += dot(xt_ref[0:ONES, rows], grad_low, 1, 0)
            dvt_ref[:, at] += dot(xt_ref[ONES:, rows], probs_low, 1, 0)
            return 0

        lax.fori_loop(0, i + 1, gradients, 0)
        dq = acc_ref[...]
        rows_ref[:, rows] = dq.T[HD : HD + 8]
        dq = dq * scale
        for b in range(blk // LANES):
            top = dq[b * LANES : b * LANES + HD]
            bottom = dq[b * LANES + HD : (b + 1) * LANES]
            packed = jnp.where(low[0:HD], top, pltpu.roll(bottom, HD, 1))
            dq_ref[i * (blk // LANES) + b] = packed.astype(bf16)
        return 0

    lax.fori_loop(0, count, query_block, 0)
    for b in range(seq // LANES):
        at = slice(b * LANES, (b + 1) * LANES)
        dkv_ref[b % members, b // members, 0:HD, :] = (dkt_ref[0:HD, at] * scale).astype(bf16)
        dkv_ref[b % members, b // members, HD:, :] = dvt_ref[:, at].astype(bf16)
    gcum_ref[...] = rows_ref[0:1, :] - dkt_ref[HD : HD + 1, :]


def attend(x, kv, cum, members):
    seq = x.shape[0]
    owners = seq // LANES
    return call(
        functools.partial(attend_kernel, blk=BLOCK, seq=seq, members=members),
        (
            shape((owners, HD, LANES)),
            shape((members, owners // members, LANES, LANES)),
            shape((1, seq), f32),
        ),
        x, kv, cum,
        scratch=[
            VMEM((seq, 2 * LANES), bf16),
            VMEM((seq, 2 * LANES), bf16),
            VMEM((seq, LANES), bf16),
            VMEM((BLOCK, seq), f32),
            VMEM((BLOCK, seq), f32),
            VMEM((ONES + HD, seq), bf16),
            VMEM((ONES, seq), f32),
            VMEM((HD, seq), f32),
            VMEM((8, seq), f32),
            VMEM((BLOCK, LANES), f32),
        ],
    )


def group_sum_kernel(me_ref, terms_ref, *refs):
    owners = terms_ref.shape[1]
    rows_refs, sums_refs, part_ref = refs[:owners], refs[owners : 2 * owners], refs[2 * owners]
    part = None
    for k in range(owners):
        owner = lax.rem(me_ref[0] + k, owners)
        total = terms_ref[0, owner].astype(f32)
        for member in range(1, terms_ref.shape[0]):
            total = total + terms_ref[member, owner].astype(f32)
        low = total.astype(bf16)
        sums_refs[k][...] = low
        product = dot(low, rows_refs[(owners - k) % owners][...], 1, 0)
        part = product if part is None else part + product
    for chunk in range(part_ref.shape[0]):
        part_ref[chunk] = part[:, chunk * LANES : (chunk + 1) * LANES].astype(bf16)


def unpack_queries_kernel(packed_ref, out_ref):
    for pair in range(packed_ref.shape[0] // 2):
        top, bottom = merge_pair(
            packed_ref[2 * pair].astype(f32), packed_ref[2 * pair + 1].astype(f32)
        )
        at = slice(pair * LANES, (pair + 1) * LANES)
        out_ref[0:HD, at] = top.astype(bf16)
        out_ref[HD:, at] = bottom.astype(bf16)


def grad_input_kernel(me_ref, weight_ref, *refs):
    sums_refs, out_ref = refs[:-1], refs[-1]
    groups = len(sums_refs)
    total = None
    for k in range(groups):
        g = lax.rem(me_ref[0] + groups - k, groups)
        columns = pl.ds(pl.multiple_of(g * LANES, LANES), LANES)
        product = dot(sums_refs[k][...], weight_ref[:, columns], 0, 1)
        total = product if total is None else total + product
    out_ref[...] = total.astype(bf16)


def sum_parts_kernel(parts_ref, out_ref):
    total = parts_ref[0].astype(f32)
    for k in range(1, parts_ref.shape[0]):
        total = total + parts_ref[k].astype(f32)
    out_ref[...] = total.astype(bf16)


def sum_ring_kernel(me_ref, *refs):
    parts, out_ref, held_ref = refs[:-2], refs[-2], refs[-1]
    count = len(parts)
    for k in range(count):
        held_ref[lax.rem(me_ref[0] + count - k, count)] = parts[k][...].astype(f32)
    total = held_ref[0]
    for k in range(1, count):
        total = total + held_ref[k]
    out_ref[...] = total.astype(bf16)


def finish_kernel(me_ref, *refs):
    parts, (key_ref, value_ref, held_ref) = refs[:-3], refs[-3:]
    count = len(parts)
    for k in range(count):
        held_ref[lax.rem(me_ref[0] + count - k, count)] = parts[k][...].astype(f32).T
    for pair in range(count // 2):
        at = slice(pair * LANES, (pair + 1) * LANES)
        keys, values = merge_pair(held_ref[2 * pair], held_ref[2 * pair + 1])
        key_ref[:, at] = keys
        value_ref[:, at] = values


def exchange(x, axes):
    return lax.all_to_all(x, axes, split_axis=0, concat_axis=0, tiled=True)


def shift(x, axis, size, by):
    return lax.ppermute(x, axis, [(k, (k + by) % size) for k in range(size)])


def per_device(inputs, w_key, w_value, queries, cotangent, cum_gate, **sizes):
    return program(inputs, w_key, w_value, queries, cotangent, cum_gate, **sizes)


def program(inputs, w_key, w_value, queries, cotangent, cum_gate, *, heads, dp, zg, zp, xs):
    _, positions, features = inputs.shape
    kv_width = w_key.shape[1]
    kv_heads = kv_width // HD
    owners, members = zg, zp * xs
    rows = inputs.reshape(positions, features)
    width = 2 * kv_width
    block = shape((LANES, LANES))
    me = {axis: lax.axis_index(axis).astype(jnp.int32).reshape(1) for axis in SP}

    weight = call(pack_weights_kernel, shape((w_key.shape[0], width)), w_key, w_value)
    weight = lax.all_gather(weight, "dp", axis=0, tiled=True)
    packed = call(
        pack_queries_kernel, shape((heads, positions, LANES)),
        queries.reshape(positions, -1), cotangent.reshape(positions, -1),
    )
    head_rows = exchange(packed, SP).reshape(heads * positions, LANES)
    projected = call(
        functools.partial(project_kernel, group=heads // kv_heads),
        shape((heads, positions, LANES)), rows, weight,
    )
    head_kv = exchange(projected, SP).reshape(heads * positions, LANES)
    head_kv, late_rows = lax.optimization_barrier((head_kv, rows))
    near_rows = [late_rows] + [shift(late_rows, "zg", zg, k) for k in range(1, zg)]

    dq, dkv, grad_cum = attend(head_rows, head_kv, cum_gate[0], members)
    terms = exchange(dkv, GROUP)
    *sums, part = call(
        group_sum_kernel,
        (*[shape((LANES, positions))] * owners, shape((dp, LANES, LANES))),
        me["zg"], terms, *near_rows,
    )
    parts = exchange(part, "dp")
    own_sums = [sums[0]] + [shift(sums[k], "zg", zg, k) for k in range(1, zg)]
    grad_input = call(grad_input_kernel, shape((positions, features)), me["zg"], weight, *own_sums)
    summed = call(sum_parts_kernel, block, parts)
    query_parts = exchange(dq, SP)
    grad_queries = call(unpack_queries_kernel, shape((positions, features)), query_parts)

    def held(count):
        return [VMEM((count, LANES, LANES), f32)]

    along = [summed] + [shift(summed, "x", xs, k) for k in range(1, xs)]
    summed = call(sum_ring_kernel, block, me["x"], *along, scratch=held(xs))
    along = [summed] + [shift(summed, "zp", zp, k) for k in range(1, zp)]
    summed = call(sum_ring_kernel, block, me["zp"], *along, scratch=held(zp))
    along = [summed] + [shift(summed, "zg", zg, k) for k in range(1, zg)]
    half = shape((LANES, kv_width), f32)
    grad_key, grad_value = call(finish_kernel, (half, half), me["zg"], *along, scratch=held(zg))
    return grad_input[None], grad_queries[None], grad_cum[None], grad_key, grad_value


def solution(mesh):
    sizes = {"heads": mesh.shape["sp"], "dp": mesh.shape["dp"], "zg": 4, "zp": 2, "xs": 4}
    split = Mesh(
        mesh.devices.reshape(sizes["zg"], sizes["zp"], sizes["xs"], sizes["dp"]),
        ("zg", "zp", "x", "dp"),
    )
    rows = P("dp", SP, None)
    weights = P("dp", None)
    return jax.shard_map(
        functools.partial(per_device, **sizes),
        mesh=split,
        in_specs=(rows, weights, weights, rows, rows, rows),
        out_specs=(rows, rows, rows, weights, weights),
        check_vma=False,
    )
```

time: 579 us -> 347 us (0.60)
  the two profiles are of different devices: /device:TPU:24 before, /device:TPU:6 now
where the time goes in v1:
time: 347 us; the launch traced here: 345 us
  waiting for transfers between devices  147 us (42%)
  starting transfers between devices  82.1 us (24%)
  Pallas kernels  75.3 us (22%)
  blocking collectives  20.7 us (6%)
  between operations  14.3 us (4%)
  local copies, waits for them, and re-layouts  6.08 us (2%)
    pallas_call x11, Pallas kernels, call(): pl.pallas_call(kernel, out_shape=out_shapes, in_specs=[pl.BlockSpec(memor...  75.3 us
    all_to_all x4, waiting for transfers between devices, exchange(): return lax.all_to_all(x, axes, split_axis=0, concat_axis=0, tiled=True)  53 us
    ppermute x13, starting transfers between devices, shift(): return lax.ppermute(x, axis, [(k, (k + by) % size) for k in range(size)])  49.2 us
    all_gather x1, waiting for transfers between devices, program(): weight = lax.all_gather(weight, 'dp', axis=0, tiled=True)  48.2 us
    ppermute x13, waiting for transfers between devices, shift(): return lax.ppermute(x, axis, [(k, (k + by) % size) for k in range(size)])  45.6 us
    all_to_all x4, starting transfers between devices, exchange(): return lax.all_to_all(x, axes, split_axis=0, concat_axis=0, tiled=True)  32.8 us
    all_to_all x1, blocking collectives, exchange(): return lax.all_to_all(x, axes, split_axis=0, concat_axis=0, tiled=True)  20.7 us
  transfers between devices with their start and end apart: 18, of which 7 were waited for; matrix products, arithmetic and copies ran while one was open for 0% of the time, Pallas kernels for 4%

profile of v1, /device:TPU:6, one launch (start us, length us, event | category | flops | bytes accessed | tf_op | source)
XLA Modules:
  0.0 345.2 jit_solution(17285453544063078411)
XLA Ops:
  7.2 0.0 all-gather.2.cloned.1.call-start
  7.2 1.6 shard_map.101
  8.8 0.0 all-gather.2.cloned.1.call-update
  8.9 48.2 %all-gather.2.cloned.1.call-done.weight_ref = bf16[2048,512]{1,0:T(8,128)(2,1)} async-done(((bf16[128,512]{1,0:T(8,128)(2,1)}), bf16[2048,512]{1,0:T(8,128)(2,1)}) %all-gather.2.cloned.1.call-update) | async-done | bytes 2097168 | tf_op jit(solution)/shard_map/all_gather | solution.py:319
  57.1 3.3 shard_map.103
  60.4 10.5 %all-to-all-start.1 = ((bf16[32,128,128]{2,1,0:T(8,128)(2,1)}), bf16[32,128,128]{2,1,0:T(8,128)(2,1)S(1)}, u32[]{:S(2)}, u32[]{:S(2)}) async-start(bf16[32,128,128]{2,1,0:T(8,128)(2,1)} %shard_map.103), calls=%async_computation.1 | async-start | bytes 2097152 | tf_op jit(solution)/shard_map/all_to_all | solution.py:297
  70.9 2.6 shard_map.102
  73.4 25.9 %all-to-all-done.1 = bf16[32,128,128]{2,1,0:T(8,128)(2,1)S(1)} async-done(((bf16[32,128,128]{2,1,0:T(8,128)(2,1)}), bf16[32,128,128]{2,1,0:T(8,128)(2,1)S(1)}, u32[]{:S(2)}, u32[]{:S(2)}) %all-to-all-start.1) | async-done | bytes 1048608 | tf_op jit(solution)/shard_map/all_to_all | solution.py:297
  99.3 5.6 %all-to-all-start = ((bf16[32,128,128]{2,1,0:T(8,128)(2,1)}), bf16[32,128,128]{2,1,0:T(8,128)(2,1)S(1)}, u32[]{:S(2)}, u32[]{:S(2)}) async-start(bf16[32,128,128]{2,1,0:T(8,128)(2,1)} %shard_map.102), calls=%async_computation | async-start | bytes 2097152 | tf_op jit(solution)/shard_map/all_to_all | solution.py:297
  104.9 27.1 %all-to-all-done = bf16[32,128,128]{2,1,0:T(8,128)(2,1)S(1)} async-done(((bf16[32,128,128]{2,1,0:T(8,128)(2,1)}), bf16[32,128,128]{2,1,0:T(8,128)(2,1)S(1)}, u32[]{:S(2)}, u32[]{:S(2)}) %all-to-all-start) | async-done | bytes 1048608 | tf_op jit(solution)/shard_map/all_to_all | solution.py:297
  132.0 1.0 copy-done.2
  133.0 52.9 %shard_map.104 = (bf16[32,64,128]{2,1,0:T(8,128)(2,1)}, bf16[8,4,128,128]{3,2,1,0:T(8,128)(2,1)}, f32[1,4096]{1,0:T(1,128)}) custom-call(bf16[4096,128]{1,0:T(8,128)(2,1)} %bitcast.13, bf16[4096,128]{1,0:T(8,128)(2,1)} %bitcast.12, f32[1,4096]{1,0:T(1,128)} %bitcast.23), custom_call_target="tpu_custom_call" | custom-call | tf_op jit(solution)/shard_map/pallas_call | solution.py:48
  185.9 4.8 %all-to-all-start.2 = ((bf16[8,4,128,128]{3,2,1,0:T(8,128)(2,1)}), bf16[8,4,128,128]{3,2,1,0:T(8,128)(2,1)S(1)}, u32[]{:S(2)}, u32[]{:S(2)}) async-start(bf16[8,4,128,128]{3,2,1,0:T(8,128)(2,1)} %get-tuple-element.18), calls=%async_computation.2 | async-start | bytes 2097152 | tf_op jit(solution)/shard_map/all_to_all | solution.py:297
  190.7 3.6 %collective-permute-start = (bf16[128,2048]{1,0:T(8,128)(2,1)S(1)}, bf16[128,2048]{1,0:T(8,128)(2,1)S(1)}, u32[]{:S(2)}, u32[]{:S(2)}) collective-permute-start(bf16[128,2048]{1,0:T(8,128)(2,1)S(1)} %bitcast.16), channel_id=1, source_target_pairs={{0,128},{128,256},{256,384},{384,0},{1,129},{129,257},{257,385},{3... | collective-permute-start | bytes 1572872 | tf_op jit(solution)/shard_map/ppermute | solution.py:301
  194.3 3.1 collective-permute-start.1
  197.5 4.8 %collective-permute-start.2 = (bf16[128,2048]{1,0:T(8,128)(2,1)S(1)}, bf16[128,2048]{1,0:T(8,128)(2,1)S(1)}, u32[]{:S(2)}, u32[]{:S(2)}) collective-permute-start(bf16[128,2048]{1,0:T(8,128)(2,1)S(1)} %bitcast.18), channel_id=1, source_target_pairs={{0,384},{128,0},{256,128},{384,256},{1,385},{129,1},{257,129},{385... | collective-permute-start | bytes 1572872 | tf_op jit(solution)/shard_map/ppermute | solution.py:301
  202.3 27.1 %collective-permute-done.refs_1_ = bf16[128,2048]{1,0:T(8,128)(2,1)S(1)} collective-permute-done((bf16[128,2048]{1,0:T(8,128)(2,1)S(1)}, bf16[128,2048]{1,0:T(8,128)(2,1)S(1)}, u32[]{:S(2)}, u32[]{:S(2)}) %collective-permute-start) | collective-permute-done | bytes 524320 | tf_op jit(solution)/shard_map/ppermute | solution.py:301
  229.4 13.0 %collective-permute-done.1.refs_2_ = bf16[128,2048]{1,0:T(8,128)(2,1)S(1)} collective-permute-done((bf16[128,2048]{1,0:T(8,128)(2,1)S(1)}, bf16[128,2048]{1,0:T(8,128)(2,1)S(1)}, u32[]{:S(2)}, u32[]{:S(2)}) %collective-permute-start.1) | collective-permute-done | bytes 524320 | tf_op jit(solution)/shard_map/ppermute | solution.py:301
  242.4 0.8 copy-done.6
  243.2 0.2 copy-done.7
  243.4 0.3 copy-done
  243.7 3.3 shard_map.105
  247.1 20.7 %all_to_all.25.parts_ref = bf16[16,128,128]{2,1,0:T(8,128)(2,1)} all-to-all(bf16[16,128,128]{2,1,0:T(8,128)(2,1)} %get-tuple-element.26), channel_id=1, replica_groups=mesh['zg'=4,'zp'=2,'x'=4,'dp'=16] {'dp'}, dimensions={0} | all-to-all | bytes 1048576 | tf_op jit(solution)/shard_map/all_to_all | solution.py:297
  267.8 11.9 %all-to-all-start.3 = ((bf16[32,64,128]{2,1,0:T(8,128)(2,1)}), bf16[32,64,128]{2,1,0:T(8,128)(2,1)S(1)}, u32[]{:S(2)}, u32[]{:S(2)}) async-start(bf16[32,64,128]{2,1,0:T(8,128)(2,1)} %get-tuple-element.24), calls=%async_computation.3 | async-start | bytes 1048576 | tf_op jit(solution)/shard_map/all_to_all | solution.py:297
  279.7 1.7 shard_map.108.refs_0_
  281.4 2.1 collective-permute-start.6
  283.6 4.6 %collective-permute-start.7 = (bf16[128,128]{1,0:T(8,128)(2,1)}, bf16[128,128]{1,0:T(8,128)(2,1)S(1)}, u32[]{:S(2)}, u32[]{:S(2)}) collective-permute-start(bf16[128,128]{1,0:T(8,128)(2,1)} %shard_map.108.refs_0_), channel_id=1, source_target_pairs={{0,32},{16,48},{32,0},{48,16},{1,33},{17,49},{33,1},{49,17},{2,34}... | collective-permute-start | bytes 98312 | tf_op jit(solution)/shard_map/ppermute | solution.py:301
  288.2 1.9 collective-permute-start.8
  290.1 1.4 collective-permute-done.7.refs_2_
  291.5 4.1 %collective-permute-done.8.refs_3_ = bf16[128,128]{1,0:T(8,128)(2,1)S(1)} collective-permute-done((bf16[128,128]{1,0:T(8,128)(2,1)}, bf16[128,128]{1,0:T(8,128)(2,1)S(1)}, u32[]{:S(2)}, u32[]{:S(2)}) %collective-permute-start.8) | collective-permute-done | bytes 32800 | tf_op jit(solution)/shard_map/ppermute | solution.py:301
  295.6 0.6 copy-done.14
  296.2 1.4 shard_map.109.refs_0_
  297.6 3.4 collective-permute-start.9
  301.0 4.1 %collective-permute-start.3 = (bf16[128,128]{1,0:T(8,128)(2,1)S(1)}, bf16[128,128]{1,0:T(8,128)(2,1)S(1)}, u32[]{:S(2)}, u32[]{:S(2)}) collective-permute-start(bf16[128,128]{1,0:T(8,128)(2,1)S(1)} %copy-done.20), channel_id=1, source_target_pairs={{0,128},{128,256},{256,384},{384,0},{1,129},{129,257},{257,385},{3... | collective-permute-start | bytes 98312 | tf_op jit(solution)/shard_map/ppermute | solution.py:301
  305.2 4.6 %collective-permute-start.4 = (bf16[128,128]{1,0:T(8,128)(2,1)S(1)}, bf16[128,128]{1,0:T(8,128)(2,1)S(1)}, u32[]{:S(2)}, u32[]{:S(2)}) collective-permute-start(bf16[128,128]{1,0:T(8,128)(2,1)S(1)} %copy-done.19), channel_id=1, source_target_pairs={{0,256},{128,384},{256,0},{384,128},{1,257},{129,385},{257,1},{385... | collective-permute-start | bytes 98312 | tf_op jit(solution)/shard_map/ppermute | solution.py:301
  309.8 5.4 %collective-permute-start.5 = (bf16[128,128]{1,0:T(8,128)(2,1)S(1)}, bf16[128,128]{1,0:T(8,128)(2,1)S(1)}, u32[]{:S(2)}, u32[]{:S(2)}) collective-permute-start(bf16[128,128]{1,0:T(8,128)(2,1)S(1)} %copy-done.18), channel_id=1, source_target_pairs={{0,384},{128,0},{256,128},{384,256},{1,385},{129,1},{257,129},{385... | collective-permute-start | bytes 98312 | tf_op jit(solution)/shard_map/ppermute | solution.py:301
  315.3 0.6 copy-done.12
  315.9 1.4 shard_map.110.refs_0_
  317.3 1.9 collective-permute-start.10
  319.2 4.5 %collective-permute-start.11 = (bf16[128,128]{1,0:T(8,128)(2,1)}, bf16[128,128]{1,0:T(8,128)(2,1)S(1)}, u32[]{:S(2)}, u32[]{:S(2)}) collective-permute-start(bf16[128,128]{1,0:T(8,128)(2,1)} %shard_map.110.refs_0_), channel_id=1, source_target_pairs={{0,256},{128,384},{256,0},{384,128},{1,257},{129,385},{257,1},{385... | collective-permute-start | bytes 98312 | tf_op jit(solution)/shard_map/ppermute | solution.py:301
  323.7 5.0 %collective-permute-start.12 = (bf16[128,128]{1,0:T(8,128)(2,1)}, bf16[128,128]{1,0:T(8,128)(2,1)S(1)}, u32[]{:S(2)}, u32[]{:S(2)}) collective-permute-start(bf16[128,128]{1,0:T(8,128)(2,1)} %shard_map.110.refs_0_), channel_id=1, source_target_pairs={{0,384},{128,0},{256,128},{384,256},{1,385},{129,1},{257,129},{385... | collective-permute-start | bytes 98312 | tf_op jit(solution)/shard_map/ppermute | solution.py:301
  328.8 0.8 copy-done.4
  329.6 2.1 shard_map.107
  331.7 0.6 copy-done.9
  332.3 3.2 shard_map.106
  335.5 0.6 copy-done.15
  336.0 0.6 copy-done.17
  336.6 1.7 shard_map.111
  (43 shorter events, 0.1 us)
Async XLA Ops:
  7.2 49.9 %all-gather.2.cloned.1.call-start = ((), (), s32[]{:S(2)}) async-start(), calls=%async_computation.5 | async-start | bytes 2228224 | tf_op jit(solution)/shard_map/all_gather | solution.py:319
  60.4 39.0 %all-to-all-start.1 = ((bf16[32,128,128]{2,1,0:T(8,128)(2,1)}), bf16[32,128,128]{2,1,0:T(8,128)(2,1)S(1)}, u32[]{:S(2)}, u32[]{:S(2)}) async-start(bf16[32,128,128]{2,1,0:T(8,128)(2,1)} %shard_map.103), calls=%async_computation.1 | async-start | bytes 2097152 | tf_op jit(solution)/shard_map/all_to_all | solution.py:297
  99.3 32.7 %copy-start.1 = (bf16[32,128,128]{2,1,0:T(8,128)(2,1)}, bf16[32,128,128]{2,1,0:T(8,128)(2,1)S(1)}, u32[]{:S(2)}) copy-start(bf16[32,128,128]{2,1,0:T(8,128)(2,1)S(1)} %all-to-all-done.1) | copy-start | bytes 3145732
  99.3 32.7 %all-to-all-start = ((bf16[32,128,128]{2,1,0:T(8,128)(2,1)}), bf16[32,128,128]{2,1,0:T(8,128)(2,1)S(1)}, u32[]{:S(2)}, u32[]{:S(2)}) async-start(bf16[32,128,128]{2,1,0:T(8,128)(2,1)} %shard_map.102), calls=%async_computation | async-start | bytes 2097152 | tf_op jit(solution)/shard_map/all_to_all | solution.py:297
  132.0 1.0 copy-start.2
  133.0 57.8 %copy-start.3 = (bf16[1,128,2048]{2,1,0:T(8,128)(2,1)S(1)}, bf16[1,128,2048]{2,1,0:T(8,128)(2,1)}, u32[]{:S(2)}) copy-start(bf16[1,128,2048]{2,1,0:T(8,128)(2,1)} %param.6) | copy-start | bytes 1572868
  185.9 56.5 %all-to-all-start.2 = ((bf16[8,4,128,128]{3,2,1,0:T(8,128)(2,1)}), bf16[8,4,128,128]{3,2,1,0:T(8,128)(2,1)S(1)}, u32[]{:S(2)}, u32[]{:S(2)}) async-start(bf16[8,4,128,128]{3,2,1,0:T(8,128)(2,1)} %get-tuple-element.18), calls=%async_computation.2 | async-start | bytes 2097152 | tf_op jit(solution)/shard_map/all_to_all | solution.py:297
  190.7 38.7 %collective-permute-start = (bf16[128,2048]{1,0:T(8,128)(2,1)S(1)}, bf16[128,2048]{1,0:T(8,128)(2,1)S(1)}, u32[]{:S(2)}, u32[]{:S(2)}) collective-permute-start(bf16[128,2048]{1,0:T(8,128)(2,1)S(1)} %bitcast.16), channel_id=1, source_target_pairs={{0,128},{128,256},{256,384},{384,0},{1,129},{129,257},{257,385},{3... | collective-permute-start | bytes 1572872 | tf_op jit(solution)/shard_map/ppermute | solution.py:301
  194.3 48.1 %collective-permute-start.1 = (bf16[128,2048]{1,0:T(8,128)(2,1)S(1)}, bf16[128,2048]{1,0:T(8,128)(2,1)S(1)}, u32[]{:S(2)}, u32[]{:S(2)}) collective-permute-start(bf16[128,2048]{1,0:T(8,128)(2,1)S(1)} %bitcast.17), channel_id=1, source_target_pairs={{0,256},{128,384},{256,0},{384,128},{1,257},{129,385},{257,1},{385... | collective-permute-start | bytes 1572872 | tf_op jit(solution)/shard_map/ppermute | solution.py:301
  197.5 45.0 %collective-permute-start.2 = (bf16[128,2048]{1,0:T(8,128)(2,1)S(1)}, bf16[128,2048]{1,0:T(8,128)(2,1)S(1)}, u32[]{:S(2)}, u32[]{:S(2)}) collective-permute-start(bf16[128,2048]{1,0:T(8,128)(2,1)S(1)} %bitcast.18), channel_id=1, source_target_pairs={{0,384},{128,0},{256,128},{384,256},{1,385},{129,1},{257,129},{385... | collective-permute-start | bytes 1572872 | tf_op jit(solution)/shard_map/ppermute | solution.py:301
  229.4 13.0 %copy-start.5 = (bf16[128,2048]{1,0:T(8,128)(2,1)}, bf16[128,2048]{1,0:T(8,128)(2,1)S(1)}, u32[]{:S(2)}) copy-start(bf16[128,2048]{1,0:T(8,128)(2,1)S(1)} %collective-permute-done.refs_1_) | copy-start | bytes 1572868
  242.4 0.8 copy-start.6
  242.4 1.0 copy-start.7
  242.4 1.3 copy-start
  247.0 54.0 %copy-start.20 = (bf16[128,128]{1,0:T(8,128)(2,1)S(1)}, bf16[128,128]{1,0:T(8,128)(2,1)}, u32[]{:S(2)}) copy-start(bf16[128,128]{1,0:T(8,128)(2,1)} %get-tuple-element.21) | copy-start | bytes 98308
  247.0 58.1 %copy-start.19 = (bf16[128,128]{1,0:T(8,128)(2,1)S(1)}, bf16[128,128]{1,0:T(8,128)(2,1)}, u32[]{:S(2)}) copy-start(bf16[128,128]{1,0:T(8,128)(2,1)} %get-tuple-element.22) | copy-start | bytes 98308
  247.0 62.7 %copy-start.18 = (bf16[128,128]{1,0:T(8,128)(2,1)S(1)}, bf16[128,128]{1,0:T(8,128)(2,1)}, u32[]{:S(2)}) copy-start(bf16[128,128]{1,0:T(8,128)(2,1)} %get-tuple-element.23) | copy-start | bytes 98308
  267.8 61.0 %all-to-all-start.3 = ((bf16[32,64,128]{2,1,0:T(8,128)(2,1)}), bf16[32,64,128]{2,1,0:T(8,128)(2,1)S(1)}, u32[]{:S(2)}, u32[]{:S(2)}) async-start(bf16[32,64,128]{2,1,0:T(8,128)(2,1)} %get-tuple-element.24), calls=%async_computation.3 | async-start | bytes 1048576 | tf_op jit(solution)/shard_map/all_to_all | solution.py:297
  281.4 8.7 %collective-permute-start.6 = (bf16[128,128]{1,0:T(8,128)(2,1)}, bf16[128,128]{1,0:T(8,128)(2,1)S(1)}, u32[]{:S(2)}, u32[]{:S(2)}) collective-permute-start(bf16[128,128]{1,0:T(8,128)(2,1)} %shard_map.108.refs_0_), channel_id=1, source_target_pairs={{0,16},{16,32},{32,48},{48,0},{1,17},{17,33},{33,49},{49,1},{2,18}... | collective-permute-start | bytes 98312 | tf_op jit(solution)/shard_map/ppermute | solution.py:301
  283.6 7.9 %collective-permute-start.7 = (bf16[128,128]{1,0:T(8,128)(2,1)}, bf16[128,128]{1,0:T(8,128)(2,1)S(1)}, u32[]{:S(2)}, u32[]{:S(2)}) collective-permute-start(bf16[128,128]{1,0:T(8,128)(2,1)} %shard_map.108.refs_0_), channel_id=1, source_target_pairs={{0,32},{16,48},{32,0},{48,16},{1,33},{17,49},{33,1},{49,17},{2,34}... | collective-permute-start | bytes 98312 | tf_op jit(solution)/shard_map/ppermute | solution.py:301
  288.2 7.4 %collective-permute-start.8 = (bf16[128,128]{1,0:T(8,128)(2,1)}, bf16[128,128]{1,0:T(8,128)(2,1)S(1)}, u32[]{:S(2)}, u32[]{:S(2)}) collective-permute-start(bf16[128,128]{1,0:T(8,128)(2,1)} %shard_map.108.refs_0_), channel_id=1, source_target_pairs={{0,48},{16,0},{32,16},{48,32},{1,49},{17,1},{33,17},{49,33},{2,50}... | collective-permute-start | bytes 98312 | tf_op jit(solution)/shard_map/ppermute | solution.py:301
  290.1 5.5 %copy-start.11 = (bf16[128,128]{1,0:T(8,128)(2,1)}, bf16[128,128]{1,0:T(8,128)(2,1)S(1)}, u32[]{:S(2)}) copy-start(bf16[128,128]{1,0:T(8,128)(2,1)S(1)} %collective-permute-done.6.refs_1_) | copy-start | bytes 98308
  291.5 4.1 %copy-start.13 = (bf16[128,128]{1,0:T(8,128)(2,1)}, bf16[128,128]{1,0:T(8,128)(2,1)S(1)}, u32[]{:S(2)}) copy-start(bf16[128,128]{1,0:T(8,128)(2,1)S(1)} %collective-permute-done.7.refs_2_) | copy-start | bytes 98308
  295.6 0.6 copy-start.14
  297.6 17.6 %collective-permute-start.9 = (bf16[128,128]{1,0:T(8,128)(2,1)}, bf16[128,128]{1,0:T(8,128)(2,1)S(1)}, u32[]{:S(2)}, u32[]{:S(2)}) collective-permute-start(bf16[128,128]{1,0:T(8,128)(2,1)} %shard_map.109.refs_0_), channel_id=1, source_target_pairs={{0,64},{64,0},{1,65},{65,1},{2,66},{66,2},{3,67},{67,3},{4,68},{68... | collective-permute-start | bytes 98312 | tf_op jit(solution)/shard_map/ppermute | solution.py:301
  301.0 22.7 %collective-permute-start.3 = (bf16[128,128]{1,0:T(8,128)(2,1)S(1)}, bf16[128,128]{1,0:T(8,128)(2,1)S(1)}, u32[]{:S(2)}, u32[]{:S(2)}) collective-permute-start(bf16[128,128]{1,0:T(8,128)(2,1)S(1)} %copy-done.20), channel_id=1, source_target_pairs={{0,128},{128,256},{256,384},{384,0},{1,129},{129,257},{257,385},{3... | collective-permute-start | bytes 98312 | tf_op jit(solution)/shard_map/ppermute | solution.py:301
  305.2 26.5 %collective-permute-start.4 = (bf16[128,128]{1,0:T(8,128)(2,1)S(1)}, bf16[128,128]{1,0:T(8,128)(2,1)S(1)}, u32[]{:S(2)}, u32[]{:S(2)}) collective-permute-start(bf16[128,128]{1,0:T(8,128)(2,1)S(1)} %copy-done.19), channel_id=1, source_target_pairs={{0,256},{128,384},{256,0},{384,128},{1,257},{129,385},{257,1},{385... | collective-permute-start | bytes 98312 | tf_op jit(solution)/shard_map/ppermute | solution.py:301
  309.8 21.9 %collective-permute-start.5 = (bf16[128,128]{1,0:T(8,128)(2,1)S(1)}, bf16[128,128]{1,0:T(8,128)(2,1)S(1)}, u32[]{:S(2)}, u32[]{:S(2)}) collective-permute-start(bf16[128,128]{1,0:T(8,128)(2,1)S(1)} %copy-done.18), channel_id=1, source_target_pairs={{0,384},{128,0},{256,128},{384,256},{1,385},{129,1},{257,129},{385... | collective-permute-start | bytes 98312 | tf_op jit(solution)/shard_map/ppermute | solution.py:301
  315.2 0.6 copy-start.12
  317.3 18.2 %collective-permute-start.10 = (bf16[128,128]{1,0:T(8,128)(2,1)}, bf16[128,128]{1,0:T(8,128)(2,1)S(1)}, u32[]{:S(2)}, u32[]{:S(2)}) collective-permute-start(bf16[128,128]{1,0:T(8,128)(2,1)} %shard_map.110.refs_0_), channel_id=1, source_target_pairs={{0,128},{128,256},{256,384},{384,0},{1,129},{129,257},{257,385},{3... | collective-permute-start | bytes 98312 | tf_op jit(solution)/shard_map/ppermute | solution.py:301
  319.2 16.3 %collective-permute-start.11 = (bf16[128,128]{1,0:T(8,128)(2,1)}, bf16[128,128]{1,0:T(8,128)(2,1)S(1)}, u32[]{:S(2)}, u32[]{:S(2)}) collective-permute-start(bf16[128,128]{1,0:T(8,128)(2,1)} %shard_map.110.refs_0_), channel_id=1, source_target_pairs={{0,256},{128,384},{256,0},{384,128},{1,257},{129,385},{257,1},{385... | collective-permute-start | bytes 98312 | tf_op jit(solution)/shard_map/ppermute | solution.py:301
  323.7 8.0 %copy-start.8 = (bf16[128,128]{1,0:T(8,128)(2,1)}, bf16[128,128]{1,0:T(8,128)(2,1)S(1)}, u32[]{:S(2)}) copy-start(bf16[128,128]{1,0:T(8,128)(2,1)S(1)} %collective-permute-done.3.refs_1_) | copy-start | bytes 98308
  323.7 11.7 %collective-permute-start.12 = (bf16[128,128]{1,0:T(8,128)(2,1)}, bf16[128,128]{1,0:T(8,128)(2,1)S(1)}, u32[]{:S(2)}, u32[]{:S(2)}) collective-permute-start(bf16[128,128]{1,0:T(8,128)(2,1)} %shard_map.110.refs_0_), channel_id=1, source_target_pairs={{0,384},{128,0},{256,128},{384,256},{1,385},{129,1},{257,129},{385... | collective-permute-start | bytes 98312 | tf_op jit(solution)/shard_map/ppermute | solution.py:301
  328.8 0.8 copy-start.4
  331.7 0.6 copy-start.9
  331.7 0.6 copy-start.10
  335.4 0.6 copy-start.15
  335.4 0.6 copy-start.16
  336.0 0.6 copy-start.17
Sparse Core Ops, SparseCore 0:
  10.7 46.3 all-gather.1

commit v2 on v1

--- a/solution.py
+++ b/solution.py
@@ -13,6 +13,7 @@
 LANES = 128
 LOG2E = 1.4426950408889634
 BLOCK = 512
+UPPER = 80
 ONES = HD + 16
 SP = ("zg", "zp", "x")
 GROUP = ("zp", "x")
@@ -78,16 +79,25 @@
         out_ref[2 * pair + 1] = second.astype(bf16)
 
 
-def project_kernel(rows_ref, weight_ref, out_ref, *, group):
+def project_kernel(rows_ref, first_ref, second_ref, out_ref, weight_ref):
+    depth = weight_ref.shape[0] // LANES
+    upper, lower = first_ref.shape[0] // depth, second_ref.shape[0] // depth
+    for k in range(depth):
+        weight_ref[k * LANES : k * LANES + upper] = first_ref[k * upper : (k + 1) * upper]
+        weight_ref[k * LANES + upper : (k + 1) * LANES] = second_ref[k * lower : (k + 1) * lower]
     projected = dot(rows_ref[...], weight_ref[...], 1, 0).astype(bf16)
-    for head in range(out_ref.shape[0]):
-        g = head // group
-        out_ref[head] = projected[:, g * LANES : (g + 1) * LANES]
+    for g in range(out_ref.shape[0]):
+        out_ref[g] = projected[:, g * LANES : (g + 1) * LANES]
+
+
+def copies_kernel(x_ref, out_ref):
+    for k in range(out_ref.shape[0]):
+        out_ref[k] = x_ref[...]
 
 
 def attend_kernel(
-    x_ref, kv_ref, cum_ref, dq_ref, dkv_ref, gcum_ref,
-    qa_ref, ka_ref, kn_ref, s_ref, dp_ref, xt_ref, dkt_ref, dvt_ref, rows_ref, acc_ref,
+    x_ref, parts_ref, cum_ref, dq_ref, dkv_ref, gcum_ref,
+    kv_ref, qa_ref, ka_ref, kn_ref, s_ref, dp_ref, xt_ref, dkt_ref, dvt_ref, rows_ref, acc_ref,
     *, blk, seq, members,
 ):
     count = seq // blk
@@ -99,6 +109,10 @@
     def prepare(i, _):
         at = pl.ds(pl.multiple_of(i * blk, blk), blk)
         x = x_ref[at, :].astype(f32)
+        for b in range(blk // LANES):
+            owner = i * (blk // LANES) + b
+            block = parts_ref[lax.rem(owner, members), lax.div(owner, members)]
+            kv_ref[pl.ds(pl.multiple_of(owner * LANES, LANES), LANES), :] = block
         kv = kv_ref[at, :].astype(f32)
         c1, c2, c3 = pieces(jnp.broadcast_to(cum_ref[:, at] * LOG2E, (LANES, blk)))
         one = jnp.ones_like(c1)
@@ -198,7 +212,8 @@
     gcum_ref[...] = rows_ref[0:1, :] - dkt_ref[HD : HD + 1, :]
 
 
-def attend(x, kv, cum, members):
+def attend(x, parts, cum):
+    members = parts.shape[0]
     seq = x.shape[0]
     owners = seq // LANES
     return call(
@@ -208,8 +223,9 @@
             shape((members, owners // members, LANES, LANES)),
             shape((1, seq), f32),
         ),
-        x, kv, cum,
+        x, parts, cum,
         scratch=[
+            VMEM((seq, LANES), bf16),
             VMEM((seq, 2 * LANES), bf16),
             VMEM((seq, 2 * LANES), bf16),
             VMEM((seq, LANES), bf16),
@@ -224,9 +240,9 @@
     )
 
 
-def group_sum_kernel(me_ref, terms_ref, *refs):
+def group_sum_kernel(me_ref, terms_ref, rows_ref, *refs):
     owners = terms_ref.shape[1]
-    rows_refs, sums_refs, part_ref = refs[:owners], refs[owners : 2 * owners], refs[2 * owners]
+    sums_refs, part_ref = refs[:owners], refs[owners]
     part = None
     for k in range(owners):
         owner = lax.rem(me_ref[0] + k, owners)
@@ -235,7 +251,7 @@
             total = total + terms_ref[member, owner].astype(f32)
         low = total.astype(bf16)
         sums_refs[k][...] = low
-        product = dot(low, rows_refs[(owners - k) % owners][...], 1, 0)
+        product = dot(low, rows_ref[owner], 1, 0)
         part = product if part is None else part + product
     for chunk in range(part_ref.shape[0]):
         part_ref[chunk] = part[:, chunk * LANES : (chunk + 1) * LANES].astype(bf16)
@@ -270,31 +286,20 @@
     out_ref[...] = total.astype(bf16)
 
 
-def sum_ring_kernel(me_ref, *refs):
-    parts, out_ref, held_ref = refs[:-2], refs[-2], refs[-1]
-    count = len(parts)
-    for k in range(count):
-        held_ref[lax.rem(me_ref[0] + count - k, count)] = parts[k][...].astype(f32)
-    total = held_ref[0]
-    for k in range(1, count):
-        total = total + held_ref[k]
-    out_ref[...] = total.astype(bf16)
-
-
-def finish_kernel(me_ref, *refs):
-    parts, (key_ref, value_ref, held_ref) = refs[:-3], refs[-3:]
-    count = len(parts)
-    for k in range(count):
-        held_ref[lax.rem(me_ref[0] + count - k, count)] = parts[k][...].astype(f32).T
-    for pair in range(count // 2):
+def finish_kernel(parts_ref, key_ref, value_ref):
+    for pair in range(parts_ref.shape[0] // 2):
         at = slice(pair * LANES, (pair + 1) * LANES)
-        keys, values = merge_pair(held_ref[2 * pair], held_ref[2 * pair + 1])
-        key_ref[:, at] = keys
-        value_ref[:, at] = values
+        first = parts_ref[2 * pair].astype(f32).T
+        second = parts_ref[2 * pair + 1].astype(f32).T
+        key_ref[:, at], value_ref[:, at] = merge_pair(first, second)
 
 
 def exchange(x, axes):
     return lax.all_to_all(x, axes, split_axis=0, concat_axis=0, tiled=True)
+
+
+def gather(x, axes, tiled):
+    return lax.all_gather(x, axes, axis=0, tiled=tiled)
 
 
 def shift(x, axis, size, by):
@@ -313,47 +318,46 @@
     rows = inputs.reshape(positions, features)
     width = 2 * kv_width
     block = shape((LANES, LANES))
-    me = {axis: lax.axis_index(axis).astype(jnp.int32).reshape(1) for axis in SP}
-
-    weight = call(pack_weights_kernel, shape((w_key.shape[0], width)), w_key, w_value)
-    weight = lax.all_gather(weight, "dp", axis=0, tiled=True)
+    me = lax.axis_index("zg").astype(jnp.int32).reshape(1)
+
+    local = call(pack_weights_kernel, shape((w_key.shape[0], width)), w_key, w_value)
+    first = gather(local[:UPPER], "dp", True)
     packed = call(
         pack_queries_kernel, shape((heads, positions, LANES)),
         queries.reshape(positions, -1), cotangent.reshape(positions, -1),
     )
     head_rows = exchange(packed, SP).reshape(heads * positions, LANES)
-    projected = call(
-        functools.partial(project_kernel, group=heads // kv_heads),
-        shape((heads, positions, LANES)), rows, weight,
-    )
-    head_kv = exchange(projected, SP).reshape(heads * positions, LANES)
+    second = gather(local[UPPER:], "dp", True)
+    projected, weight = call(
+        project_kernel,
+        (shape((kv_heads, positions, LANES)), shape((features, width))),
+        rows, first, second,
+    )
+    group_kv = exchange(projected, "zg")
+    copies = call(copies_kernel, shape((members, *group_kv.shape)), group_kv)
+    head_kv = exchange(copies, GROUP)
     head_kv, late_rows = lax.optimization_barrier((head_kv, rows))
-    near_rows = [late_rows] + [shift(late_rows, "zg", zg, k) for k in range(1, zg)]
-
-    dq, dkv, grad_cum = attend(head_rows, head_kv, cum_gate[0], members)
+    near_rows = gather(late_rows, "zg", False)
+
+    dq, dkv, grad_cum = attend(head_rows, head_kv, cum_gate[0])
     terms = exchange(dkv, GROUP)
     *sums, part = call(
         group_sum_kernel,
         (*[shape((LANES, positions))] * owners, shape((dp, LANES, LANES))),
-        me["zg"], terms, *near_rows,
+        me, terms, near_rows,
     )
     parts = exchange(part, "dp")
     own_sums = [sums[0]] + [shift(sums[k], "zg", zg, k) for k in range(1, zg)]
-    grad_input = call(grad_input_kernel, shape((positions, features)), me["zg"], weight, *own_sums)
+    grad_input = call(grad_input_kernel, shape((positions, features)), me, weight, *own_sums)
     summed = call(sum_parts_kernel, block, parts)
     query_parts = exchange(dq, SP)
     grad_queries = call(unpack_queries_kernel, shape((positions, features)), query_parts)
 
-    def held(count):
-        return [VMEM((count, LANES, LANES), f32)]
-
-    along = [summed] + [shift(summed, "x", xs, k) for k in range(1, xs)]
-    summed = call(sum_ring_kernel, block, me["x"], *along, scratch=held(xs))
-    along = [summed] + [shift(summed, "zp", zp, k) for k in range(1, zp)]
-    summed = call(sum_ring_kernel, block, me["zp"], *along, scratch=held(zp))
-    along = [summed] + [shift(summed, "zg", zg, k) for k in range(1, zg)]
+    along = gather(summed, GROUP, False)
+    summed = call(sum_parts_kernel, block, along)
+    along = gather(summed, "zg", False)
     half = shape((LANES, kv_width), f32)
-    grad_key, grad_value = call(finish_kernel, (half, half), me["zg"], *along, scratch=held(zg))
+    grad_key, grad_value = call(finish_kernel, (half, half), along)
     return grad_input[None], grad_queries[None], grad_cum[None], grad_key, grad_value
 
 

time: 347 us -> 309 us (0.89)
  the two profiles are of different devices: /device:TPU:6 before, /device:TPU:8 now
where the time goes in v2:
time: 309 us; the launch traced here: 307 us
  blocking collectives  105 us (34%)
  waiting for transfers between devices  77.3 us (25%)
  Pallas kernels  76.1 us (25%)
  starting transfers between devices  30.5 us (10%)
  between operations  14.1 us (5%)
  local copies, waits for them, and re-layouts  4.72 us (2%)
    pallas_call x11, Pallas kernels, call(): pl.pallas_call(kernel, out_shape=out_shapes, in_specs=[pl.BlockSpec(memor...  76.1 us
    all_gather x3, blocking collectives, gather(): return lax.all_gather(x, axes, axis=0, tiled=tiled)  70 us
    all_to_all x4, waiting for transfers between devices, exchange(): return lax.all_to_all(x, axes, split_axis=0, concat_axis=0, tiled=True)  54.4 us
    all_to_all x2, blocking collectives, exchange(): return lax.all_to_all(x, axes, split_axis=0, concat_axis=0, tiled=True)  34.5 us
    all_gather x2, waiting for transfers between devices, gather(): return lax.all_gather(x, axes, axis=0, tiled=tiled)  21.3 us
    all_to_all x4, starting transfers between devices, exchange(): return lax.all_to_all(x, axes, split_axis=0, concat_axis=0, tiled=True)  19 us
    ppermute x3, starting transfers between devices, shift(): return lax.ppermute(x, axis, [(k, (k + by) % size) for k in range(size)])  11.4 us
  transfers between devices with their start and end apart: 9, of which 5 were waited for; matrix products, arithmetic and copies ran while one was open for 0% of the time, Pallas kernels for 21%

profile of v2, /device:TPU:8, one launch (start us, length us, event | category | flops | bytes accessed | tf_op | source)
XLA Modules:
  0.0 307.3 jit_solution(8777814738225935220)
XLA Ops:
  7.2 0.0 all-gather.6.cloned.1.call-start
  7.2 1.6 shard_map.101
  8.8 1.5 slice.8
  10.4 0.0 all-gather.6.cloned.1.call-update
  10.4 0.8 slice.9
  11.2 23.4 %all_gather.25.second_ref = bf16[768,512]{1,0:T(8,128)(2,1)} all-gather(bf16[48,512]{1,0:T(8,128)(2,1)S(1)} %slice.9), channel_id=1, replica_groups=mesh['zg'=4,'zp'=2,'x'=4,'dp'=16] {'dp'}, dimensions={0}, use_global_device_ids=true | all-gather | bytes 835584 | tf_op jit(solution)/shard_map/all_gather | solution.py:302
  34.6 21.3 %all-gather.6.cloned.1.call-done.first_ref = bf16[1280,512]{1,0:T(8,128)(2,1)} async-done(((bf16[80,512]{1,0:T(8,128)(2,1)}), bf16[1280,512]{1,0:T(8,128)(2,1)}) %all-gather.6.cloned.1.call-update) | async-done | bytes 1310736 | tf_op jit(solution)/shard_map/all_gather | solution.py:302
  56.0 3.3 %shard_map.102 = (bf16[4,128,128]{2,1,0:T(8,128)(2,1)}, bf16[2048,512]{1,0:T(8,128)(2,1)}) custom-call(bf16[128,2048]{1,0:T(8,128)(2,1)} %bitcast.13, bf16[1280,512]{1,0:T(8,128)(2,1)} %all-gather.6.cloned.1.call-done.first_ref, bf16[768,512]{1,0:T(8,128)(2,1)} %all_gather.25.second_ref), custom_call_target="tpu_custom_call" | custom-call | tf_op jit(solution)/shard_map/pallas_call | solution.py:49
  59.3 16.7 %all_to_all.30.x_ref = bf16[4,128,128]{2,1,0:T(8,128)(2,1)} all-to-all(bf16[4,128,128]{2,1,0:T(8,128)(2,1)} %get-tuple-element.20), channel_id=1, replica_groups=mesh['zg'=4,'zp'=2,'x'=4,'dp'=16] {'zg'}, dimensions={0} | all-to-all | bytes 262144 | tf_op jit(solution)/shard_map/all_to_all | solution.py:298
  76.0 2.0 shard_map.104
  78.0 4.5 %all-to-all-start.2 = ((bf16[8,4,128,128]{3,2,1,0:T(8,128)(2,1)}), bf16[8,4,128,128]{3,2,1,0:T(8,128)(2,1)S(1)}, u32[]{:S(2)}, u32[]{:S(2)}) async-start(bf16[8,4,128,128]{3,2,1,0:T(8,128)(2,1)} %shard_map.104), calls=%async_computation.2 | async-start | bytes 2097152 | tf_op jit(solution)/shard_map/all_to_all | solution.py:298
  82.5 2.6 shard_map.103
  85.1 10.3 %all-to-all-done.2.parts_ref = bf16[8,4,128,128]{3,2,1,0:T(8,128)(2,1)S(1)} async-done(((bf16[8,4,128,128]{3,2,1,0:T(8,128)(2,1)}), bf16[8,4,128,128]{3,2,1,0:T(8,128)(2,1)S(1)}, u32[]{:S(2)}, u32[]{:S(2)}) %all-to-all-start.2) | async-done | bytes 1048608 | tf_op jit(solution)/shard_map/all_to_all | solution.py:298
  95.5 0.0 copy-start
  95.5 5.3 %all-to-all-start = ((bf16[32,128,128]{2,1,0:T(8,128)(2,1)}), bf16[32,128,128]{2,1,0:T(8,128)(2,1)S(1)}, u32[]{:S(2)}, u32[]{:S(2)}) async-start(bf16[32,128,128]{2,1,0:T(8,128)(2,1)} %shard_map.103), calls=%async_computation | async-start | bytes 2097152 | tf_op jit(solution)/shard_map/all_to_all | solution.py:298
  100.7 0.0 all-gather.8.cloned.1.call-start
  100.8 0.7 all-gather.8.cloned.1.call-update
  101.5 32.6 %all-to-all-done = bf16[32,128,128]{2,1,0:T(8,128)(2,1)S(1)} async-done(((bf16[32,128,128]{2,1,0:T(8,128)(2,1)}), bf16[32,128,128]{2,1,0:T(8,128)(2,1)S(1)}, u32[]{:S(2)}, u32[]{:S(2)}) %all-to-all-start) | async-done | bytes 1048608 | tf_op jit(solution)/shard_map/all_to_all | solution.py:298
  134.1 0.0 copy-start.1
  134.1 0.0 copy-done
  134.1 1.0 copy-done.1
  135.0 52.7 %shard_map.105 = (bf16[32,64,128]{2,1,0:T(8,128)(2,1)}, bf16[8,4,128,128]{3,2,1,0:T(8,128)(2,1)}, f32[1,4096]{1,0:T(1,128)}) custom-call(bf16[4096,128]{1,0:T(8,128)(2,1)} %bitcast.12, bf16[8,4,128,128]{3,2,1,0:T(8,128)(2,1)} %copy-done, f32[1,4096]{1,0:T(1,128)} %bitcast.22), custom_call_target="tpu_custom_call" | custom-call | tf_op jit(solution)/shard_map/pallas_call | solution.py:49
  187.8 17.8 %all_to_all.31.terms_ref = bf16[8,4,128,128]{3,2,1,0:T(8,128)(2,1)} all-to-all(bf16[8,4,128,128]{3,2,1,0:T(8,128)(2,1)} %get-tuple-element.22), channel_id=1, replica_groups=mesh['zg'=4,'zp'=2,'x'=4,'dp'=16] {'zp','x'}, dimensions={0} | all-to-all | bytes 2097152 | tf_op jit(solution)/shard_map/all_to_all | solution.py:298
  205.5 3.9 %all-to-all-start.4 = ((bf16[32,64,128]{2,1,0:T(8,128)(2,1)}), bf16[32,64,128]{2,1,0:T(8,128)(2,1)S(1)}, u32[]{:S(2)}, u32[]{:S(2)}) async-start(bf16[32,64,128]{2,1,0:T(8,128)(2,1)} %get-tuple-element.28), calls=%async_computation.4 | async-start | bytes 1048576 | tf_op jit(solution)/shard_map/all_to_all | solution.py:298
  209.5 0.0 all-gather.8.cloned.1.call-done
  209.5 3.4 %shard_map.106 = (bf16[128,128]{1,0:T(8,128)(2,1)}, bf16[128,128]{1,0:T(8,128)(2,1)}, bf16[128,128]{1,0:T(8,128)(2,1)}, bf16[128,128]{1,0:T(8,128)(2,1)}, bf16[16,128,128]{2,1,0:T(8,128)(2,1)}) custom-call(s32[1]{0:T(128)} %bitcast.me_ref, bf16[8,4,128,128]{3,2,1,0:T(8,128)(2,1)} %all_to_all.31.terms_ref, bf16[4,128,2048]{2,1,0:T(8,128)(2,1)} %bitcast.15), custom_call_target="tpu_custom_call" | custom-call | tf_op jit(solution)/shard_map/pallas_call | solution.py:49
  212.9 11.5 %all-to-all-done.4.packed_ref = bf16[32,64,128]{2,1,0:T(8,128)(2,1)S(1)} async-done(((bf16[32,64,128]{2,1,0:T(8,128)(2,1)}), bf16[32,64,128]{2,1,0:T(8,128)(2,1)S(1)}, u32[]{:S(2)}, u32[]{:S(2)}) %all-to-all-start.4) | async-done | bytes 524320 | tf_op jit(solution)/shard_map/all_to_all | solution.py:298
  224.4 5.3 %all-to-all-start.5 = ((bf16[16,128,128]{2,1,0:T(8,128)(2,1)}), bf16[16,128,128]{2,1,0:T(8,128)(2,1)S(1)}, u32[]{:S(2)}, u32[]{:S(2)}) async-start(bf16[16,128,128]{2,1,0:T(8,128)(2,1)} %get-tuple-element.30), calls=%async_computation.5 | async-start | bytes 1048576 | tf_op jit(solution)/shard_map/all_to_all | solution.py:298
  229.7 3.4 %collective-permute-start = (bf16[128,128]{1,0:T(8,128)(2,1)}, bf16[128,128]{1,0:T(8,128)(2,1)S(1)}, u32[]{:S(2)}, u32[]{:S(2)}) collective-permute-start(bf16[128,128]{1,0:T(8,128)(2,1)} %get-tuple-element.25), channel_id=1, source_target_pairs={{0,128},{128,256},{256,384},{384,0},{1,129},{129,257},{257,385},{3... | collective-permute-start | bytes 98312 | tf_op jit(solution)/shard_map/ppermute | solution.py:306
  233.2 4.0 %collective-permute-start.1 = (bf16[128,128]{1,0:T(8,128)(2,1)}, bf16[128,128]{1,0:T(8,128)(2,1)S(1)}, u32[]{:S(2)}, u32[]{:S(2)}) collective-permute-start(bf16[128,128]{1,0:T(8,128)(2,1)} %get-tuple-element.26), channel_id=1, source_target_pairs={{0,256},{128,384},{256,0},{384,128},{1,257},{129,385},{257,1},{385... | collective-permute-start | bytes 98312 | tf_op jit(solution)/shard_map/ppermute | solution.py:306
  237.2 4.0 %collective-permute-start.2 = (bf16[128,128]{1,0:T(8,128)(2,1)}, bf16[128,128]{1,0:T(8,128)(2,1)S(1)}, u32[]{:S(2)}, u32[]{:S(2)}) collective-permute-start(bf16[128,128]{1,0:T(8,128)(2,1)} %get-tuple-element.27), channel_id=1, source_target_pairs={{0,384},{128,0},{256,128},{384,256},{1,385},{129,1},{257,129},{385... | collective-permute-start | bytes 98312 | tf_op jit(solution)/shard_map/ppermute | solution.py:306
  241.2 0.0 copy-done.2
  241.2 2.1 shard_map.108
  243.2 0.0 collective-permute-done.refs_1_
  243.2 0.0 collective-permute-done.1.refs_2_
  243.3 0.0 copy-start.5
  243.3 0.8 collective-permute-done.2.refs_3_
  244.1 0.0 copy-done.4
  244.1 0.0 copy-done.5
  244.1 0.6 copy-done.6
  244.7 3.2 %shard_map.107 = bf16[128,2048]{1,0:T(8,128)(2,1)} custom-call(s32[1]{0:T(128)} %bitcast.me_ref, bf16[2048,512]{1,0:T(8,128)(2,1)} %get-tuple-element.19.weight_ref, bf16[128,128]{1,0:T(8,128)(2,1)} %get-tuple-element.24.refs_0_, bf16[128,128]{1,0:T(8,128)(2,1)} %copy-done.4, bf16[128,128]{1,0:T(8,128)(2,1)} %copy-done.5, bf16[128,128]{1,0:T(8,128)(2,1)} %copy-done.6), custom_call_target="tpu_custom_call" | custom-call | tf_op jit(solution)/shard_map/pallas_call | solution.py:49
  247.9 0.0 all-to-all-done.5.parts_ref
  247.9 0.8 copy-done.3
  248.7 1.7 shard_map.109
  250.4 30.7 %all-gather.1 = bf16[1024,128]{1,0:T(8,128)(2,1)} all-gather(bf16[128,128]{1,0:T(8,128)(2,1)} %shard_map.109), channel_id=3, replica_groups=mesh['zg'=4,'zp'=2,'x'=4,'dp'=16] {'zp','x'}, dimensions={0}, use_global_device_ids=true | all-gather | bytes 294912 | tf_op jit(solution)/shard_map/all_gather | solution.py:302
  281.1 1.6 shard_map.110
  282.7 15.9 %all-gather.2 = bf16[512,128]{1,0:T(8,128)(2,1)} all-gather(bf16[128,128]{1,0:T(8,128)(2,1)} %shard_map.110), channel_id=4, replica_groups=mesh['zg'=4,'zp'=2,'x'=4,'dp'=16] {'zg'}, dimensions={0}, use_global_device_ids=true | all-gather | bytes 163840 | tf_op jit(solution)/shard_map/all_gather | solution.py:302
  298.6 1.8 shard_map.111
  (4 shorter events, 0.0 us)
Async XLA Ops:
  7.2 48.8 %all-gather.6.cloned.1.call-start = ((), (), s32[]{:S(2)}) async-start(), calls=%async_computation.6 | async-start | bytes 1392640 | tf_op jit(solution)/shard_map/all_gather | solution.py:302
  78.0 17.4 %all-to-all-start.2 = ((bf16[8,4,128,128]{3,2,1,0:T(8,128)(2,1)}), bf16[8,4,128,128]{3,2,1,0:T(8,128)(2,1)S(1)}, u32[]{:S(2)}, u32[]{:S(2)}) async-start(bf16[8,4,128,128]{3,2,1,0:T(8,128)(2,1)} %shard_map.104), calls=%async_computation.2 | async-start | bytes 2097152 | tf_op jit(solution)/shard_map/all_to_all | solution.py:298
  95.5 38.6 %copy-start = (bf16[8,4,128,128]{3,2,1,0:T(8,128)(2,1)}, bf16[8,4,128,128]{3,2,1,0:T(8,128)(2,1)S(1)}, u32[]{:S(2)}) copy-start(bf16[8,4,128,128]{3,2,1,0:T(8,128)(2,1)S(1)} %all-to-all-done.2.parts_ref) | copy-start | bytes 3145732
  95.5 38.6 %all-to-all-start = ((bf16[32,128,128]{2,1,0:T(8,128)(2,1)}), bf16[32,128,128]{2,1,0:T(8,128)(2,1)S(1)}, u32[]{:S(2)}, u32[]{:S(2)}) async-start(bf16[32,128,128]{2,1,0:T(8,128)(2,1)} %shard_map.103), calls=%async_computation | async-start | bytes 2097152 | tf_op jit(solution)/shard_map/all_to_all | solution.py:298
  100.7 108.7 %all-gather.8.cloned.1.call-start = ((), (), s32[]{:S(2)}) async-start(), calls=%async_computation.7 | async-start | bytes 2621440 | tf_op jit(solution)/shard_map/all_gather | solution.py:302
  134.1 1.0 copy-start.1
  205.5 18.9 %all-to-all-start.4 = ((bf16[32,64,128]{2,1,0:T(8,128)(2,1)}), bf16[32,64,128]{2,1,0:T(8,128)(2,1)S(1)}, u32[]{:S(2)}, u32[]{:S(2)}) async-start(bf16[32,64,128]{2,1,0:T(8,128)(2,1)} %get-tuple-element.28), calls=%async_computation.4 | async-start | bytes 1048576 | tf_op jit(solution)/shard_map/all_to_all | solution.py:298
  224.4 16.7 %copy-start.2 = (bf16[32,64,128]{2,1,0:T(8,128)(2,1)}, bf16[32,64,128]{2,1,0:T(8,128)(2,1)S(1)}, u32[]{:S(2)}) copy-start(bf16[32,64,128]{2,1,0:T(8,128)(2,1)S(1)} %all-to-all-done.4.packed_ref) | copy-start | bytes 1572868
  224.4 23.5 %all-to-all-start.5 = ((bf16[16,128,128]{2,1,0:T(8,128)(2,1)}), bf16[16,128,128]{2,1,0:T(8,128)(2,1)S(1)}, u32[]{:S(2)}, u32[]{:S(2)}) async-start(bf16[16,128,128]{2,1,0:T(8,128)(2,1)} %get-tuple-element.30), calls=%async_computation.5 | async-start | bytes 1048576 | tf_op jit(solution)/shard_map/all_to_all | solution.py:298
  229.7 13.5 %collective-permute-start = (bf16[128,128]{1,0:T(8,128)(2,1)}, bf16[128,128]{1,0:T(8,128)(2,1)S(1)}, u32[]{:S(2)}, u32[]{:S(2)}) collective-permute-start(bf16[128,128]{1,0:T(8,128)(2,1)} %get-tuple-element.25), channel_id=1, source_target_pairs={{0,128},{128,256},{256,384},{384,0},{1,129},{129,257},{257,385},{3... | collective-permute-start | bytes 98312 | tf_op jit(solution)/shard_map/ppermute | solution.py:306
  233.2 10.1 %collective-permute-start.1 = (bf16[128,128]{1,0:T(8,128)(2,1)}, bf16[128,128]{1,0:T(8,128)(2,1)S(1)}, u32[]{:S(2)}, u32[]{:S(2)}) collective-permute-start(bf16[128,128]{1,0:T(8,128)(2,1)} %get-tuple-element.26), channel_id=1, source_target_pairs={{0,256},{128,384},{256,0},{384,128},{1,257},{129,385},{257,1},{385... | collective-permute-start | bytes 98312 | tf_op jit(solution)/shard_map/ppermute | solution.py:306
  237.2 6.9 %collective-permute-start.2 = (bf16[128,128]{1,0:T(8,128)(2,1)}, bf16[128,128]{1,0:T(8,128)(2,1)S(1)}, u32[]{:S(2)}, u32[]{:S(2)}) collective-permute-start(bf16[128,128]{1,0:T(8,128)(2,1)} %get-tuple-element.27), channel_id=1, source_target_pairs={{0,384},{128,0},{256,128},{384,256},{1,385},{129,1},{257,129},{385... | collective-permute-start | bytes 98312 | tf_op jit(solution)/shard_map/ppermute | solution.py:306
  243.2 0.9 copy-start.4
  243.3 0.9 copy-start.5
  244.1 0.6 copy-start.6
  247.9 0.8 copy-start.3
Sparse Core Ops, SparseCore 0:
  10.7 45.2 all-gather.5
  103.7 53.9 all-gather.7

commit v3 on v2

v3 whole, which is shorter than its diff:
```python
import functools

import jax
import jax.numpy as jnp
from jax import lax
from jax.experimental import pallas as pl
from jax.experimental.pallas import tpu as pltpu
from jax.sharding import Mesh
from jax.sharding import PartitionSpec as P


HD = 64
LANES = 128
LOG2E = 1.4426950408889634
BLOCK = 512
ONES = HD + 16
SP = ("z", "x")
LOWEST = -3.4028235e38
bf16 = jnp.bfloat16
f32 = jnp.float32
VMEM = pltpu.VMEM


def dot(a, b, ca, cb):
    return lax.dot_general(a, b, (((ca,), (cb,)), ((), ())), preferred_element_type=f32)


def low_half(rows):
    return lax.broadcasted_iota(jnp.int32, (rows, LANES), 1) < HD


def merge_pair(a, b):
    low = low_half(a.shape[0])
    return jnp.where(low, a, pltpu.roll(b, HD, 1)), jnp.where(low, pltpu.roll(a, HD, 1), b)


def pieces(value):
    first = value.astype(bf16).astype(f32)
    rest = value - first
    second = rest.astype(bf16).astype(f32)
    third = (rest - second).astype(bf16).astype(f32)
    return first, second, third


def call(kernel, out_shapes, *args, scratch=(), vmem=60):
    many = isinstance(out_shapes, tuple)
    specs = pl.BlockSpec(memory_space=VMEM)
    return pl.pallas_call(
        kernel,
        out_shape=out_shapes,
        in_specs=[
            pl.BlockSpec(memory_space=pltpu.SMEM) if arg.dtype == jnp.int32 else specs
            for arg in args
        ],
        out_specs=(specs,) * len(out_shapes) if many else specs,
        scratch_shapes=scratch,
        compiler_params=pltpu.CompilerParams(vmem_limit_bytes=vmem * 1024 * 1024),
    )(*args)


def shape(dims, dtype=bf16):
    return jax.ShapeDtypeStruct(dims, dtype)


def pack_weights_kernel(me_ref, key_ref, value_ref, out_ref):
    at = pl.ds(pl.multiple_of(lax.div(me_ref[0], 2) * LANES, LANES), LANES)
    first, second = merge_pair(key_ref[:, at].astype(f32), value_ref[:, at].astype(f32))
    out_ref[...] = jnp.where(lax.rem(me_ref[0], 2) == 0, first, second).astype(bf16)


def pack_queries_kernel(query_ref, grad_ref, out_ref, *, members):
    heads = out_ref.shape[0]
    quads = heads // members
    for pair in range(heads // 2):
        at = slice(pair * LANES, (pair + 1) * LANES)
        blocks = merge_pair(query_ref[:, at].astype(f32), grad_ref[:, at].astype(f32))
        for k in range(2):
            head = 2 * pair + k
            out_ref[head % members * quads + head // members] = blocks[k].astype(bf16)


def project_kernel(me_ref, weight_ref, *refs):
    rows_refs, (out_ref, copies_ref) = refs[:-2], refs[-2:]
    quads = len(rows_refs)
    weight = weight_ref[...]
    for k in range(quads):
        owner = lax.rem(me_ref[0] + quads - k, quads)
        projected = dot(rows_refs[k][...], weight, 1, 0).astype(bf16)
        for member in range(out_ref.shape[0]):
            out_ref[member, owner] = projected
    for k in range(copies_ref.shape[0]):
        copies_ref[k] = weight


def attend_kernel(
    x_ref, kv_ref, cum_ref, dq_ref, dkv_ref, gcum_ref,
    qa_ref, ka_ref, kn_ref, s_ref, dp_ref, xt_ref, dkt_ref, dvt_ref, rows_ref, acc_ref, stat_ref,
    *, blk, seq,
):
    count = seq // blk
    quads = dkv_ref.shape[1]
    scale = HD**-0.5
    lane = lax.broadcasted_iota(jnp.int32, (blk, LANES), 1)
    low = lane < HD
    row_id = lax.broadcasted_iota(jnp.int32, (LANES, blk), 0)

    def span(i):
        return pl.ds(pl.multiple_of(i * blk, blk), blk)

    def prepare(i, _):
        at = span(i)
        x = x_ref[at, :].astype(f32)
        kv = kv_ref[at, :].astype(f32)
        c1, c2, c3 = pieces(jnp.broadcast_to(cum_ref[:, at] * LOG2E, (LANES, blk)))
        one = jnp.ones_like(c1)

        def extra(values):
            total = jnp.zeros_like(c1)
            for k, value in enumerate(values):
                total = jnp.where(row_id == HD + k, value, total)
            return total.T

        q1, q2, q3 = pieces(x * (LOG2E * scale))
        qa_ref[at, 0:LANES] = jnp.where(low, q1, pltpu.roll(q2, HD, 1)).astype(bf16)
        qa_ref[at, LANES:] = jnp.where(low, q3, extra((c1, c2, c3, one, one, one))).astype(bf16)
        ka_ref[at, 0:LANES] = jnp.where(low, kv, pltpu.roll(kv, HD, 1)).astype(bf16)
        ka_ref[at, LANES:] = jnp.where(low, kv, extra((one, one, one, -c1, -c2, -c3))).astype(bf16)
        kn_ref[at, :] = jnp.where(low, kv, jnp.where(lane == HD, 1.0, 0.0)).astype(bf16)
        xt = x.T
        ones_row = jnp.where(row_id == HD, 1.0, 0.0)
        xt_ref[0:ONES, at] = jnp.where(row_id < HD, xt, ones_row)[0:ONES].astype(bf16)
        xt_ref[ONES:, at] = xt[HD:].astype(bf16)
        dkt_ref[:, at] = jnp.zeros((ONES, blk), f32)
        dvt_ref[:, at] = jnp.zeros((HD, blk), f32)
        return 0

    lax.fori_loop(0, count, prepare, 0)

    def tiles(block):
        return [block[:, k * LANES : (k + 1) * LANES] for k in range(blk // LANES)]

    def query_block(i, _):
        rows = span(i)

        def score(j, diagonal):
            at = span(j)
            x = x_ref[rows, :]
            scores = dot(qa_ref[rows, :], ka_ref[at, :], 1, 1)
            if diagonal:
                sub = lax.broadcasted_iota(jnp.int32, (blk, blk), 0)
                col = lax.broadcasted_iota(jnp.int32, (blk, blk), 1)
                scores = jnp.where(col <= sub, scores, LOWEST)
            weights = dot(jnp.where(low, jnp.zeros_like(x), x), kv_ref[at, :], 1, 1)
            s_ref[:, at] = scores
            dp_ref[:, at] = weights
            return tiles(scores), tiles(weights)

        def tally(scores, weights, best):
            total = weighted = None
            for s, w in zip(scores, weights):
                e = jnp.exp2(s - best)
                total = e if total is None else total + e
                weighted = e * w if weighted is None else weighted + e * w
            return total, weighted

        scores, weights = score(i, True)
        best = functools.reduce(jnp.maximum, scores)
        stat_ref[0] = best
        stat_ref[1], stat_ref[2] = tally(scores, weights, best)

        def full_block(j, _):
            scores, weights = score(j, False)
            old = stat_ref[0]
            best = functools.reduce(jnp.maximum, scores, old)
            shrink = jnp.exp2(old - best)
            total, weighted = tally(scores, weights, best)
            stat_ref[0] = best
            stat_ref[1] = stat_ref[1] * shrink + total
            stat_ref[2] = stat_ref[2] * shrink + weighted
            return 0

        lax.fori_loop(0, i, full_block, 0)
        best = stat_ref[0]
        top = jnp.max(best, axis=1, keepdims=True)
        shrink = jnp.exp2(best - top)
        total = jnp.sum(stat_ref[1] * shrink, axis=1, keepdims=True)
        row_dot = jnp.sum(stat_ref[2] * shrink, axis=1, keepdims=True) / total
        stat_ref[0] = jnp.broadcast_to(top + jnp.log2(total), (blk, LANES))
        stat_ref[1] = jnp.broadcast_to(row_dot, (blk, LANES))
        acc_ref[...] = jnp.zeros((blk, LANES), f32)

        def gradients(j, _):
            at = span(j)
            level, row_dot = stat_ref[0], stat_ref[1]
            probs = [jnp.exp2(s - level) for s in tiles(s_ref[:, at])]
            grads = [p * (w - row_dot) for p, w in zip(probs, tiles(dp_ref[:, at]))]
            grad_low = jnp.concatenate([g.astype(bf16) for g in grads], axis=1)
            probs_low = jnp.concatenate([p.astype(bf16) for p in probs], axis=1)
            acc_ref[...] += dot(grad_low, kn_ref[at, :], 1, 0)
            dkt_ref[:, at] += dot(xt_ref[0:ONES, rows], grad_low, 1, 0)
            dvt_ref[:, at] += dot(xt_ref[ONES:, rows], probs_low, 1, 0)
            return 0

        lax.fori_loop(0, i + 1, gradients, 0)
        dq = acc_ref[...]
        rows_ref[:, rows] = dq.T[HD : HD + 8]
        dq = dq * scale
        for b in range(blk // LANES):
            upper = dq[b * LANES : b * LANES + HD]
            lower = dq[b * LANES + HD : (b + 1) * LANES]
            packed = jnp.where(low[0:HD], upper, pltpu.roll(lower, HD, 1))
            dq_ref[i * (blk // LANES) + b] = packed.astype(bf16)
        return 0

    lax.fori_loop(0, count, query_block, 0)
    for b in range(seq // LANES):
        at = slice(b * LANES, (b + 1) * LANES)
        dkv_ref[b // quads, b % quads, 0:HD, :] = (dkt_ref[0:HD, at] * scale).astype(bf16)
        dkv_ref[b // quads, b % quads, HD:, :] = dvt_ref[:, at].astype(bf16)
    gcum_ref[...] = rows_ref[0:1, :] - dkt_ref[HD : HD + 1, :]


def attend(x, kv, cum, quads):
    seq = x.shape[0]
    owners = seq // LANES
    return call(
        functools.partial(attend_kernel, blk=BLOCK, seq=seq),
        (
            shape((owners, HD, LANES)),
            shape((owners // quads, quads, LANES, LANES)),
            shape((1, seq), f32),
        ),
        x, kv, cum,
        scratch=[
            VMEM((seq, 2 * LANES), bf16),
            VMEM((seq, 2 * LANES), bf16),
            VMEM((seq, LANES), bf16),
            VMEM((BLOCK, seq), f32),
            VMEM((BLOCK, seq), f32),
            VMEM((ONES + HD, seq), bf16),
            VMEM((ONES, seq), f32),
            VMEM((HD, seq), f32),
            VMEM((8, seq), f32),
            VMEM((BLOCK, LANES), f32),
            VMEM((3, BLOCK, LANES), f32),
        ],
    )


def group_sum_kernel(me_ref, terms_ref, *refs):
    owners = terms_ref.shape[1]
    rows_refs, sums_refs, part_ref = refs[:owners], refs[owners : 2 * owners], refs[2 * owners]
    part = None
    for k in range(owners):
        owner = lax.rem(me_ref[0] + k, owners)
        total = terms_ref[0, owner].astype(f32)
        for member in range(1, terms_ref.shape[0]):
            total = total + terms_ref[member, owner].astype(f32)
        low = total.astype(bf16)
        sums_refs[k][...] = low
        product = dot(low, rows_refs[(owners - k) % owners][...], 1, 0)
        part = product if part is None else part + product
    for chunk in range(part_ref.shape[0]):
        part_ref[chunk] = part[:, chunk * LANES : (chunk + 1) * LANES].astype(bf16)


def unpack_queries_kernel(packed_ref, out_ref, *, members):
    heads = packed_ref.shape[0]
    quads = heads // members
    for pair in range(heads // 2):
        blocks = [
            packed_ref[head % members * quads + head // members].astype(f32)
            for head in (2 * pair, 2 * pair + 1)
        ]
        upper, lower = merge_pair(*blocks)
        at = slice(pair * LANES, (pair + 1) * LANES)
        out_ref[0:HD, at] = upper.astype(bf16)
        out_ref[HD:, at] = lower.astype(bf16)


def grad_input_kernel(me_ref, weight_ref, *refs):
    sums_refs, out_ref = refs[:-1], refs[-1]
    groups = len(sums_refs)
    total = None
    for k in range(groups):
        g = lax.rem(me_ref[0] + groups - k, groups)
        product = dot(sums_refs[k][...], weight_ref[g], 0, 1)
        total = product if total is None else total + product
    out_ref[...] = total.astype(bf16)


def sum_parts_kernel(parts_ref, out_ref):
    total = parts_ref[0].astype(f32)
    for k in range(1, parts_ref.shape[0]):
        total = total + parts_ref[k].astype(f32)
    low = total.astype(bf16)
    for k in range(out_ref.shape[0]):
        out_ref[k] = low


def finish_kernel(parts_ref, key_ref, value_ref):
    for pair in range(parts_ref.shape[0] // 2):
        at = slice(pair * LANES, (pair + 1) * LANES)
        first = parts_ref[2 * pair].astype(f32).T
        second = parts_ref[2 * pair + 1].astype(f32).T
        key_ref[:, at], value_ref[:, at] = merge_pair(first, second)


def exchange(x, axes):
    return lax.all_to_all(x, axes, split_axis=0, concat_axis=0, tiled=True)


def shift(x, axis, size, by):
    return lax.ppermute(x, axis, [(k, (k + by) % size) for k in range(size)])


def per_device(inputs, w_key, w_value, queries, cotangent, cum_gate, **sizes):
    return program(inputs, w_key, w_value, queries, cotangent, cum_gate, **sizes)


def program(inputs, w_key, w_value, queries, cotangent, cum_gate, *, heads, dp, zs, xs):
    _, positions, features = inputs.shape
    kv_width = w_key.shape[1]
    rows = inputs.reshape(positions, features)
    me = lax.axis_index("x").astype(jnp.int32).reshape(1)
    to_head = [(head, head % zs * xs + head // zs) for head in range(heads)]

    packed = call(
        functools.partial(pack_queries_kernel, members=zs),
        shape((heads, positions, LANES)),
        queries.reshape(positions, -1), cotangent.reshape(positions, -1),
    )
    head_rows = exchange(packed, SP).reshape(heads * positions, LANES)
    cum = lax.ppermute(cum_gate[0], SP, to_head)
    near_rows = [rows] + [shift(rows, "x", xs, k) for k in range(1, xs)]
    weight = call(pack_weights_kernel, shape((w_key.shape[0], LANES)), me, w_key, w_value)
    weight = lax.all_gather(weight, "dp", axis=0, tiled=True)
    projected, copies = call(
        project_kernel,
        (shape((zs, xs, positions, LANES)), shape((xs, features, LANES))),
        me, weight, *near_rows,
    )
    head_kv = exchange(projected, "z").reshape(heads * positions, LANES)
    head_kv, copies = lax.optimization_barrier((head_kv, copies))
    weights = exchange(copies, "x")

    dq, dkv, grad_cum = attend(head_rows, head_kv, cum, xs)
    terms = exchange(dkv, "z")
    query_parts = exchange(dq, SP)
    *sums, part = call(
        group_sum_kernel,
        (*[shape((LANES, positions))] * xs, shape((dp, LANES, LANES))),
        me, terms, *near_rows,
    )
    own_sums = [sums[0]] + [shift(sums[k], "x", xs, k) for k in range(1, xs)]
    grad_input = call(grad_input_kernel, shape((positions, features)), me, weights, *own_sums)
    grad_cum = lax.ppermute(grad_cum, SP, [(b, a) for a, b in to_head])
    parts = exchange(part, "dp")
    grad_queries = call(
        functools.partial(unpack_queries_kernel, members=zs),
        shape((positions, features)), query_parts,
    )
    along = call(sum_parts_kernel, shape((zs, LANES, LANES)), parts)
    along = exchange(along, "z")
    along = call(sum_parts_kernel, shape((xs, LANES, LANES)), along)
    along = exchange(along, "x")
    half = shape((LANES, kv_width), f32)
    grad_key, grad_value = call(finish_kernel, (half, half), along)
    return grad_input[None], grad_queries[None], grad_cum[None], grad_key, grad_value


def solution(mesh):
    sizes = {"heads": mesh.shape["sp"], "dp": mesh.shape["dp"], "zs": 8, "xs": 4}
    split = Mesh(mesh.devices.reshape(sizes["zs"], sizes["xs"], sizes["dp"]), ("z", "x", "dp"))
    rows = P("dp", SP, None)
    weights = P("dp", None)
    return jax.shard_map(
        functools.partial(per_device, **sizes),
        mesh=split,
        in_specs=(rows, weights, weights, rows, rows, rows),
        out_specs=(rows, rows, rows, weights, weights),
        check_vma=False,
    )
```

time: 309 us -> 319 us (1.032)
  the two profiles are of different devices: /device:TPU:8 before, /device:TPU:6 now
where the time goes in v3:
time: 319 us; the launch traced here: 318 us
  waiting for transfers between devices  93.5 us (29%)
  blocking collectives  87.5 us (27%)
  Pallas kernels  68.9 us (22%)
  starting transfers between devices  62.6 us (20%)
  local copies, waits for them, and re-layouts  4.63 us (1%)
    all_to_all x3, blocking collectives, exchange(): return lax.all_to_all(x, axes, split_axis=0, concat_axis=0, tiled=True)  70.1 us
    pallas_call x10, Pallas kernels, call(): pl.pallas_call(kernel, out_shape=out_shapes, in_specs=[pl.BlockSpec(memor...  68.9 us
    all_to_all x5, waiting for transfers between devices, exchange(): return lax.all_to_all(x, axes, split_axis=0, concat_axis=0, tiled=True)  66.6 us
    all_to_all x5, starting transfers between devices, exchange(): return lax.all_to_all(x, axes, split_axis=0, concat_axis=0, tiled=True)  32 us
    ppermute x1, waiting for transfers between devices, program(): cum = lax.ppermute(cum_gate[0], SP, to_head)  21.7 us
    ppermute x6, starting transfers between devices, shift(): return lax.ppermute(x, axis, [(k, (k + by) % size) for k in range(size)])  21.1 us
    all_gather x1, blocking collectives, program(): weight = lax.all_gather(weight, 'dp', axis=0, tiled=True)  17.3 us
  transfers between devices with their start and end apart: 13, of which 6 were waited for; matrix products, arithmetic and copies ran while one was open for 0% of the time, Pallas kernels for 4%

profile of v3, /device:TPU:6, one launch (start us, length us, event | category | flops | bytes accessed | tf_op | source)
XLA Modules:
  0.0 318.0 jit_solution(16095081489405078944)
XLA Ops:
  0.6 7.7 %collective-permute-start = (bf16[128,2048]{1,0:T(8,128)(2,1)}, bf16[128,2048]{1,0:T(8,128)(2,1)S(1)}, u32[]{:S(2)}, u32[]{:S(2)}) collective-permute-start(bf16[128,2048]{1,0:T(8,128)(2,1)} %bitcast.12), channel_id=1, source_target_pairs={{0,16},{16,32},{32,48},{48,0},{1,17},{17,33},{33,49},{49,1},{2,18}... | collective-permute-start | bytes 1572872 | tf_op jit(solution)/shard_map/ppermute | solution.py:314
  8.4 1.9 collective-permute-start.1
  10.3 2.8 collective-permute-start.2
  13.1 1.6 shard_map.101
  14.7 17.3 %all_gather.3.weight_ref = bf16[2048,128]{1,0:T(8,128)(2,1)} all-gather(bf16[128,128]{1,0:T(8,128)(2,1)} %shard_map.101), channel_id=1, replica_groups=mesh['z'=8,'x'=4,'dp'=16] {'dp'}, dimensions={0}, use_global_device_ids=true | all-gather | bytes 557056 | tf_op jit(solution)/shard_map/all_gather | solution.py:337
  32.0 0.0 collective-permute-done.refs_1_
  32.0 0.0 collective-permute-done.1.refs_2_
  32.0 0.0 copy-start.5
  32.0 0.0 collective-permute-done.2.refs_3_
  32.0 0.8 copy-done.4
  32.8 0.2 copy-done.5
  33.0 0.8 copy-done.6
  33.8 3.6 %shard_map.102 = (bf16[8,4,128,128]{3,2,1,0:T(8,128)(2,1)}, bf16[4,2048,128]{2,1,0:T(8,128)(2,1)}) custom-call(s32[1]{0:T(128)} %bitcast.me_ref, bf16[2048,128]{1,0:T(8,128)(2,1)} %all_gather.3.weight_ref, bf16[128,2048]{1,0:T(8,128)(2,1)} %bitcast.15, bf16[128,2048]{1,0:T(8,128)(2,1)} %copy-done.4, bf16[128,2048]{1,0:T(8,128)(2,1)} %copy-done.5, ...), custom_call_target="tpu_custom_call" | custom-call | tf_op jit(solution)/shard_map/pallas_call | solution.py:48
  37.4 9.8 %all-to-all-start = ((bf16[8,4,128,128]{3,2,1,0:T(8,128)(2,1)}), bf16[8,4,128,128]{3,2,1,0:T(8,128)(2,1)S(1)}, u32[]{:S(2)}, u32[]{:S(2)}) async-start(bf16[8,4,128,128]{3,2,1,0:T(8,128)(2,1)} %get-tuple-element.19), calls=%async_computation | async-start | bytes 2097152 | tf_op jit(solution)/shard_map/all_to_all | solution.py:310
  47.3 2.6 shard_map.103
  49.9 26.7 %all-to-all-done = bf16[8,4,128,128]{3,2,1,0:T(8,128)(2,1)S(1)} async-done(((bf16[8,4,128,128]{3,2,1,0:T(8,128)(2,1)}), bf16[8,4,128,128]{3,2,1,0:T(8,128)(2,1)S(1)}, u32[]{:S(2)}, u32[]{:S(2)}) %all-to-all-start) | async-done | bytes 1048608 | tf_op jit(solution)/shard_map/all_to_all | solution.py:310
  76.5 6.8 %all-to-all-start.2 = ((bf16[32,128,128]{2,1,0:T(8,128)(2,1)}), bf16[32,128,128]{2,1,0:T(8,128)(2,1)S(1)}, u32[]{:S(2)}, u32[]{:S(2)}) async-start(bf16[32,128,128]{2,1,0:T(8,128)(2,1)} %shard_map.103), calls=%async_computation.2 | async-start | bytes 2097152 | tf_op jit(solution)/shard_map/all_to_all | solution.py:310
  83.4 5.2 %collective-permute-start.3 = (f32[1,4096]{1,0:T(1,128)S(1)}, f32[1,4096]{1,0:T(1,128)S(1)}, u32[]{:S(2)}, u32[]{:S(2)}) collective-permute-start(f32[1,4096]{1,0:T(1,128)S(1)} %bitcast.22), channel_id=1, source_target_pairs={{0,0},{16,64},{32,128},{48,192},{64,256},{80,320},{96,384},{112,44... | collective-permute-start | bytes 49160 | tf_op jit(solution)/shard_map/ppermute | solution.py:334
  88.6 21.7 %collective-permute-done.3.cum_ref = f32[1,4096]{1,0:T(1,128)S(1)} collective-permute-done((f32[1,4096]{1,0:T(1,128)S(1)}, f32[1,4096]{1,0:T(1,128)S(1)}, u32[]{:S(2)}, u32[]{:S(2)}) %collective-permute-start.3) | collective-permute-done | bytes 16416 | tf_op jit(solution)/shard_map/ppermute | solution.py:334
  110.3 1.0 all-to-all-done.2
  111.4 1.0 copy-done.2
  112.4 47.2 %shard_map.104 = (bf16[32,64,128]{2,1,0:T(8,128)(2,1)}, bf16[8,4,128,128]{3,2,1,0:T(8,128)(2,1)}, f32[1,4096]{1,0:T(1,128)}) custom-call(bf16[4096,128]{1,0:T(8,128)(2,1)} %bitcast.11, bf16[4096,128]{1,0:T(8,128)(2,1)} %bitcast.10, f32[1,4096]{1,0:T(1,128)} %copy-done.11), custom_call_target="tpu_custom_call" | custom-call | tf_op jit(solution)/shard_map/pallas_call | solution.py:48
  159.6 33.2 %all_to_all.40.terms_ref = bf16[8,4,128,128]{3,2,1,0:T(8,128)(2,1)} all-to-all(bf16[8,4,128,128]{3,2,1,0:T(8,128)(2,1)} %get-tuple-element.23), channel_id=1, replica_groups=mesh['z'=8,'x'=4,'dp'=16] {'z'}, dimensions={0} | all-to-all | bytes 2097152 | tf_op jit(solution)/shard_map/all_to_all | solution.py:310
  192.8 3.3 %shard_map.105 = (bf16[128,128]{1,0:T(8,128)(2,1)}, bf16[128,128]{1,0:T(8,128)(2,1)}, bf16[128,128]{1,0:T(8,128)(2,1)}, bf16[128,128]{1,0:T(8,128)(2,1)}, bf16[16,128,128]{2,1,0:T(8,128)(2,1)}) custom-call(s32[1]{0:T(128)} %bitcast.me_ref, bf16[8,4,128,128]{3,2,1,0:T(8,128)(2,1)} %all_to_all.40.terms_ref, bf16[128,2048]{1,0:T(8,128)(2,1)} %bitcast.16, ...), custom_call_target="tpu_custom_call" | custom-call | tf_op jit(solution)/shard_map/pallas_call | solution.py:48
  196.1 20.5 %all_to_all.41.parts_ref = bf16[16,128,128]{2,1,0:T(8,128)(2,1)} all-to-all(bf16[16,128,128]{2,1,0:T(8,128)(2,1)} %get-tuple-element.30), channel_id=1, replica_groups=mesh['z'=8,'x'=4,'dp'=16] {'dp'}, dimensions={0} | all-to-all | bytes 1048576 | tf_op jit(solution)/shard_map/all_to_all | solution.py:310
  216.5 5.0 %all-to-all-start.4 = ((bf16[32,64,128]{2,1,0:T(8,128)(2,1)}), bf16[32,64,128]{2,1,0:T(8,128)(2,1)S(1)}, u32[]{:S(2)}, u32[]{:S(2)}) async-start(bf16[32,64,128]{2,1,0:T(8,128)(2,1)} %get-tuple-element.28), calls=%async_computation.4 | async-start | bytes 1048576 | tf_op jit(solution)/shard_map/all_to_all | solution.py:310
  221.6 1.8 shard_map.108
  223.4 16.1 %all-to-all-done.4.packed_ref = bf16[32,64,128]{2,1,0:T(8,128)(2,1)S(1)} async-done(((bf16[32,64,128]{2,1,0:T(8,128)(2,1)}), bf16[32,64,128]{2,1,0:T(8,128)(2,1)S(1)}, u32[]{:S(2)}, u32[]{:S(2)}) %all-to-all-start.4) | async-done | bytes 524320 | tf_op jit(solution)/shard_map/all_to_all | solution.py:310
  239.5 16.5 %all_to_all.42.parts_ref = bf16[8,128,128]{2,1,0:T(8,128)(2,1)} all-to-all(bf16[8,128,128]{2,1,0:T(8,128)(2,1)} %shard_map.108), channel_id=1, replica_groups=mesh['z'=8,'x'=4,'dp'=16] {'z'}, dimensions={0} | all-to-all | bytes 524288 | tf_op jit(solution)/shard_map/all_to_all | solution.py:310
  256.0 4.9 %all-to-all-start.1 = ((bf16[4,2048,128]{2,1,0:T(8,128)(2,1)}), bf16[4,2048,128]{2,1,0:T(8,128)(2,1)S(1)}, u32[]{:S(2)}, u32[]{:S(2)}) async-start(bf16[4,2048,128]{2,1,0:T(8,128)(2,1)} %get-tuple-element.21), calls=%async_computation.1 | async-start | bytes 4194304 | tf_op jit(solution)/shard_map/all_to_all | solution.py:310
  261.0 1.6 shard_map.109
  262.6 22.8 %all-to-all-done.1.weight_ref = bf16[4,2048,128]{2,1,0:T(8,128)(2,1)S(1)} async-done(((bf16[4,2048,128]{2,1,0:T(8,128)(2,1)}), bf16[4,2048,128]{2,1,0:T(8,128)(2,1)S(1)}, u32[]{:S(2)}, u32[]{:S(2)}) %all-to-all-start.1) | async-done | bytes 2097184 | tf_op jit(solution)/shard_map/all_to_all | solution.py:310
  285.4 5.4 %all-to-all-start.7 = ((bf16[4,128,128]{2,1,0:T(8,128)(2,1)}), bf16[4,128,128]{2,1,0:T(8,128)(2,1)S(1)}, u32[]{:S(2)}, u32[]{:S(2)}) async-start(bf16[4,128,128]{2,1,0:T(8,128)(2,1)} %shard_map.109), calls=%async_computation.7 | async-start | bytes 262144 | tf_op jit(solution)/shard_map/all_to_all | solution.py:310
  290.8 2.0 collective-permute-start.4
  292.8 4.8 %collective-permute-start.5 = (bf16[128,128]{1,0:T(8,128)(2,1)S(1)}, bf16[128,128]{1,0:T(8,128)(2,1)S(1)}, u32[]{:S(2)}, u32[]{:S(2)}) collective-permute-start(bf16[128,128]{1,0:T(8,128)(2,1)S(1)} %copy-done.13), channel_id=1, source_target_pairs={{0,32},{16,48},{32,0},{48,16},{1,33},{17,49},{33,1},{49,17},{2,34}... | collective-permute-start | bytes 98312 | tf_op jit(solution)/shard_map/ppermute | solution.py:314
  297.6 1.9 collective-permute-start.6
  299.5 4.3 %collective-permute-start.7 = (f32[1,4096]{1,0:T(1,128)S(1)}, f32[1,4096]{1,0:T(1,128)S(1)}, u32[]{:S(2)}, u32[]{:S(2)}) collective-permute-start(f32[1,4096]{1,0:T(1,128)S(1)} %copy-done.16), channel_id=1, source_target_pairs={{0,0},{64,16},{128,32},{192,48},{256,64},{320,80},{384,96},{448,11... | collective-permute-start | bytes 49160 | tf_op jit(solution)/shard_map/ppermute | solution.py:357
  303.8 5.2 %collective-permute-done.7 = f32[1,4096]{1,0:T(1,128)S(1)} collective-permute-done((f32[1,4096]{1,0:T(1,128)S(1)}, f32[1,4096]{1,0:T(1,128)S(1)}, u32[]{:S(2)}, u32[]{:S(2)}) %collective-permute-start.7) | collective-permute-done | bytes 16416 | tf_op jit(solution)/shard_map/ppermute | solution.py:357
  309.1 2.1 shard_map.107
  311.1 0.0 collective-permute-done.4.refs_1_
  311.1 0.0 collective-permute-done.5.refs_2_
  311.2 0.6 copy-done.8
  311.8 0.0 copy-done.9
  311.8 0.0 copy-done.10
  311.8 3.2 shard_map.106
  314.9 0.6 copy-done.7
  315.6 1.8 shard_map.110
  317.4 0.6 copy.12
  (27 shorter events, 0.1 us)
Async XLA Ops:
  0.6 31.4 %collective-permute-start = (bf16[128,2048]{1,0:T(8,128)(2,1)}, bf16[128,2048]{1,0:T(8,128)(2,1)S(1)}, u32[]{:S(2)}, u32[]{:S(2)}) collective-permute-start(bf16[128,2048]{1,0:T(8,128)(2,1)} %bitcast.12), channel_id=1, source_target_pairs={{0,16},{16,32},{32,48},{48,0},{1,17},{17,33},{33,49},{49,1},{2,18}... | collective-permute-start | bytes 1572872 | tf_op jit(solution)/shard_map/ppermute | solution.py:314
  8.4 23.6 %collective-permute-start.1 = (bf16[128,2048]{1,0:T(8,128)(2,1)}, bf16[128,2048]{1,0:T(8,128)(2,1)S(1)}, u32[]{:S(2)}, u32[]{:S(2)}) collective-permute-start(bf16[128,2048]{1,0:T(8,128)(2,1)} %bitcast.13), channel_id=1, source_target_pairs={{0,32},{16,48},{32,0},{48,16},{1,33},{17,49},{33,1},{49,17},{2,34}... | collective-permute-start | bytes 1572872 | tf_op jit(solution)/shard_map/ppermute | solution.py:314
  10.3 21.7 %collective-permute-start.2 = (bf16[128,2048]{1,0:T(8,128)(2,1)}, bf16[128,2048]{1,0:T(8,128)(2,1)S(1)}, u32[]{:S(2)}, u32[]{:S(2)}) collective-permute-start(bf16[128,2048]{1,0:T(8,128)(2,1)} %bitcast.14), channel_id=1, source_target_pairs={{0,48},{16,0},{32,16},{48,32},{1,49},{17,1},{33,17},{49,33},{2,50}... | collective-permute-start | bytes 1572872 | tf_op jit(solution)/shard_map/ppermute | solution.py:314
  32.0 0.8 copy-start.4
  32.0 1.0 copy-start.5
  33.0 0.8 copy-start.6
  37.4 39.1 %all-to-all-start = ((bf16[8,4,128,128]{3,2,1,0:T(8,128)(2,1)}), bf16[8,4,128,128]{3,2,1,0:T(8,128)(2,1)S(1)}, u32[]{:S(2)}, u32[]{:S(2)}) async-start(bf16[8,4,128,128]{3,2,1,0:T(8,128)(2,1)} %get-tuple-element.19), calls=%async_computation | async-start | bytes 2097152 | tf_op jit(solution)/shard_map/all_to_all | solution.py:310
  47.2 36.1 %copy-start.15 = (f32[1,1,4096]{2,1,0:T(1,128)S(1)}, f32[1,1,4096]{2,1,0:T(1,128)}, u32[]{:S(2)}) copy-start(f32[1,1,4096]{2,1,0:T(1,128)} %param.11) | copy-start | bytes 49156
  76.5 34.8 %copy-start.1 = (bf16[8,4,128,128]{3,2,1,0:T(8,128)(2,1)}, bf16[8,4,128,128]{3,2,1,0:T(8,128)(2,1)S(1)}, u32[]{:S(2)}) copy-start(bf16[8,4,128,128]{3,2,1,0:T(8,128)(2,1)S(1)} %all-to-all-done) | copy-start | bytes 3145732
  76.5 34.8 %all-to-all-start.2 = ((bf16[32,128,128]{2,1,0:T(8,128)(2,1)}), bf16[32,128,128]{2,1,0:T(8,128)(2,1)S(1)}, u32[]{:S(2)}, u32[]{:S(2)}) async-start(bf16[32,128,128]{2,1,0:T(8,128)(2,1)} %shard_map.103), calls=%async_computation.2 | async-start | bytes 2097152 | tf_op jit(solution)/shard_map/all_to_all | solution.py:310
  83.4 26.9 %collective-permute-start.3 = (f32[1,4096]{1,0:T(1,128)S(1)}, f32[1,4096]{1,0:T(1,128)S(1)}, u32[]{:S(2)}, u32[]{:S(2)}) collective-permute-start(f32[1,4096]{1,0:T(1,128)S(1)} %bitcast.22), channel_id=1, source_target_pairs={{0,0},{16,64},{32,128},{48,192},{64,256},{80,320},{96,384},{112,44... | collective-permute-start | bytes 49160 | tf_op jit(solution)/shard_map/ppermute | solution.py:334
  110.3 1.0 copy-start.11
  111.4 1.0 copy-start.2
  216.5 23.0 %all-to-all-start.4 = ((bf16[32,64,128]{2,1,0:T(8,128)(2,1)}), bf16[32,64,128]{2,1,0:T(8,128)(2,1)S(1)}, u32[]{:S(2)}, u32[]{:S(2)}) async-start(bf16[32,64,128]{2,1,0:T(8,128)(2,1)} %get-tuple-element.28), calls=%async_computation.4 | async-start | bytes 1048576 | tf_op jit(solution)/shard_map/all_to_all | solution.py:310
  239.5 16.5 %copy-start.3 = (bf16[32,64,128]{2,1,0:T(8,128)(2,1)}, bf16[32,64,128]{2,1,0:T(8,128)(2,1)S(1)}, u32[]{:S(2)}) copy-start(bf16[32,64,128]{2,1,0:T(8,128)(2,1)S(1)} %all-to-all-done.4.packed_ref) | copy-start | bytes 1572868
  256.0 34.8 %copy-start.14 = (bf16[128,128]{1,0:T(8,128)(2,1)S(1)}, bf16[128,128]{1,0:T(8,128)(2,1)}, u32[]{:S(2)}) copy-start(bf16[128,128]{1,0:T(8,128)(2,1)} %get-tuple-element.25) | copy-start | bytes 98308
  256.0 36.8 %copy-start.13 = (bf16[128,128]{1,0:T(8,128)(2,1)S(1)}, bf16[128,128]{1,0:T(8,128)(2,1)}, u32[]{:S(2)}) copy-start(bf16[128,128]{1,0:T(8,128)(2,1)} %get-tuple-element.26) | copy-start | bytes 98308
  256.0 41.5 %copy-start.12 = (bf16[128,128]{1,0:T(8,128)(2,1)S(1)}, bf16[128,128]{1,0:T(8,128)(2,1)}, u32[]{:S(2)}) copy-start(bf16[128,128]{1,0:T(8,128)(2,1)} %get-tuple-element.27) | copy-start | bytes 98308
  256.0 43.5 %copy-start.16 = (f32[1,4096]{1,0:T(1,128)S(1)}, f32[1,4096]{1,0:T(1,128)}, u32[]{:S(2)}) copy-start(f32[1,4096]{1,0:T(1,128)} %get-tuple-element.29) | copy-start | bytes 49156
  256.0 29.4 %all-to-all-start.1 = ((bf16[4,2048,128]{2,1,0:T(8,128)(2,1)}), bf16[4,2048,128]{2,1,0:T(8,128)(2,1)S(1)}, u32[]{:S(2)}, u32[]{:S(2)}) async-start(bf16[4,2048,128]{2,1,0:T(8,128)(2,1)} %get-tuple-element.21), calls=%async_computation.1 | async-start | bytes 4194304 | tf_op jit(solution)/shard_map/all_to_all | solution.py:310
  285.4 25.7 %copy-start = (bf16[4,2048,128]{2,1,0:T(8,128)(2,1)}, bf16[4,2048,128]{2,1,0:T(8,128)(2,1)S(1)}, u32[]{:S(2)}) copy-start(bf16[4,2048,128]{2,1,0:T(8,128)(2,1)S(1)} %all-to-all-done.1.weight_ref) | copy-start | bytes 6291460
  285.4 29.5 %all-to-all-start.7 = ((bf16[4,128,128]{2,1,0:T(8,128)(2,1)}), bf16[4,128,128]{2,1,0:T(8,128)(2,1)S(1)}, u32[]{:S(2)}, u32[]{:S(2)}) async-start(bf16[4,128,128]{2,1,0:T(8,128)(2,1)} %shard_map.109), calls=%async_computation.7 | async-start | bytes 262144 | tf_op jit(solution)/shard_map/all_to_all | solution.py:310
  290.8 20.3 %collective-permute-start.4 = (bf16[128,128]{1,0:T(8,128)(2,1)S(1)}, bf16[128,128]{1,0:T(8,128)(2,1)S(1)}, u32[]{:S(2)}, u32[]{:S(2)}) collective-permute-start(bf16[128,128]{1,0:T(8,128)(2,1)S(1)} %copy-done.14), channel_id=1, source_target_pairs={{0,16},{16,32},{32,48},{48,0},{1,17},{17,33},{33,49},{49,1},{2,18}... | collective-permute-start | bytes 98312 | tf_op jit(solution)/shard_map/ppermute | solution.py:314
  292.8 18.4 %collective-permute-start.5 = (bf16[128,128]{1,0:T(8,128)(2,1)S(1)}, bf16[128,128]{1,0:T(8,128)(2,1)S(1)}, u32[]{:S(2)}, u32[]{:S(2)}) collective-permute-start(bf16[128,128]{1,0:T(8,128)(2,1)S(1)} %copy-done.13), channel_id=1, source_target_pairs={{0,32},{16,48},{32,0},{48,16},{1,33},{17,49},{33,1},{49,17},{2,34}... | collective-permute-start | bytes 98312 | tf_op jit(solution)/shard_map/ppermute | solution.py:314
  297.6 13.6 %collective-permute-start.6 = (bf16[128,128]{1,0:T(8,128)(2,1)S(1)}, bf16[128,128]{1,0:T(8,128)(2,1)S(1)}, u32[]{:S(2)}, u32[]{:S(2)}) collective-permute-start(bf16[128,128]{1,0:T(8,128)(2,1)S(1)} %copy-done.12), channel_id=1, source_target_pairs={{0,48},{16,0},{32,16},{48,32},{1,49},{17,1},{33,17},{49,33},{2,50}... | collective-permute-start | bytes 98312 | tf_op jit(solution)/shard_map/ppermute | solution.py:314
  299.5 9.5 %collective-permute-start.7 = (f32[1,4096]{1,0:T(1,128)S(1)}, f32[1,4096]{1,0:T(1,128)S(1)}, u32[]{:S(2)}, u32[]{:S(2)}) collective-permute-start(f32[1,4096]{1,0:T(1,128)S(1)} %copy-done.16), channel_id=1, source_target_pairs={{0,0},{64,16},{128,32},{192,48},{256,64},{320,80},{384,96},{448,11... | collective-permute-start | bytes 49160 | tf_op jit(solution)/shard_map/ppermute | solution.py:357
  311.1 0.6 copy-start.8
  311.1 0.6 copy-start.9
  311.2 0.6 copy-start.10
  314.9 0.6 copy-start.7

commit v4 on v3

--- a/solution.py
+++ b/solution.py
@@ -14,7 +14,8 @@
 LOG2E = 1.4426950408889634
 BLOCK = 512
 ONES = HD + 16
-SP = ("z", "x")
+SP = ("zg", "zp", "x")
+GROUP = ("zp", "x")
 LOWEST = -3.4028235e38
 bf16 = jnp.bfloat16
 f32 = jnp.float32
@@ -62,43 +63,41 @@
     return jax.ShapeDtypeStruct(dims, dtype)
 
 
-def pack_weights_kernel(me_ref, key_ref, value_ref, out_ref):
-    at = pl.ds(pl.multiple_of(lax.div(me_ref[0], 2) * LANES, LANES), LANES)
-    first, second = merge_pair(key_ref[:, at].astype(f32), value_ref[:, at].astype(f32))
-    out_ref[...] = jnp.where(lax.rem(me_ref[0], 2) == 0, first, second).astype(bf16)
-
-
-def pack_queries_kernel(query_ref, grad_ref, out_ref, *, members):
-    heads = out_ref.shape[0]
-    quads = heads // members
-    for pair in range(heads // 2):
+def pack_weights_kernel(key_ref, value_ref, out_ref):
+    for pair in range(key_ref.shape[1] // LANES):
+        at = slice(pair * LANES, (pair + 1) * LANES)
+        blocks = merge_pair(key_ref[:, at].astype(f32), value_ref[:, at].astype(f32))
+        for k in range(2):
+            g = 2 * pair + k
+            out_ref[:, g * LANES : (g + 1) * LANES] = blocks[k].astype(bf16)
+
+
+def pack_queries_kernel(query_ref, grad_ref, out_ref):
+    for pair in range(out_ref.shape[0] // 2):
         at = slice(pair * LANES, (pair + 1) * LANES)
         blocks = merge_pair(query_ref[:, at].astype(f32), grad_ref[:, at].astype(f32))
         for k in range(2):
-            head = 2 * pair + k
-            out_ref[head % members * quads + head // members] = blocks[k].astype(bf16)
-
-
-def project_kernel(me_ref, weight_ref, *refs):
-    rows_refs, (out_ref, copies_ref) = refs[:-2], refs[-2:]
-    quads = len(rows_refs)
-    weight = weight_ref[...]
-    for k in range(quads):
-        owner = lax.rem(me_ref[0] + quads - k, quads)
-        projected = dot(rows_refs[k][...], weight, 1, 0).astype(bf16)
-        for member in range(out_ref.shape[0]):
-            out_ref[member, owner] = projected
-    for k in range(copies_ref.shape[0]):
-        copies_ref[k] = weight
+            out_ref[2 * pair + k] = blocks[k].astype(bf16)
+
+
+def project_kernel(rows_ref, weight_ref, out_ref):
+    projected = dot(rows_ref[...], weight_ref[...], 1, 0).astype(bf16)
+    for g in range(out_ref.shape[0]):
+        out_ref[g] = projected[:, g * LANES : (g + 1) * LANES]
+
+
+def copies_kernel(x_ref, out_ref):
+    for k in range(out_ref.shape[0]):
+        out_ref[k] = x_ref[...]
 
 
 def attend_kernel(
-    x_ref, kv_ref, cum_ref, dq_ref, dkv_ref, gcum_ref,
-    qa_ref, ka_ref, kn_ref, s_ref, dp_ref, xt_ref, dkt_ref, dvt_ref, rows_ref, acc_ref, stat_ref,
+    x_ref, parts_ref, cum_ref, dq_ref, dkv_ref, gcum_ref,
+    kv_ref, qa_ref, ka_ref, kn_ref, s_ref, dp_ref, xt_ref, dkt_ref, dvt_ref, rows_ref, acc_ref, stat_ref,
     *, blk, seq,
 ):
     count = seq // blk
-    quads = dkv_ref.shape[1]
+    members = dkv_ref.shape[0]
     scale = HD**-0.5
     lane = lax.broadcasted_iota(jnp.int32, (blk, LANES), 1)
     low = lane < HD
@@ -110,6 +109,10 @@
     def prepare(i, _):
         at = span(i)
         x = x_ref[at, :].astype(f32)
+        for b in range(blk // LANES):
+            owner = i * (blk // LANES) + b
+            block = parts_ref[lax.rem(owner, members), lax.div(owner, members)]
+            kv_ref[pl.ds(pl.multiple_of(owner * LANES, LANES), LANES), :] = block
         kv = kv_ref[at, :].astype(f32)
         c1, c2, c3 = pieces(jnp.broadcast_to(cum_ref[:, at] * LOG2E, (LANES, blk)))
         one = jnp.ones_like(c1)
@@ -215,23 +218,25 @@
     lax.fori_loop(0, count, query_block, 0)
     for b in range(seq // LANES):
         at = slice(b * LANES, (b + 1) * LANES)
-        dkv_ref[b // quads, b % quads, 0:HD, :] = (dkt_ref[0:HD, at] * scale).astype(bf16)
-        dkv_ref[b // quads, b % quads, HD:, :] = dvt_ref[:, at].astype(bf16)
+        dkv_ref[b % members, b // members, 0:HD, :] = (dkt_ref[0:HD, at] * scale).astype(bf16)
+        dkv_ref[b % members, b // members, HD:, :] = dvt_ref[:, at].astype(bf16)
     gcum_ref[...] = rows_ref[0:1, :] - dkt_ref[HD : HD + 1, :]
 
 
-def attend(x, kv, cum, quads):
+def attend(x, parts, cum):
+    members = parts.shape[0]
     seq = x.shape[0]
     owners = seq // LANES
     return call(
         functools.partial(attend_kernel, blk=BLOCK, seq=seq),
         (
             shape((owners, HD, LANES)),
-            shape((owners // quads, quads, LANES, LANES)),
+            shape((members, owners // members, LANES, LANES)),
             shape((1, seq), f32),
         ),
-        x, kv, cum,
+        x, parts, cum,
         scratch=[
+            VMEM((seq, LANES), bf16),
             VMEM((seq, 2 * LANES), bf16),
             VMEM((seq, 2 * LANES), bf16),
             VMEM((seq, LANES), bf16),
@@ -247,9 +252,9 @@
     )
 
 
-def group_sum_kernel(me_ref, terms_ref, *refs):
+def group_sum_kernel(me_ref, terms_ref, rows_ref, *refs):
     owners = terms_ref.shape[1]
-    rows_refs, sums_refs, part_ref = refs[:owners], refs[owners : 2 * owners], refs[2 * owners]
+    sums_refs, part_ref = refs[:owners], refs[owners]
     part = None
     for k in range(owners):
         owner = lax.rem(me_ref[0] + k, owners)
@@ -258,21 +263,17 @@
             total = total + terms_ref[member, owner].astype(f32)
         low = total.astype(bf16)
         sums_refs[k][...] = low
-        product = dot(low, rows_refs[(owners - k) % owners][...], 1, 0)
+        product = dot(low, rows_ref[owner], 1, 0)
         part = product if part is None else part + product
     for chunk in range(part_ref.shape[0]):
         part_ref[chunk] = part[:, chunk * LANES : (chunk + 1) * LANES].astype(bf16)
 
 
-def unpack_queries_kernel(packed_ref, out_ref, *, members):
-    heads = packed_ref.shape[0]
-    quads = heads // members
-    for pair in range(heads // 2):
-        blocks = [
-            packed_ref[head % members * quads + head // members].astype(f32)
-            for head in (2 * pair, 2 * pair + 1)
-        ]
-        upper, lower = merge_pair(*blocks)
+def unpack_queries_kernel(packed_ref, out_ref):
+    for pair in range(packed_ref.shape[0] // 2):
+        upper, lower = merge_pair(
+            packed_ref[2 * pair].astype(f32), packed_ref[2 * pair + 1].astype(f32)
+        )
         at = slice(pair * LANES, (pair + 1) * LANES)
         out_ref[0:HD, at] = upper.astype(bf16)
         out_ref[HD:, at] = lower.astype(bf16)
@@ -284,7 +285,8 @@
     total = None
     for k in range(groups):
         g = lax.rem(me_ref[0] + groups - k, groups)
-        product = dot(sums_refs[k][...], weight_ref[g], 0, 1)
+        columns = pl.ds(pl.multiple_of(g * LANES, LANES), LANES)
+        product = dot(sums_refs[k][...], weight_ref[:, columns], 0, 1)
         total = product if total is None else total + product
     out_ref[...] = total.astype(bf16)
 
@@ -310,6 +312,10 @@
     return lax.all_to_all(x, axes, split_axis=0, concat_axis=0, tiled=True)
 
 
+def gather(x, axes, tiled):
+    return lax.all_gather(x, axes, axis=0, tiled=tiled)
+
+
 def shift(x, axis, size, by):
     return lax.ppermute(x, axis, [(k, (k + by) % size) for k in range(size)])
 
@@ -318,60 +324,55 @@
     return program(inputs, w_key, w_value, queries, cotangent, cum_gate, **sizes)
 
 
-def program(inputs, w_key, w_value, queries, cotangent, cum_gate, *, heads, dp, zs, xs):
+def program(inputs, w_key, w_value, queries, cotangent, cum_gate, *, heads, dp, zg, zp, xs):
     _, positions, features = inputs.shape
     kv_width = w_key.shape[1]
+    kv_heads = kv_width // HD
+    members = zp * xs
     rows = inputs.reshape(positions, features)
-    me = lax.axis_index("x").astype(jnp.int32).reshape(1)
-    to_head = [(head, head % zs * xs + head // zs) for head in range(heads)]
-
+    me = lax.axis_index("zg").astype(jnp.int32).reshape(1)
+
+    weight = call(pack_weights_kernel, shape((w_key.shape[0], 2 * kv_width)), w_key, w_value)
+    weight = gather(weight, "dp", True)
     packed = call(
-        functools.partial(pack_queries_kernel, members=zs),
-        shape((heads, positions, LANES)),
+        pack_queries_kernel, shape((heads, positions, LANES)),
         queries.reshape(positions, -1), cotangent.reshape(positions, -1),
     )
     head_rows = exchange(packed, SP).reshape(heads * positions, LANES)
-    cum = lax.ppermute(cum_gate[0], SP, to_head)
-    near_rows = [rows] + [shift(rows, "x", xs, k) for k in range(1, xs)]
-    weight = call(pack_weights_kernel, shape((w_key.shape[0], LANES)), me, w_key, w_value)
-    weight = lax.all_gather(weight, "dp", axis=0, tiled=True)
-    projected, copies = call(
-        project_kernel,
-        (shape((zs, xs, positions, LANES)), shape((xs, features, LANES))),
-        me, weight, *near_rows,
-    )
-    head_kv = exchange(projected, "z").reshape(heads * positions, LANES)
-    head_kv, copies = lax.optimization_barrier((head_kv, copies))
-    weights = exchange(copies, "x")
-
-    dq, dkv, grad_cum = attend(head_rows, head_kv, cum, xs)
-    terms = exchange(dkv, "z")
+    projected = call(project_kernel, shape((kv_heads, positions, LANES)), rows, weight)
+    group_kv = exchange(projected, "zg")
+    copies = call(copies_kernel, shape((members, *group_kv.shape)), group_kv)
+    head_kv = exchange(copies, GROUP)
+    head_kv, late_rows = lax.optimization_barrier((head_kv, rows))
+    near_rows = gather(late_rows, "zg", False)
+
+    dq, dkv, grad_cum = attend(head_rows, head_kv, cum_gate[0])
+    terms = exchange(dkv, GROUP)
     query_parts = exchange(dq, SP)
     *sums, part = call(
         group_sum_kernel,
-        (*[shape((LANES, positions))] * xs, shape((dp, LANES, LANES))),
-        me, terms, *near_rows,
-    )
-    own_sums = [sums[0]] + [shift(sums[k], "x", xs, k) for k in range(1, xs)]
-    grad_input = call(grad_input_kernel, shape((positions, features)), me, weights, *own_sums)
-    grad_cum = lax.ppermute(grad_cum, SP, [(b, a) for a, b in to_head])
+        (*[shape((LANES, positions))] * zg, shape((dp, LANES, LANES))),
+        me, terms, near_rows,
+    )
+    own_sums = [sums[0]] + [shift(sums[k], "zg", zg, k) for k in range(1, zg)]
+    grad_input = call(grad_input_kernel, shape((positions, features)), me, weight, *own_sums)
     parts = exchange(part, "dp")
-    grad_queries = call(
-        functools.partial(unpack_queries_kernel, members=zs),
-        shape((positions, features)), query_parts,
-    )
-    along = call(sum_parts_kernel, shape((zs, LANES, LANES)), parts)
-    along = exchange(along, "z")
-    along = call(sum_parts_kernel, shape((xs, LANES, LANES)), along)
-    along = exchange(along, "x")
+    grad_queries = call(unpack_queries_kernel, shape((positions, features)), query_parts)
+    along = call(sum_parts_kernel, shape((members, LANES, LANES)), parts)
+    along = exchange(along, GROUP)
+    along = call(sum_parts_kernel, shape((zg, LANES, LANES)), along)
+    along = exchange(along, "zg")
     half = shape((LANES, kv_width), f32)
     grad_key, grad_value = call(finish_kernel, (half, half), along)
     return grad_input[None], grad_queries[None], grad_cum[None], grad_key, grad_value
 
 
 def solution(mesh):
-    sizes = {"heads": mesh.shape["sp"], "dp": mesh.shape["dp"], "zs": 8, "xs": 4}
-    split = Mesh(mesh.devices.reshape(sizes["zs"], sizes["xs"], sizes["dp"]), ("z", "x", "dp"))
+    sizes = {"heads": mesh.shape["sp"], "dp": mesh.shape["dp"], "zg": 4, "zp": 2, "xs": 4}
+    split = Mesh(
+        mesh.devices.reshape(sizes["zg"], sizes["zp"], sizes["xs"], sizes["dp"]),
+        ("zg", "zp", "x", "dp"),
+    )
     rows = P("dp", SP, None)
     weights = P("dp", None)
     return jax.shard_map(

time: 319 us -> 296 us (0.928)
  the two profiles are of different devices: /device:TPU:6 before, /device:TPU:2 now
where the time goes in v4:
time: 296 us; the launch traced here: 295 us
  waiting for transfers between devices  118 us (40%)
  Pallas kernels  70.3 us (24%)
  blocking collectives  48.1 us (16%)
  starting transfers between devices  41 us (14%)
  between operations  14.2 us (5%)
  local copies, waits for them, and re-layouts  3.25 us (1%)
    pallas_call x11, Pallas kernels, call(): pl.pallas_call(kernel, out_shape=out_shapes, in_specs=[pl.BlockSpec(memor...  70.3 us
    all_to_all x5, waiting for transfers between devices, exchange(): return lax.all_to_all(x, axes, split_axis=0, concat_axis=0, tiled=True)  69.3 us
    all_gather x2, waiting for transfers between devices, gather(): return lax.all_gather(x, axes, axis=0, tiled=tiled)  48.2 us
    all_to_all x3, blocking collectives, exchange(): return lax.all_to_all(x, axes, split_axis=0, concat_axis=0, tiled=True)  48.1 us
    all_to_all x5, starting transfers between devices, exchange(): return lax.all_to_all(x, axes, split_axis=0, concat_axis=0, tiled=True)  25.2 us
    ppermute x3, starting transfers between devices, shift(): return lax.ppermute(x, axis, [(k, (k + by) % size) for k in range(size)])  15.7 us
  transfers between devices with their start and end apart: 10, of which 5 were waited for; matrix products, arithmetic and copies ran while one was open for 0% of the time, Pallas kernels for 19%

profile of v4, /device:TPU:2, one launch (start us, length us, event | category | flops | bytes accessed | tf_op | source)
XLA Modules:
  0.0 295.1 jit_solution(3021319033426474558)
XLA Ops:
  7.2 0.0 all-gather.4.cloned.1.call-start
  7.2 1.6 shard_map.101
  8.8 0.0 all-gather.4.cloned.1.call-update
  8.9 48.2 %all-gather.4.cloned.1.call-done.weight_ref = bf16[2048,512]{1,0:T(8,128)(2,1)} async-done(((bf16[128,512]{1,0:T(8,128)(2,1)}), bf16[2048,512]{1,0:T(8,128)(2,1)}) %all-gather.4.cloned.1.call-update) | async-done | bytes 2097168 | tf_op jit(solution)/shard_map/all_gather | solution.py:316
  57.1 2.9 shard_map.103
  60.0 16.7 %all_to_all.40.x_ref = bf16[4,128,128]{2,1,0:T(8,128)(2,1)} all-to-all(bf16[4,128,128]{2,1,0:T(8,128)(2,1)} %shard_map.103), channel_id=1, replica_groups=mesh['zg'=4,'zp'=2,'x'=4,'dp'=16] {'zg'}, dimensions={0} | all-to-all | bytes 262144 | tf_op jit(solution)/shard_map/all_to_all | solution.py:312
  76.7 2.0 shard_map.104
  78.7 5.1 %all-to-all-start.2 = ((bf16[8,4,128,128]{3,2,1,0:T(8,128)(2,1)}), bf16[8,4,128,128]{3,2,1,0:T(8,128)(2,1)S(1)}, u32[]{:S(2)}, u32[]{:S(2)}) async-start(bf16[8,4,128,128]{3,2,1,0:T(8,128)(2,1)} %shard_map.104), calls=%async_computation.2 | async-start | bytes 2097152 | tf_op jit(solution)/shard_map/all_to_all | solution.py:312
  83.8 2.6 shard_map.102
  86.4 9.1 %all-to-all-done.2.parts_ref = bf16[8,4,128,128]{3,2,1,0:T(8,128)(2,1)S(1)} async-done(((bf16[8,4,128,128]{3,2,1,0:T(8,128)(2,1)}), bf16[8,4,128,128]{3,2,1,0:T(8,128)(2,1)S(1)}, u32[]{:S(2)}, u32[]{:S(2)}) %all-to-all-start.2) | async-done | bytes 1048608 | tf_op jit(solution)/shard_map/all_to_all | solution.py:312
  95.6 6.2 %all-to-all-start = ((bf16[32,128,128]{2,1,0:T(8,128)(2,1)}), bf16[32,128,128]{2,1,0:T(8,128)(2,1)S(1)}, u32[]{:S(2)}, u32[]{:S(2)}) async-start(bf16[32,128,128]{2,1,0:T(8,128)(2,1)} %shard_map.102), calls=%async_computation | async-start | bytes 2097152 | tf_op jit(solution)/shard_map/all_to_all | solution.py:312
  101.8 0.0 all-gather.6.cloned.1.call-start
  101.8 0.7 all-gather.6.cloned.1.call-update
  102.5 33.3 %all-to-all-done = bf16[32,128,128]{2,1,0:T(8,128)(2,1)S(1)} async-done(((bf16[32,128,128]{2,1,0:T(8,128)(2,1)}), bf16[32,128,128]{2,1,0:T(8,128)(2,1)S(1)}, u32[]{:S(2)}, u32[]{:S(2)}) %all-to-all-start) | async-done | bytes 1048608 | tf_op jit(solution)/shard_map/all_to_all | solution.py:312
  135.8 0.0 copy-done
  135.8 1.0 copy-done.2
  136.8 47.2 %shard_map.105 = (bf16[32,64,128]{2,1,0:T(8,128)(2,1)}, bf16[8,4,128,128]{3,2,1,0:T(8,128)(2,1)}, f32[1,4096]{1,0:T(1,128)}) custom-call(bf16[4096,128]{1,0:T(8,128)(2,1)} %bitcast.10, bf16[8,4,128,128]{3,2,1,0:T(8,128)(2,1)} %copy-done, f32[1,4096]{1,0:T(1,128)} %bitcast.18), custom_call_target="tpu_custom_call" | custom-call | tf_op jit(solution)/shard_map/pallas_call | solution.py:49
  184.0 4.7 %all-to-all-start.3 = ((bf16[8,4,128,128]{3,2,1,0:T(8,128)(2,1)}), bf16[8,4,128,128]{3,2,1,0:T(8,128)(2,1)S(1)}, u32[]{:S(2)}, u32[]{:S(2)}) async-start(bf16[8,4,128,128]{3,2,1,0:T(8,128)(2,1)} %get-tuple-element.18), calls=%async_computation.3 | async-start | bytes 2097152 | tf_op jit(solution)/shard_map/all_to_all | solution.py:312
  188.7 10.9 %all-to-all-done.3.terms_ref = bf16[8,4,128,128]{3,2,1,0:T(8,128)(2,1)S(1)} async-done(((bf16[8,4,128,128]{3,2,1,0:T(8,128)(2,1)}), bf16[8,4,128,128]{3,2,1,0:T(8,128)(2,1)S(1)}, u32[]{:S(2)}, u32[]{:S(2)}) %all-to-all-start.3) | async-done | bytes 1048608 | tf_op jit(solution)/shard_map/all_to_all | solution.py:312
  199.6 1.0 copy-done.1
  200.6 3.4 %shard_map.106 = (bf16[128,128]{1,0:T(8,128)(2,1)}, bf16[128,128]{1,0:T(8,128)(2,1)}, bf16[128,128]{1,0:T(8,128)(2,1)}, bf16[128,128]{1,0:T(8,128)(2,1)}, bf16[16,128,128]{2,1,0:T(8,128)(2,1)}) custom-call(s32[1]{0:T(128)} %bitcast.me_ref, bf16[8,4,128,128]{3,2,1,0:T(8,128)(2,1)} %copy-done.1, bf16[4,128,2048]{2,1,0:T(8,128)(2,1)} %bitcast.11), custom_call_target="tpu_custom_call" | custom-call | tf_op jit(solution)/shard_map/pallas_call | solution.py:49
  204.0 20.5 %all_to_all.41.parts_ref = bf16[16,128,128]{2,1,0:T(8,128)(2,1)} all-to-all(bf16[16,128,128]{2,1,0:T(8,128)(2,1)} %get-tuple-element.26), channel_id=1, replica_groups=mesh['zg'=4,'zp'=2,'x'=4,'dp'=16] {'dp'}, dimensions={0} | all-to-all | bytes 1048576 | tf_op jit(solution)/shard_map/all_to_all | solution.py:312
  224.5 1.8 shard_map.109
  226.3 10.9 %all_to_all.42.parts_ref = bf16[8,128,128]{2,1,0:T(8,128)(2,1)} all-to-all(bf16[8,128,128]{2,1,0:T(8,128)(2,1)} %shard_map.109), channel_id=1, replica_groups=mesh['zg'=4,'zp'=2,'x'=4,'dp'=16] {'zp','x'}, dimensions={0} | all-to-all | bytes 524288 | tf_op jit(solution)/shard_map/all_to_all | solution.py:312
  237.2 5.9 %all-to-all-start.4 = ((bf16[32,64,128]{2,1,0:T(8,128)(2,1)}), bf16[32,64,128]{2,1,0:T(8,128)(2,1)S(1)}, u32[]{:S(2)}, u32[]{:S(2)}) async-start(bf16[32,64,128]{2,1,0:T(8,128)(2,1)} %get-tuple-element.24), calls=%async_computation.4 | async-start | bytes 1048576 | tf_op jit(solution)/shard_map/all_to_all | solution.py:312
  243.1 1.6 shard_map.110
  244.7 16.0 %all-to-all-done.4.packed_ref = bf16[32,64,128]{2,1,0:T(8,128)(2,1)S(1)} async-done(((bf16[32,64,128]{2,1,0:T(8,128)(2,1)}), bf16[32,64,128]{2,1,0:T(8,128)(2,1)S(1)}, u32[]{:S(2)}, u32[]{:S(2)}) %all-to-all-start.4) | async-done | bytes 524320 | tf_op jit(solution)/shard_map/all_to_all | solution.py:312
  260.8 3.3 %all-to-all-start.7 = ((bf16[4,128,128]{2,1,0:T(8,128)(2,1)}), bf16[4,128,128]{2,1,0:T(8,128)(2,1)S(1)}, u32[]{:S(2)}, u32[]{:S(2)}) async-start(bf16[4,128,128]{2,1,0:T(8,128)(2,1)} %shard_map.110), calls=%async_computation.7 | async-start | bytes 262144 | tf_op jit(solution)/shard_map/all_to_all | solution.py:312
  264.1 0.0 copy-done.10
  264.1 4.8 %collective-permute-start = (bf16[128,128]{1,0:T(8,128)(2,1)S(1)}, bf16[128,128]{1,0:T(8,128)(2,1)S(1)}, u32[]{:S(2)}, u32[]{:S(2)}) collective-permute-start(bf16[128,128]{1,0:T(8,128)(2,1)S(1)} %copy-done.10), channel_id=1, source_target_pairs={{0,128},{128,256},{256,384},{384,0},{1,129},{129,257},{257,385},{3... | collective-permute-start | bytes 98312 | tf_op jit(solution)/shard_map/ppermute | solution.py:320
  268.9 0.0 copy-done.9
  268.9 5.5 %collective-permute-start.1 = (bf16[128,128]{1,0:T(8,128)(2,1)S(1)}, bf16[128,128]{1,0:T(8,128)(2,1)S(1)}, u32[]{:S(2)}, u32[]{:S(2)}) collective-permute-start(bf16[128,128]{1,0:T(8,128)(2,1)S(1)} %copy-done.9), channel_id=1, source_target_pairs={{0,256},{128,384},{256,0},{384,128},{1,257},{129,385},{257,1},{385... | collective-permute-start | bytes 98312 | tf_op jit(solution)/shard_map/ppermute | solution.py:320
  274.4 0.0 copy-done.8
  274.4 5.5 %collective-permute-start.2 = (bf16[128,128]{1,0:T(8,128)(2,1)S(1)}, bf16[128,128]{1,0:T(8,128)(2,1)S(1)}, u32[]{:S(2)}, u32[]{:S(2)}) collective-permute-start(bf16[128,128]{1,0:T(8,128)(2,1)S(1)} %copy-done.8), channel_id=1, source_target_pairs={{0,384},{128,0},{256,128},{384,256},{1,385},{129,1},{257,129},{385... | collective-permute-start | bytes 98312 | tf_op jit(solution)/shard_map/ppermute | solution.py:320
  279.9 0.0 copy-done.3
  279.9 2.1 shard_map.108
  282.0 0.0 collective-permute-done.refs_1_
  282.0 0.0 collective-permute-done.1.refs_2_
  282.0 0.0 copy-start.6
  282.0 0.0 collective-permute-done.2.refs_3_
  282.0 0.0 copy-start.7
  282.0 0.6 copy-done.5
  282.6 0.0 copy-done.6
  282.6 0.0 copy-done.7
  282.6 3.2 %shard_map.107 = bf16[128,2048]{1,0:T(8,128)(2,1)} custom-call(s32[1]{0:T(128)} %bitcast.me_ref, bf16[2048,512]{1,0:T(8,128)(2,1)} %all-gather.4.cloned.1.call-done.weight_ref, bf16[128,128]{1,0:T(8,128)(2,1)} %get-tuple-element.20.refs_0_, bf16[128,128]{1,0:T(8,128)(2,1)} %copy-done.5, bf16[128,128]{1,0:T(8,128)(2,1)} %copy-done.6, bf16[128,128]{1,0:T(8,128)(2,1)} %copy-done.7), custom_call_target="tpu_custom_call" | custom-call | tf_op jit(solution)/shard_map/pallas_call | solution.py:49
  285.8 0.0 all-to-all-done.7.parts_ref
  285.8 0.7 copy-done.4
  286.4 1.8 shard_map.111
  (10 shorter events, 0.0 us)
Async XLA Ops:
  7.2 49.9 %all-gather.4.cloned.1.call-start = ((), (), s32[]{:S(2)}) async-start(), calls=%async_computation.8 | async-start | bytes 2228224 | tf_op jit(solution)/shard_map/all_gather | solution.py:316
  78.7 16.8 %all-to-all-start.2 = ((bf16[8,4,128,128]{3,2,1,0:T(8,128)(2,1)}), bf16[8,4,128,128]{3,2,1,0:T(8,128)(2,1)S(1)}, u32[]{:S(2)}, u32[]{:S(2)}) async-start(bf16[8,4,128,128]{3,2,1,0:T(8,128)(2,1)} %shard_map.104), calls=%async_computation.2 | async-start | bytes 2097152 | tf_op jit(solution)/shard_map/all_to_all | solution.py:312
  95.6 40.3 %copy-start = (bf16[8,4,128,128]{3,2,1,0:T(8,128)(2,1)}, bf16[8,4,128,128]{3,2,1,0:T(8,128)(2,1)S(1)}, u32[]{:S(2)}) copy-start(bf16[8,4,128,128]{3,2,1,0:T(8,128)(2,1)S(1)} %all-to-all-done.2.parts_ref) | copy-start | bytes 3145732
  95.6 40.3 %all-to-all-start = ((bf16[32,128,128]{2,1,0:T(8,128)(2,1)}), bf16[32,128,128]{2,1,0:T(8,128)(2,1)S(1)}, u32[]{:S(2)}, u32[]{:S(2)}) async-start(bf16[32,128,128]{2,1,0:T(8,128)(2,1)} %shard_map.102), calls=%async_computation | async-start | bytes 2097152 | tf_op jit(solution)/shard_map/all_to_all | solution.py:312
  101.8 97.8 %all-gather.6.cloned.1.call-start = ((), (), s32[]{:S(2)}) async-start(), calls=%async_computation.9 | async-start | bytes 2621440 | tf_op jit(solution)/shard_map/all_gather | solution.py:316
  135.8 1.0 copy-start.2
  184.0 15.6 %all-to-all-start.3 = ((bf16[8,4,128,128]{3,2,1,0:T(8,128)(2,1)}), bf16[8,4,128,128]{3,2,1,0:T(8,128)(2,1)S(1)}, u32[]{:S(2)}, u32[]{:S(2)}) async-start(bf16[8,4,128,128]{3,2,1,0:T(8,128)(2,1)} %get-tuple-element.18), calls=%async_computation.3 | async-start | bytes 2097152 | tf_op jit(solution)/shard_map/all_to_all | solution.py:312
  199.6 1.0 copy-start.1
  204.0 60.1 %copy-start.10 = (bf16[128,128]{1,0:T(8,128)(2,1)S(1)}, bf16[128,128]{1,0:T(8,128)(2,1)}, u32[]{:S(2)}) copy-start(bf16[128,128]{1,0:T(8,128)(2,1)} %get-tuple-element.21) | copy-start | bytes 98308
  204.0 64.9 %copy-start.9 = (bf16[128,128]{1,0:T(8,128)(2,1)S(1)}, bf16[128,128]{1,0:T(8,128)(2,1)}, u32[]{:S(2)}) copy-start(bf16[128,128]{1,0:T(8,128)(2,1)} %get-tuple-element.22) | copy-start | bytes 98308
  204.0 70.4 %copy-start.8 = (bf16[128,128]{1,0:T(8,128)(2,1)S(1)}, bf16[128,128]{1,0:T(8,128)(2,1)}, u32[]{:S(2)}) copy-start(bf16[128,128]{1,0:T(8,128)(2,1)} %get-tuple-element.23) | copy-start | bytes 98308
  237.2 23.5 %all-to-all-start.4 = ((bf16[32,64,128]{2,1,0:T(8,128)(2,1)}), bf16[32,64,128]{2,1,0:T(8,128)(2,1)S(1)}, u32[]{:S(2)}, u32[]{:S(2)}) async-start(bf16[32,64,128]{2,1,0:T(8,128)(2,1)} %get-tuple-element.24), calls=%async_computation.4 | async-start | bytes 1048576 | tf_op jit(solution)/shard_map/all_to_all | solution.py:312
  260.8 19.1 %copy-start.3 = (bf16[32,64,128]{2,1,0:T(8,128)(2,1)}, bf16[32,64,128]{2,1,0:T(8,128)(2,1)S(1)}, u32[]{:S(2)}) copy-start(bf16[32,64,128]{2,1,0:T(8,128)(2,1)S(1)} %all-to-all-done.4.packed_ref) | copy-start | bytes 1572868
  260.8 25.0 %all-to-all-start.7 = ((bf16[4,128,128]{2,1,0:T(8,128)(2,1)}), bf16[4,128,128]{2,1,0:T(8,128)(2,1)S(1)}, u32[]{:S(2)}, u32[]{:S(2)}) async-start(bf16[4,128,128]{2,1,0:T(8,128)(2,1)} %shard_map.110), calls=%async_computation.7 | async-start | bytes 262144 | tf_op jit(solution)/shard_map/all_to_all | solution.py:312
  264.1 17.9 %collective-permute-start = (bf16[128,128]{1,0:T(8,128)(2,1)S(1)}, bf16[128,128]{1,0:T(8,128)(2,1)S(1)}, u32[]{:S(2)}, u32[]{:S(2)}) collective-permute-start(bf16[128,128]{1,0:T(8,128)(2,1)S(1)} %copy-done.10), channel_id=1, source_target_pairs={{0,128},{128,256},{256,384},{384,0},{1,129},{129,257},{257,385},{3... | collective-permute-start | bytes 98312 | tf_op jit(solution)/shard_map/ppermute | solution.py:320
  268.9 13.1 %collective-permute-start.1 = (bf16[128,128]{1,0:T(8,128)(2,1)S(1)}, bf16[128,128]{1,0:T(8,128)(2,1)S(1)}, u32[]{:S(2)}, u32[]{:S(2)}) collective-permute-start(bf16[128,128]{1,0:T(8,128)(2,1)S(1)} %copy-done.9), channel_id=1, source_target_pairs={{0,256},{128,384},{256,0},{384,128},{1,257},{129,385},{257,1},{385... | collective-permute-start | bytes 98312 | tf_op jit(solution)/shard_map/ppermute | solution.py:320
  274.4 7.6 %collective-permute-start.2 = (bf16[128,128]{1,0:T(8,128)(2,1)S(1)}, bf16[128,128]{1,0:T(8,128)(2,1)S(1)}, u32[]{:S(2)}, u32[]{:S(2)}) collective-permute-start(bf16[128,128]{1,0:T(8,128)(2,1)S(1)} %copy-done.8), channel_id=1, source_target_pairs={{0,384},{128,0},{256,128},{384,256},{1,385},{129,1},{257,129},{385... | collective-permute-start | bytes 98312 | tf_op jit(solution)/shard_map/ppermute | solution.py:320
  282.0 0.6 copy-start.5
  282.0 0.6 copy-start.6
  282.0 0.6 copy-start.7
  285.8 0.7 copy-start.4
Sparse Core Ops, SparseCore 0:
  10.7 46.4 all-gather.3
  104.7 54.3 all-gather.5

commit v5 on v4

--- a/solution.py
+++ b/solution.py
@@ -12,7 +12,10 @@
 HD = 64
 LANES = 128
 LOG2E = 1.4426950408889634
-BLOCK = 512
+BLOCK = 1024
+STRIP = 32
+PARTS = 4
+GRAD_PARTS = 1
 ONES = HD + 16
 SP = ("zg", "zp", "x")
 GROUP = ("zp", "x")
@@ -140,46 +143,52 @@
     lax.fori_loop(0, count, prepare, 0)
 
     def tiles(block):
-        return [block[:, k * LANES : (k + 1) * LANES] for k in range(blk // LANES)]
+        return [block[:, k * LANES : (k + 1) * LANES] for k in range(block.shape[1] // LANES)]
+
+    half = blk // 2
 
     def query_block(i, _):
-        rows = span(i)
-
-        def score(j, diagonal):
-            at = span(j)
-            x = x_ref[rows, :]
-            scores = dot(qa_ref[rows, :], ka_ref[at, :], 1, 1)
+        def columns(j, width):
+            return pl.ds(pl.multiple_of(j * blk, blk), width)
+
+        def own_rows(first, size):
+            return pl.ds(pl.multiple_of(i * blk + first, size), size)
+
+        def score(first, size, at, width, diagonal):
+            own = own_rows(first, size)
+            x = x_ref[own, :]
+            here = slice(first, first + size)
+            scores = dot(qa_ref[own, :], ka_ref[at, :], 1, 1)
             if diagonal:
-                sub = lax.broadcasted_iota(jnp.int32, (blk, blk), 0)
-                col = lax.broadcasted_iota(jnp.int32, (blk, blk), 1)
+                sub = lax.broadcasted_iota(jnp.int32, (size, width), 0) + first
+                col = lax.broadcasted_iota(jnp.int32, (size, width), 1)
                 scores = jnp.where(col <= sub, scores, LOWEST)
-            weights = dot(jnp.where(low, jnp.zeros_like(x), x), kv_ref[at, :], 1, 1)
-            s_ref[:, at] = scores
-            dp_ref[:, at] = weights
-            return tiles(scores), tiles(weights)
-
-        def tally(scores, weights, best):
-            total = weighted = None
-            for s, w in zip(scores, weights):
-                e = jnp.exp2(s - best)
-                total = e if total is None else total + e
-                weighted = e * w if weighted is None else weighted + e * w
-            return total, weighted
-
-        scores, weights = score(i, True)
-        best = functools.reduce(jnp.maximum, scores)
-        stat_ref[0] = best
-        stat_ref[1], stat_ref[2] = tally(scores, weights, best)
+            s_ref[here, at] = scores
+            dp_ref[here, at] = dot(jnp.where(low_half(size), jnp.zeros_like(x), x), kv_ref[at, :], 1, 1)
+            for strip in range(size // STRIP):
+                part = slice(first + strip * STRIP, first + (strip + 1) * STRIP)
+                scores, weights = tiles(s_ref[part, at]), tiles(dp_ref[part, at])
+                if diagonal:
+                    best = functools.reduce(jnp.maximum, scores)
+                    total = weighted = jnp.zeros((STRIP, LANES), f32)
+                else:
+                    old = stat_ref[0, part]
+                    best = functools.reduce(jnp.maximum, scores, old)
+                    shrink = jnp.exp2(old - best)
+                    total, weighted = stat_ref[1, part] * shrink, stat_ref[2, part] * shrink
+                for s, w in zip(scores, weights):
+                    e = jnp.exp2(s - best)
+                    total, weighted = total + e, weighted + e * w
+                stat_ref[0, part] = best
+                stat_ref[1, part] = total
+                stat_ref[2, part] = weighted
+
+        score(0, half, columns(i, half), half, True)
+        score(half, half, columns(i, blk), blk, True)
 
         def full_block(j, _):
-            scores, weights = score(j, False)
-            old = stat_ref[0]
-            best = functools.reduce(jnp.maximum, scores, old)
-            shrink = jnp.exp2(old - best)
-            total, weighted = tally(scores, weights, best)
-            stat_ref[0] = best
-            stat_ref[1] = stat_ref[1] * shrink + total
-            stat_ref[2] = stat_ref[2] * shrink + weighted
+            for k in range(PARTS):
+                score(k * blk // PARTS, blk // PARTS, columns(j, blk), blk, False)
             return 0
 
         lax.fori_loop(0, i, full_block, 0)
@@ -192,19 +201,27 @@
         stat_ref[1] = jnp.broadcast_to(row_dot, (blk, LANES))
         acc_ref[...] = jnp.zeros((blk, LANES), f32)
 
-        def gradients(j, _):
-            at = span(j)
-            level, row_dot = stat_ref[0], stat_ref[1]
-            probs = [jnp.exp2(s - level) for s in tiles(s_ref[:, at])]
-            grads = [p * (w - row_dot) for p, w in zip(probs, tiles(dp_ref[:, at]))]
+        def gradients(first, size, at):
+            own = own_rows(first, size)
+            here = slice(first, first + size)
+            level, row_dot = stat_ref[0, here], stat_ref[1, here]
+            probs = [jnp.exp2(s - level) for s in tiles(s_ref[here, at])]
+            grads = [p * (w - row_dot) for p, w in zip(probs, tiles(dp_ref[here, at]))]
             grad_low = jnp.concatenate([g.astype(bf16) for g in grads], axis=1)
             probs_low = jnp.concatenate([p.astype(bf16) for p in probs], axis=1)
-            acc_ref[...] += dot(grad_low, kn_ref[at, :], 1, 0)
-            dkt_ref[:, at] += dot(xt_ref[0:ONES, rows], grad_low, 1, 0)
-            dvt_ref[:, at] += dot(xt_ref[ONES:, rows], probs_low, 1, 0)
+            acc_ref[here] += dot(grad_low, kn_ref[at, :], 1, 0)
+            dkt_ref[:, at] += dot(xt_ref[0:ONES, own], grad_low, 1, 0)
+            dvt_ref[:, at] += dot(xt_ref[ONES:, own], probs_low, 1, 0)
+
+        def full_gradients(j, _):
+            for k in range(GRAD_PARTS):
+                gradients(k * blk // GRAD_PARTS, blk // GRAD_PARTS, columns(j, blk))
             return 0
 
-        lax.fori_loop(0, i + 1, gradients, 0)
+        lax.fori_loop(0, i, full_gradients, 0)
+        gradients(0, half, columns(i, half))
+        gradients(half, half, columns(i, blk))
+        rows = own_rows(0, blk)
         dq = acc_ref[...]
         rows_ref[:, rows] = dq.T[HD : HD + 8]
         dq = dq * scale

time: 296 us -> 284 us (0.959)
  Pallas kernels: 70.3 us -> 57.9 us
    pallas_call x11, Pallas kernels: 70.3 us -> 57.9 us  [call(): pl.pallas_call(kernel, out_shape=out_shapes, in_specs=[pl.BlockSpec(memor...]
  transfers between devices with their start and end apart: 10 -> 10, of which waited for: 5 -> 5; matrix products, arithmetic and copies ran while one was open for 0% -> 0% of each run, Pallas kernels for 19% -> 16%
where the time goes in v5:
time: 284 us; the launch traced here: 283 us
  waiting for transfers between devices  118 us (42%)
  Pallas kernels  57.9 us (20%)
  blocking collectives  48.1 us (17%)
  starting transfers between devices  41 us (14%)
  between operations  14.2 us (5%)
  local copies, waits for them, and re-layouts  3.25 us (1%)
    all_to_all x5, waiting for transfers between devices, exchange(): return lax.all_to_all(x, axes, split_axis=0, concat_axis=0, tiled=True)  69.3 us
    pallas_call x11, Pallas kernels, call(): pl.pallas_call(kernel, out_shape=out_shapes, in_specs=[pl.BlockSpec(memor...  57.9 us
    all_gather x2, waiting for transfers between devices, gather(): return lax.all_gather(x, axes, axis=0, tiled=tiled)  48.2 us
    all_to_all x3, blocking collectives, exchange(): return lax.all_to_all(x, axes, split_axis=0, concat_axis=0, tiled=True)  48.1 us
    all_to_all x5, starting transfers between devices, exchange(): return lax.all_to_all(x, axes, split_axis=0, concat_axis=0, tiled=True)  25.2 us
    ppermute x3, starting transfers between devices, shift(): return lax.ppermute(x, axis, [(k, (k + by) % size) for k in range(size)])  15.7 us
  transfers between devices with their start and end apart: 10, of which 5 were waited for; matrix products, arithmetic and copies ran while one was open for 0% of the time, Pallas kernels for 16%

profile of v5, /device:TPU:2, one launch (start us, length us, event | category | flops | bytes accessed | tf_op | source)
XLA Modules:
  0.0 282.7 jit_solution(4993160137854401467)
XLA Ops:
  7.2 0.0 all-gather.4.cloned.1.call-start
  7.2 1.6 shard_map.101
  8.8 0.0 all-gather.4.cloned.1.call-update
  8.9 48.2 %all-gather.4.cloned.1.call-done.weight_ref = bf16[2048,512]{1,0:T(8,128)(2,1)} async-done(((bf16[128,512]{1,0:T(8,128)(2,1)}), bf16[2048,512]{1,0:T(8,128)(2,1)}) %all-gather.4.cloned.1.call-update) | async-done | bytes 2097168 | tf_op jit(solution)/shard_map/all_gather | solution.py:333
  57.1 2.9 %shard_map.103 = bf16[4,128,128]{2,1,0:T(8,128)(2,1)} custom-call(bf16[128,2048]{1,0:T(8,128)(2,1)} %bitcast.12, bf16[2048,512]{1,0:T(8,128)(2,1)} %all-gather.4.cloned.1.call-done.weight_ref), custom_call_target="tpu_custom_call" | custom-call | tf_op jit(solution)/shard_map/pallas_call | solution.py:52
  60.0 16.7 %all_to_all.40.x_ref = bf16[4,128,128]{2,1,0:T(8,128)(2,1)} all-to-all(bf16[4,128,128]{2,1,0:T(8,128)(2,1)} %shard_map.103), channel_id=1, replica_groups=mesh['zg'=4,'zp'=2,'x'=4,'dp'=16] {'zg'}, dimensions={0} | all-to-all | bytes 262144 | tf_op jit(solution)/shard_map/all_to_all | solution.py:329
  76.7 2.0 shard_map.104
  78.7 5.1 %all-to-all-start.2 = ((bf16[8,4,128,128]{3,2,1,0:T(8,128)(2,1)}), bf16[8,4,128,128]{3,2,1,0:T(8,128)(2,1)S(1)}, u32[]{:S(2)}, u32[]{:S(2)}) async-start(bf16[8,4,128,128]{3,2,1,0:T(8,128)(2,1)} %shard_map.104), calls=%async_computation.2 | async-start | bytes 2097152 | tf_op jit(solution)/shard_map/all_to_all | solution.py:329
  83.8 2.6 shard_map.102
  86.4 9.1 %all-to-all-done.2.parts_ref = bf16[8,4,128,128]{3,2,1,0:T(8,128)(2,1)S(1)} async-done(((bf16[8,4,128,128]{3,2,1,0:T(8,128)(2,1)}), bf16[8,4,128,128]{3,2,1,0:T(8,128)(2,1)S(1)}, u32[]{:S(2)}, u32[]{:S(2)}) %all-to-all-start.2) | async-done | bytes 1048608 | tf_op jit(solution)/shard_map/all_to_all | solution.py:329
  95.6 6.2 %all-to-all-start = ((bf16[32,128,128]{2,1,0:T(8,128)(2,1)}), bf16[32,128,128]{2,1,0:T(8,128)(2,1)S(1)}, u32[]{:S(2)}, u32[]{:S(2)}) async-start(bf16[32,128,128]{2,1,0:T(8,128)(2,1)} %shard_map.102), calls=%async_computation | async-start | bytes 2097152 | tf_op jit(solution)/shard_map/all_to_all | solution.py:329
  101.8 0.0 all-gather.6.cloned.1.call-start
  101.8 0.7 all-gather.6.cloned.1.call-update
  102.5 33.3 %all-to-all-done = bf16[32,128,128]{2,1,0:T(8,128)(2,1)S(1)} async-done(((bf16[32,128,128]{2,1,0:T(8,128)(2,1)}), bf16[32,128,128]{2,1,0:T(8,128)(2,1)S(1)}, u32[]{:S(2)}, u32[]{:S(2)}) %all-to-all-start) | async-done | bytes 1048608 | tf_op jit(solution)/shard_map/all_to_all | solution.py:329
  135.8 0.0 copy-done
  135.8 1.0 copy-done.2
  136.8 34.8 %shard_map.105 = (bf16[32,64,128]{2,1,0:T(8,128)(2,1)}, bf16[8,4,128,128]{3,2,1,0:T(8,128)(2,1)}, f32[1,4096]{1,0:T(1,128)}) custom-call(bf16[4096,128]{1,0:T(8,128)(2,1)} %bitcast.10, bf16[8,4,128,128]{3,2,1,0:T(8,128)(2,1)} %copy-done, f32[1,4096]{1,0:T(1,128)} %bitcast.18), custom_call_target="tpu_custom_call" | custom-call | tf_op jit(solution)/shard_map/pallas_call | solution.py:52
  171.6 4.7 %all-to-all-start.3 = ((bf16[8,4,128,128]{3,2,1,0:T(8,128)(2,1)}), bf16[8,4,128,128]{3,2,1,0:T(8,128)(2,1)S(1)}, u32[]{:S(2)}, u32[]{:S(2)}) async-start(bf16[8,4,128,128]{3,2,1,0:T(8,128)(2,1)} %get-tuple-element.18), calls=%async_computation.3 | async-start | bytes 2097152 | tf_op jit(solution)/shard_map/all_to_all | solution.py:329
  176.3 10.9 %all-to-all-done.3.terms_ref = bf16[8,4,128,128]{3,2,1,0:T(8,128)(2,1)S(1)} async-done(((bf16[8,4,128,128]{3,2,1,0:T(8,128)(2,1)}), bf16[8,4,128,128]{3,2,1,0:T(8,128)(2,1)S(1)}, u32[]{:S(2)}, u32[]{:S(2)}) %all-to-all-start.3) | async-done | bytes 1048608 | tf_op jit(solution)/shard_map/all_to_all | solution.py:329
  187.2 1.0 copy-done.1
  188.2 3.4 %shard_map.106 = (bf16[128,128]{1,0:T(8,128)(2,1)}, bf16[128,128]{1,0:T(8,128)(2,1)}, bf16[128,128]{1,0:T(8,128)(2,1)}, bf16[128,128]{1,0:T(8,128)(2,1)}, bf16[16,128,128]{2,1,0:T(8,128)(2,1)}) custom-call(s32[1]{0:T(128)} %bitcast.me_ref, bf16[8,4,128,128]{3,2,1,0:T(8,128)(2,1)} %copy-done.1, bf16[4,128,2048]{2,1,0:T(8,128)(2,1)} %bitcast.11), custom_call_target="tpu_custom_call" | custom-call | tf_op jit(solution)/shard_map/pallas_call | solution.py:52
  191.6 20.5 %all_to_all.41.parts_ref = bf16[16,128,128]{2,1,0:T(8,128)(2,1)} all-to-all(bf16[16,128,128]{2,1,0:T(8,128)(2,1)} %get-tuple-element.26), channel_id=1, replica_groups=mesh['zg'=4,'zp'=2,'x'=4,'dp'=16] {'dp'}, dimensions={0} | all-to-all | bytes 1048576 | tf_op jit(solution)/shard_map/all_to_all | solution.py:329
  212.1 1.8 shard_map.109
  213.9 10.9 %all_to_all.42.parts_ref = bf16[8,128,128]{2,1,0:T(8,128)(2,1)} all-to-all(bf16[8,128,128]{2,1,0:T(8,128)(2,1)} %shard_map.109), channel_id=1, replica_groups=mesh['zg'=4,'zp'=2,'x'=4,'dp'=16] {'zp','x'}, dimensions={0} | all-to-all | bytes 524288 | tf_op jit(solution)/shard_map/all_to_all | solution.py:329
  224.8 5.9 %all-to-all-start.4 = ((bf16[32,64,128]{2,1,0:T(8,128)(2,1)}), bf16[32,64,128]{2,1,0:T(8,128)(2,1)S(1)}, u32[]{:S(2)}, u32[]{:S(2)}) async-start(bf16[32,64,128]{2,1,0:T(8,128)(2,1)} %get-tuple-element.24), calls=%async_computation.4 | async-start | bytes 1048576 | tf_op jit(solution)/shard_map/all_to_all | solution.py:329
  230.7 1.6 shard_map.110
  232.3 16.0 %all-to-all-done.4.packed_ref = bf16[32,64,128]{2,1,0:T(8,128)(2,1)S(1)} async-done(((bf16[32,64,128]{2,1,0:T(8,128)(2,1)}), bf16[32,64,128]{2,1,0:T(8,128)(2,1)S(1)}, u32[]{:S(2)}, u32[]{:S(2)}) %all-to-all-start.4) | async-done | bytes 524320 | tf_op jit(solution)/shard_map/all_to_all | solution.py:329
  248.3 3.3 %all-to-all-start.7 = ((bf16[4,128,128]{2,1,0:T(8,128)(2,1)}), bf16[4,128,128]{2,1,0:T(8,128)(2,1)S(1)}, u32[]{:S(2)}, u32[]{:S(2)}) async-start(bf16[4,128,128]{2,1,0:T(8,128)(2,1)} %shard_map.110), calls=%async_computation.7 | async-start | bytes 262144 | tf_op jit(solution)/shard_map/all_to_all | solution.py:329
  251.7 0.0 copy-done.10
  251.7 4.8 %collective-permute-start = (bf16[128,128]{1,0:T(8,128)(2,1)S(1)}, bf16[128,128]{1,0:T(8,128)(2,1)S(1)}, u32[]{:S(2)}, u32[]{:S(2)}) collective-permute-start(bf16[128,128]{1,0:T(8,128)(2,1)S(1)} %copy-done.10), channel_id=1, source_target_pairs={{0,128},{128,256},{256,384},{384,0},{1,129},{129,257},{257,385},{3... | collective-permute-start | bytes 98312 | tf_op jit(solution)/shard_map/ppermute | solution.py:337
  256.4 0.0 copy-done.9
  256.5 5.5 %collective-permute-start.1 = (bf16[128,128]{1,0:T(8,128)(2,1)S(1)}, bf16[128,128]{1,0:T(8,128)(2,1)S(1)}, u32[]{:S(2)}, u32[]{:S(2)}) collective-permute-start(bf16[128,128]{1,0:T(8,128)(2,1)S(1)} %copy-done.9), channel_id=1, source_target_pairs={{0,256},{128,384},{256,0},{384,128},{1,257},{129,385},{257,1},{385... | collective-permute-start | bytes 98312 | tf_op jit(solution)/shard_map/ppermute | solution.py:337
  261.9 0.0 copy-done.8
  262.0 5.5 %collective-permute-start.2 = (bf16[128,128]{1,0:T(8,128)(2,1)S(1)}, bf16[128,128]{1,0:T(8,128)(2,1)S(1)}, u32[]{:S(2)}, u32[]{:S(2)}) collective-permute-start(bf16[128,128]{1,0:T(8,128)(2,1)S(1)} %copy-done.8), channel_id=1, source_target_pairs={{0,384},{128,0},{256,128},{384,256},{1,385},{129,1},{257,129},{385... | collective-permute-start | bytes 98312 | tf_op jit(solution)/shard_map/ppermute | solution.py:337
  267.4 0.0 copy-done.3
  267.5 2.1 shard_map.108
  269.5 0.0 collective-permute-done.refs_1_
  269.5 0.0 collective-permute-done.1.refs_2_
  269.5 0.0 copy-start.6
  269.6 0.0 collective-permute-done.2.refs_3_
  269.6 0.0 copy-start.7
  269.6 0.6 copy-done.5
  270.1 0.0 copy-done.6
  270.2 0.0 copy-done.7
  270.2 3.2 %shard_map.107 = bf16[128,2048]{1,0:T(8,128)(2,1)} custom-call(s32[1]{0:T(128)} %bitcast.me_ref, bf16[2048,512]{1,0:T(8,128)(2,1)} %all-gather.4.cloned.1.call-done.weight_ref, bf16[128,128]{1,0:T(8,128)(2,1)} %get-tuple-element.20.refs_0_, bf16[128,128]{1,0:T(8,128)(2,1)} %copy-done.5, bf16[128,128]{1,0:T(8,128)(2,1)} %copy-done.6, bf16[128,128]{1,0:T(8,128)(2,1)} %copy-done.7), custom_call_target="tpu_custom_call" | custom-call | tf_op jit(solution)/shard_map/pallas_call | solution.py:52
  273.3 0.0 all-to-all-done.7.parts_ref
  273.3 0.7 copy-done.4
  274.0 1.8 shard_map.111
  (10 shorter events, 0.0 us)
Async XLA Ops:
  7.2 49.9 %all-gather.4.cloned.1.call-start = ((), (), s32[]{:S(2)}) async-start(), calls=%async_computation.8 | async-start | bytes 2228224 | tf_op jit(solution)/shard_map/all_gather | solution.py:333
  78.7 16.8 %all-to-all-start.2 = ((bf16[8,4,128,128]{3,2,1,0:T(8,128)(2,1)}), bf16[8,4,128,128]{3,2,1,0:T(8,128)(2,1)S(1)}, u32[]{:S(2)}, u32[]{:S(2)}) async-start(bf16[8,4,128,128]{3,2,1,0:T(8,128)(2,1)} %shard_map.104), calls=%async_computation.2 | async-start | bytes 2097152 | tf_op jit(solution)/shard_map/all_to_all | solution.py:329
  95.6 40.3 %copy-start = (bf16[8,4,128,128]{3,2,1,0:T(8,128)(2,1)}, bf16[8,4,128,128]{3,2,1,0:T(8,128)(2,1)S(1)}, u32[]{:S(2)}) copy-start(bf16[8,4,128,128]{3,2,1,0:T(8,128)(2,1)S(1)} %all-to-all-done.2.parts_ref) | copy-start | bytes 3145732
  95.6 40.3 %all-to-all-start = ((bf16[32,128,128]{2,1,0:T(8,128)(2,1)}), bf16[32,128,128]{2,1,0:T(8,128)(2,1)S(1)}, u32[]{:S(2)}, u32[]{:S(2)}) async-start(bf16[32,128,128]{2,1,0:T(8,128)(2,1)} %shard_map.102), calls=%async_computation | async-start | bytes 2097152 | tf_op jit(solution)/shard_map/all_to_all | solution.py:329
  101.8 85.4 %all-gather.6.cloned.1.call-start = ((), (), s32[]{:S(2)}) async-start(), calls=%async_computation.9 | async-start | bytes 2621440 | tf_op jit(solution)/shard_map/all_gather | solution.py:333
  135.8 1.0 copy-start.2
  171.6 15.6 %all-to-all-start.3 = ((bf16[8,4,128,128]{3,2,1,0:T(8,128)(2,1)}), bf16[8,4,128,128]{3,2,1,0:T(8,128)(2,1)S(1)}, u32[]{:S(2)}, u32[]{:S(2)}) async-start(bf16[8,4,128,128]{3,2,1,0:T(8,128)(2,1)} %get-tuple-element.18), calls=%async_computation.3 | async-start | bytes 2097152 | tf_op jit(solution)/shard_map/all_to_all | solution.py:329
  187.2 1.0 copy-start.1
  191.6 60.1 %copy-start.10 = (bf16[128,128]{1,0:T(8,128)(2,1)S(1)}, bf16[128,128]{1,0:T(8,128)(2,1)}, u32[]{:S(2)}) copy-start(bf16[128,128]{1,0:T(8,128)(2,1)} %get-tuple-element.21) | copy-start | bytes 98308
  191.6 64.8 %copy-start.9 = (bf16[128,128]{1,0:T(8,128)(2,1)S(1)}, bf16[128,128]{1,0:T(8,128)(2,1)}, u32[]{:S(2)}) copy-start(bf16[128,128]{1,0:T(8,128)(2,1)} %get-tuple-element.22) | copy-start | bytes 98308
  191.6 70.4 %copy-start.8 = (bf16[128,128]{1,0:T(8,128)(2,1)S(1)}, bf16[128,128]{1,0:T(8,128)(2,1)}, u32[]{:S(2)}) copy-start(bf16[128,128]{1,0:T(8,128)(2,1)} %get-tuple-element.23) | copy-start | bytes 98308
  224.8 23.5 %all-to-all-start.4 = ((bf16[32,64,128]{2,1,0:T(8,128)(2,1)}), bf16[32,64,128]{2,1,0:T(8,128)(2,1)S(1)}, u32[]{:S(2)}, u32[]{:S(2)}) async-start(bf16[32,64,128]{2,1,0:T(8,128)(2,1)} %get-tuple-element.24), calls=%async_computation.4 | async-start | bytes 1048576 | tf_op jit(solution)/shard_map/all_to_all | solution.py:329
  248.3 19.1 %copy-start.3 = (bf16[32,64,128]{2,1,0:T(8,128)(2,1)}, bf16[32,64,128]{2,1,0:T(8,128)(2,1)S(1)}, u32[]{:S(2)}) copy-start(bf16[32,64,128]{2,1,0:T(8,128)(2,1)S(1)} %all-to-all-done.4.packed_ref) | copy-start | bytes 1572868
  248.3 25.0 %all-to-all-start.7 = ((bf16[4,128,128]{2,1,0:T(8,128)(2,1)}), bf16[4,128,128]{2,1,0:T(8,128)(2,1)S(1)}, u32[]{:S(2)}, u32[]{:S(2)}) async-start(bf16[4,128,128]{2,1,0:T(8,128)(2,1)} %shard_map.110), calls=%async_computation.7 | async-start | bytes 262144 | tf_op jit(solution)/shard_map/all_to_all | solution.py:329
  251.7 17.9 %collective-permute-start = (bf16[128,128]{1,0:T(8,128)(2,1)S(1)}, bf16[128,128]{1,0:T(8,128)(2,1)S(1)}, u32[]{:S(2)}, u32[]{:S(2)}) collective-permute-start(bf16[128,128]{1,0:T(8,128)(2,1)S(1)} %copy-done.10), channel_id=1, source_target_pairs={{0,128},{128,256},{256,384},{384,0},{1,129},{129,257},{257,385},{3... | collective-permute-start | bytes 98312 | tf_op jit(solution)/shard_map/ppermute | solution.py:337
  256.5 13.1 %collective-permute-start.1 = (bf16[128,128]{1,0:T(8,128)(2,1)S(1)}, bf16[128,128]{1,0:T(8,128)(2,1)S(1)}, u32[]{:S(2)}, u32[]{:S(2)}) collective-permute-start(bf16[128,128]{1,0:T(8,128)(2,1)S(1)} %copy-done.9), channel_id=1, source_target_pairs={{0,256},{128,384},{256,0},{384,128},{1,257},{129,385},{257,1},{385... | collective-permute-start | bytes 98312 | tf_op jit(solution)/shard_map/ppermute | solution.py:337
  262.0 7.6 %collective-permute-start.2 = (bf16[128,128]{1,0:T(8,128)(2,1)S(1)}, bf16[128,128]{1,0:T(8,128)(2,1)S(1)}, u32[]{:S(2)}, u32[]{:S(2)}) collective-permute-start(bf16[128,128]{1,0:T(8,128)(2,1)S(1)} %copy-done.8), channel_id=1, source_target_pairs={{0,384},{128,0},{256,128},{384,256},{1,385},{129,1},{257,129},{385... | collective-permute-start | bytes 98312 | tf_op jit(solution)/shard_map/ppermute | solution.py:337
  269.5 0.6 copy-start.5
  269.5 0.6 copy-start.6
  269.6 0.6 copy-start.7
  273.3 0.7 copy-start.4
Sparse Core Ops, SparseCore 0:
  10.7 46.4 all-gather.3
  104.7 54.3 all-gather.5

commit v6 on v5

--- a/solution.py
+++ b/solution.py
@@ -66,13 +66,14 @@
     return jax.ShapeDtypeStruct(dims, dtype)
 
 
-def pack_weights_kernel(key_ref, value_ref, out_ref):
+def pack_weights_kernel(me_ref, key_ref, value_ref, all_ref, own_ref):
     for pair in range(key_ref.shape[1] // LANES):
         at = slice(pair * LANES, (pair + 1) * LANES)
         blocks = merge_pair(key_ref[:, at].astype(f32), value_ref[:, at].astype(f32))
         for k in range(2):
             g = 2 * pair + k
-            out_ref[:, g * LANES : (g + 1) * LANES] = blocks[k].astype(bf16)
+            all_ref[:, g * LANES : (g + 1) * LANES] = blocks[k].astype(bf16)
+    own_ref[...] = all_ref[:, pl.ds(pl.multiple_of(me_ref[0] * LANES, LANES), LANES)]
 
 
 def pack_queries_kernel(query_ref, grad_ref, out_ref):
@@ -84,14 +85,11 @@
 
 
 def project_kernel(rows_ref, weight_ref, out_ref):
-    projected = dot(rows_ref[...], weight_ref[...], 1, 0).astype(bf16)
-    for g in range(out_ref.shape[0]):
-        out_ref[g] = projected[:, g * LANES : (g + 1) * LANES]
-
-
-def copies_kernel(x_ref, out_ref):
-    for k in range(out_ref.shape[0]):
-        out_ref[k] = x_ref[...]
+    weight = weight_ref[...]
+    for owner in range(rows_ref.shape[0]):
+        projected = dot(rows_ref[owner], weight, 1, 0).astype(bf16)
+        for member in range(out_ref.shape[0]):
+            out_ref[member, owner] = projected
 
 
 def attend_kernel(
@@ -344,24 +342,26 @@
 def program(inputs, w_key, w_value, queries, cotangent, cum_gate, *, heads, dp, zg, zp, xs):
     _, positions, features = inputs.shape
     kv_width = w_key.shape[1]
-    kv_heads = kv_width // HD
     members = zp * xs
     rows = inputs.reshape(positions, features)
     me = lax.axis_index("zg").astype(jnp.int32).reshape(1)
 
-    weight = call(pack_weights_kernel, shape((w_key.shape[0], 2 * kv_width)), w_key, w_value)
-    weight = gather(weight, "dp", True)
+    near_rows = gather(rows, "zg", False)
     packed = call(
         pack_queries_kernel, shape((heads, positions, LANES)),
         queries.reshape(positions, -1), cotangent.reshape(positions, -1),
     )
     head_rows = exchange(packed, SP).reshape(heads * positions, LANES)
-    projected = call(project_kernel, shape((kv_heads, positions, LANES)), rows, weight)
-    group_kv = exchange(projected, "zg")
-    copies = call(copies_kernel, shape((members, *group_kv.shape)), group_kv)
-    head_kv = exchange(copies, GROUP)
-    head_kv, late_rows = lax.optimization_barrier((head_kv, rows))
-    near_rows = gather(late_rows, "zg", False)
+    depth = w_key.shape[0]
+    local, own = call(
+        pack_weights_kernel,
+        (shape((depth, 2 * kv_width)), shape((depth, LANES))),
+        me, w_key, w_value,
+    )
+    weights = gather(local, "dp", True)
+    weight = gather(own, "dp", True)
+    projected = call(project_kernel, shape((members, zg, positions, LANES)), near_rows, weight)
+    head_kv = exchange(projected, GROUP)
 
     dq, dkv, grad_cum = attend(head_rows, head_kv, cum_gate[0])
     terms = exchange(dkv, GROUP)
@@ -372,7 +372,7 @@
         me, terms, near_rows,
     )
     own_sums = [sums[0]] + [shift(sums[k], "zg", zg, k) for k in range(1, zg)]
-    grad_input = call(grad_input_kernel, shape((positions, features)), me, weight, *own_sums)
+    grad_input = call(grad_input_kernel, shape((positions, features)), me, weights, *own_sums)
     parts = exchange(part, "dp")
     grad_queries = call(unpack_queries_kernel, shape((positions, features)), query_parts)
     along = call(sum_parts_kernel, shape((members, LANES, LANES)), parts)

time: 284 us -> 265 us (0.933)
  waiting for transfers between devices: 118 us -> 62 us
  blocking collectives: 48.1 us -> 83.1 us
  starting transfers between devices: 41 us -> 44.7 us
    all_to_all x5 -> x4, waiting for transfers between devices: 69.3 us -> 26.5 us  [exchange(): return lax.all_to_all(x, axes, split_axis=0, concat_axis=0, tiled=True)]
    all_gather x0 -> x1, blocking collectives: none -> 20.6 us  [gather(): return lax.all_gather(x, axes, axis=0, tiled=tiled)]
    all_to_all x3, blocking collectives: 48.1 us -> 62.5 us  [exchange(): return lax.all_to_all(x, axes, split_axis=0, concat_axis=0, tiled=True)]
    all_gather x2, waiting for transfers between devices: 48.2 us -> 34.2 us  [gather(): return lax.all_gather(x, axes, axis=0, tiled=tiled)]
    all_to_all x5 -> x4, starting transfers between devices: 25.2 us -> 28.9 us  [exchange(): return lax.all_to_all(x, axes, split_axis=0, concat_axis=0, tiled=True)]
    pallas_call x11 -> x10, Pallas kernels: 57.9 us -> 56.3 us  [call(): pl.pallas_call(kernel, out_shape=out_shapes, in_specs=[pl.BlockSpec(memor...]
  transfers between devices with their start and end apart: 10 -> 9, of which waited for: 5 -> 3; matrix products, arithmetic and copies ran while one was open for 0% -> 0% of each run, Pallas kernels for 16% -> 7%
where the time goes in v6:
time: 265 us; the launch traced here: 264 us
  blocking collectives  83.1 us (31%)
  waiting for transfers between devices  62 us (23%)
  Pallas kernels  56.3 us (21%)
  starting transfers between devices  44.7 us (17%)
  between operations  15.6 us (6%)
    all_to_all x3, blocking collectives, exchange(): return lax.all_to_all(x, axes, split_axis=0, concat_axis=0, tiled=True)  62.5 us
    pallas_call x10, Pallas kernels, call(): pl.pallas_call(kernel, out_shape=out_shapes, in_specs=[pl.BlockSpec(memor...  56.3 us
    all_gather x2, waiting for transfers between devices, gather(): return lax.all_gather(x, axes, axis=0, tiled=tiled)  34.2 us
    all_to_all x4, starting transfers between devices, exchange(): return lax.all_to_all(x, axes, split_axis=0, concat_axis=0, tiled=True)  28.9 us
    all_to_all x4, waiting for transfers between devices, exchange(): return lax.all_to_all(x, axes, split_axis=0, concat_axis=0, tiled=True)  26.5 us
    all_gather x1, blocking collectives, gather(): return lax.all_gather(x, axes, axis=0, tiled=tiled)  20.6 us
    ppermute x3, starting transfers between devices, shift(): return lax.ppermute(x, axis, [(k, (k + by) % size) for k in range(size)])  15.7 us
  transfers between devices with their start and end apart: 9, of which 3 were waited for; matrix products, arithmetic and copies ran while one was open for 0% of the time, Pallas kernels for 7%

profile of v6, /device:TPU:2, one launch (start us, length us, event | category | flops | bytes accessed | tf_op | source)
XLA Modules:
  0.0 264.0 jit_solution(14771707288437246278)
XLA Ops:
  8.0 0.0 all-gather.5.cloned.1.call-start
  8.0 0.7 all-gather.5.cloned.1.call-update
  8.7 2.6 shard_map.102
  11.3 13.5 %all-to-all-start = ((bf16[32,128,128]{2,1,0:T(8,128)(2,1)}), bf16[32,128,128]{2,1,0:T(8,128)(2,1)S(1)}, u32[]{:S(2)}, u32[]{:S(2)}) async-start(bf16[32,128,128]{2,1,0:T(8,128)(2,1)} %shard_map.102), calls=%async_computation | async-start | bytes 2097152 | tf_op jit(solution)/shard_map/all_to_all | solution.py:327
  24.8 1.6 shard_map.101
  26.4 20.6 %all_gather.11.weight_ref = bf16[2048,128]{1,0:T(8,128)(2,1)} all-gather(bf16[128,128]{1,0:T(8,128)(2,1)} %get-tuple-element.18), channel_id=1, replica_groups=mesh['zg'=4,'zp'=2,'x'=4,'dp'=16] {'dp'}, dimensions={0}, use_global_device_ids=true | all-gather | bytes 557056 | tf_op jit(solution)/shard_map/all_gather | solution.py:331
  47.1 34.2 %all-gather.5.cloned.1.call-done.rows_ref = bf16[4,128,2048]{2,1,0:T(8,128)(2,1)} async-done(((bf16[1,128,2048]{2,1,0:T(8,128)(2,1)}), bf16[4,128,2048]{2,1,0:T(8,128)(2,1)}) %all-gather.5.cloned.1.call-update) | async-done | bytes 2097168 | tf_op jit(solution)/shard_map/all_gather | solution.py:331
  81.3 3.3 %shard_map.103 = bf16[8,4,128,128]{3,2,1,0:T(8,128)(2,1)} custom-call(bf16[4,128,2048]{2,1,0:T(8,128)(2,1)} %all-gather.5.cloned.1.call-done.rows_ref, bf16[2048,128]{1,0:T(8,128)(2,1)} %all_gather.11.weight_ref), custom_call_target="tpu_custom_call" | custom-call | tf_op jit(solution)/shard_map/pallas_call | solution.py:52
  84.7 0.0 all-to-all-done
  84.7 0.0 copy-start
  84.7 23.2 %all_to_all.35.parts_ref = bf16[8,4,128,128]{3,2,1,0:T(8,128)(2,1)} all-to-all(bf16[8,4,128,128]{3,2,1,0:T(8,128)(2,1)} %shard_map.103), channel_id=1, replica_groups=mesh['zg'=4,'zp'=2,'x'=4,'dp'=16] {'zp','x'}, dimensions={0} | all-to-all | bytes 2097152 | tf_op jit(solution)/shard_map/all_to_all | solution.py:327
  107.8 0.0 copy-done
  107.8 34.8 %shard_map.104 = (bf16[32,64,128]{2,1,0:T(8,128)(2,1)}, bf16[8,4,128,128]{3,2,1,0:T(8,128)(2,1)}, f32[1,4096]{1,0:T(1,128)}) custom-call(bf16[4096,128]{1,0:T(8,128)(2,1)} %bitcast.8, bf16[8,4,128,128]{3,2,1,0:T(8,128)(2,1)} %all_to_all.35.parts_ref, f32[1,4096]{1,0:T(1,128)} %bitcast.13), custom_call_target="tpu_custom_call" | custom-call | tf_op jit(solution)/shard_map/pallas_call | solution.py:52
  142.6 5.3 %all-to-all-start.2 = ((bf16[8,4,128,128]{3,2,1,0:T(8,128)(2,1)}), bf16[8,4,128,128]{3,2,1,0:T(8,128)(2,1)S(1)}, u32[]{:S(2)}, u32[]{:S(2)}) async-start(bf16[8,4,128,128]{3,2,1,0:T(8,128)(2,1)} %get-tuple-element.19), calls=%async_computation.2 | async-start | bytes 2097152 | tf_op jit(solution)/shard_map/all_to_all | solution.py:327
  147.9 0.0 all-gather.3.cloned.1.call-start
  147.9 0.6 all-gather.3.cloned.1.call-update
  148.4 11.5 %all-to-all-done.2.terms_ref = bf16[8,4,128,128]{3,2,1,0:T(8,128)(2,1)S(1)} async-done(((bf16[8,4,128,128]{3,2,1,0:T(8,128)(2,1)}), bf16[8,4,128,128]{3,2,1,0:T(8,128)(2,1)S(1)}, u32[]{:S(2)}, u32[]{:S(2)}) %all-to-all-start.2) | async-done | bytes 1048608 | tf_op jit(solution)/shard_map/all_to_all | solution.py:327
  160.0 0.0 copy-start.1
  160.0 1.0 copy-done.1
  161.0 3.4 %shard_map.105 = (bf16[128,128]{1,0:T(8,128)(2,1)}, bf16[128,128]{1,0:T(8,128)(2,1)}, bf16[128,128]{1,0:T(8,128)(2,1)}, bf16[128,128]{1,0:T(8,128)(2,1)}, bf16[16,128,128]{2,1,0:T(8,128)(2,1)}) custom-call(s32[1]{0:T(128)} %bitcast.me_ref, bf16[8,4,128,128]{3,2,1,0:T(8,128)(2,1)} %copy-done.1, bf16[4,128,2048]{2,1,0:T(8,128)(2,1)} %all-gather.5.cloned.1.call-done.rows_ref), custom_call_target="tpu_custom_call" | custom-call | tf_op jit(solution)/shard_map/pallas_call | solution.py:52
  164.4 0.0 copy-start.9
  164.4 27.5 %all_to_all.36.parts_ref = bf16[16,128,128]{2,1,0:T(8,128)(2,1)} all-to-all(bf16[16,128,128]{2,1,0:T(8,128)(2,1)} %get-tuple-element.26), channel_id=1, replica_groups=mesh['zg'=4,'zp'=2,'x'=4,'dp'=16] {'dp'}, dimensions={0} | all-to-all | bytes 1048576 | tf_op jit(solution)/shard_map/all_to_all | solution.py:327
  191.9 1.8 shard_map.108
  193.7 11.8 %all_to_all.37.parts_ref = bf16[8,128,128]{2,1,0:T(8,128)(2,1)} all-to-all(bf16[8,128,128]{2,1,0:T(8,128)(2,1)} %shard_map.108), channel_id=1, replica_groups=mesh['zg'=4,'zp'=2,'x'=4,'dp'=16] {'zp','x'}, dimensions={0} | all-to-all | bytes 524288 | tf_op jit(solution)/shard_map/all_to_all | solution.py:327
  205.5 6.8 %all-to-all-start.3 = ((bf16[32,64,128]{2,1,0:T(8,128)(2,1)}), bf16[32,64,128]{2,1,0:T(8,128)(2,1)S(1)}, u32[]{:S(2)}, u32[]{:S(2)}) async-start(bf16[32,64,128]{2,1,0:T(8,128)(2,1)} %get-tuple-element.24), calls=%async_computation.3 | async-start | bytes 1048576 | tf_op jit(solution)/shard_map/all_to_all | solution.py:327
  212.4 1.6 shard_map.109
  214.0 15.0 %all-to-all-done.3.packed_ref = bf16[32,64,128]{2,1,0:T(8,128)(2,1)S(1)} async-done(((bf16[32,64,128]{2,1,0:T(8,128)(2,1)}), bf16[32,64,128]{2,1,0:T(8,128)(2,1)S(1)}, u32[]{:S(2)}, u32[]{:S(2)}) %all-to-all-start.3) | async-done | bytes 524320 | tf_op jit(solution)/shard_map/all_to_all | solution.py:327
  229.0 3.3 %all-to-all-start.6 = ((bf16[4,128,128]{2,1,0:T(8,128)(2,1)}), bf16[4,128,128]{2,1,0:T(8,128)(2,1)S(1)}, u32[]{:S(2)}, u32[]{:S(2)}) async-start(bf16[4,128,128]{2,1,0:T(8,128)(2,1)} %shard_map.109), calls=%async_computation.6 | async-start | bytes 262144 | tf_op jit(solution)/shard_map/all_to_all | solution.py:327
  232.4 0.0 copy-done.9
  232.4 4.8 %collective-permute-start = (bf16[128,128]{1,0:T(8,128)(2,1)S(1)}, bf16[128,128]{1,0:T(8,128)(2,1)S(1)}, u32[]{:S(2)}, u32[]{:S(2)}) collective-permute-start(bf16[128,128]{1,0:T(8,128)(2,1)S(1)} %copy-done.9), channel_id=1, source_target_pairs={{0,128},{128,256},{256,384},{384,0},{1,129},{129,257},{257,385},{3... | collective-permute-start | bytes 98312 | tf_op jit(solution)/shard_map/ppermute | solution.py:335
  237.1 0.0 copy-done.8
  237.2 5.5 %collective-permute-start.1 = (bf16[128,128]{1,0:T(8,128)(2,1)S(1)}, bf16[128,128]{1,0:T(8,128)(2,1)S(1)}, u32[]{:S(2)}, u32[]{:S(2)}) collective-permute-start(bf16[128,128]{1,0:T(8,128)(2,1)S(1)} %copy-done.8), channel_id=1, source_target_pairs={{0,256},{128,384},{256,0},{384,128},{1,257},{129,385},{257,1},{385... | collective-permute-start | bytes 98312 | tf_op jit(solution)/shard_map/ppermute | solution.py:335
  242.6 0.0 copy-done.7
  242.7 5.5 %collective-permute-start.2 = (bf16[128,128]{1,0:T(8,128)(2,1)S(1)}, bf16[128,128]{1,0:T(8,128)(2,1)S(1)}, u32[]{:S(2)}, u32[]{:S(2)}) collective-permute-start(bf16[128,128]{1,0:T(8,128)(2,1)S(1)} %copy-done.7), channel_id=1, source_target_pairs={{0,384},{128,0},{256,128},{384,256},{1,385},{129,1},{257,129},{385... | collective-permute-start | bytes 98312 | tf_op jit(solution)/shard_map/ppermute | solution.py:335
  248.1 0.0 copy-done.2
  248.2 2.1 shard_map.107
  250.2 0.0 collective-permute-done.refs_1_
  250.2 0.0 collective-permute-done.1.refs_2_
  250.2 0.0 copy-start.5
  250.3 0.0 collective-permute-done.2.refs_3_
  250.3 0.0 copy-start.6
  250.3 0.6 copy-done.4
  250.9 0.0 copy-done.5
  250.9 0.0 copy-done.6
  250.9 3.2 %shard_map.106 = bf16[128,2048]{1,0:T(8,128)(2,1)} custom-call(s32[1]{0:T(128)} %bitcast.me_ref, bf16[2048,512]{1,0:T(8,128)(2,1)} %all-gather.3.cloned.1.call-done.weight_ref, bf16[128,128]{1,0:T(8,128)(2,1)} %get-tuple-element.20.refs_0_, bf16[128,128]{1,0:T(8,128)(2,1)} %copy-done.4, bf16[128,128]{1,0:T(8,128)(2,1)} %copy-done.5, bf16[128,128]{1,0:T(8,128)(2,1)} %copy-done.6), custom_call_target="tpu_custom_call" | custom-call | tf_op jit(solution)/shard_map/pallas_call | solution.py:52
  254.0 0.0 all-to-all-done.6.parts_ref
  254.1 0.6 copy-done.3
  254.7 1.8 shard_map.110
  (6 shorter events, 0.0 us)
Async XLA Ops:
  8.0 73.3 %all-gather.5.cloned.1.call-start = ((), (), s32[]{:S(2)}) async-start(), calls=%async_computation.8 | async-start | bytes 2621440 | tf_op jit(solution)/shard_map/all_gather | solution.py:331
  11.3 73.3 %all-to-all-start = ((bf16[32,128,128]{2,1,0:T(8,128)(2,1)}), bf16[32,128,128]{2,1,0:T(8,128)(2,1)S(1)}, u32[]{:S(2)}, u32[]{:S(2)}) async-start(bf16[32,128,128]{2,1,0:T(8,128)(2,1)} %shard_map.102), calls=%async_computation | async-start | bytes 2097152 | tf_op jit(solution)/shard_map/all_to_all | solution.py:327
  84.7 23.2 %copy-start = (bf16[32,128,128]{2,1,0:T(8,128)(2,1)}, bf16[32,128,128]{2,1,0:T(8,128)(2,1)S(1)}, u32[]{:S(2)}) copy-start(bf16[32,128,128]{2,1,0:T(8,128)(2,1)S(1)} %all-to-all-done) | copy-start | bytes 3145732
  142.6 17.4 %all-to-all-start.2 = ((bf16[8,4,128,128]{3,2,1,0:T(8,128)(2,1)}), bf16[8,4,128,128]{3,2,1,0:T(8,128)(2,1)S(1)}, u32[]{:S(2)}, u32[]{:S(2)}) async-start(bf16[8,4,128,128]{3,2,1,0:T(8,128)(2,1)} %get-tuple-element.19), calls=%async_computation.2 | async-start | bytes 2097152 | tf_op jit(solution)/shard_map/all_to_all | solution.py:327
  147.9 102.4 %all-gather.3.cloned.1.call-start = ((), (), s32[]{:S(2)}) async-start(), calls=%async_computation.7 | async-start | bytes 2228224 | tf_op jit(solution)/shard_map/all_gather | solution.py:331
  160.0 1.0 copy-start.1
  164.4 68.0 %copy-start.9 = (bf16[128,128]{1,0:T(8,128)(2,1)S(1)}, bf16[128,128]{1,0:T(8,128)(2,1)}, u32[]{:S(2)}) copy-start(bf16[128,128]{1,0:T(8,128)(2,1)} %get-tuple-element.21) | copy-start | bytes 98308
  164.4 72.7 %copy-start.8 = (bf16[128,128]{1,0:T(8,128)(2,1)S(1)}, bf16[128,128]{1,0:T(8,128)(2,1)}, u32[]{:S(2)}) copy-start(bf16[128,128]{1,0:T(8,128)(2,1)} %get-tuple-element.22) | copy-start | bytes 98308
  164.4 78.2 %copy-start.7 = (bf16[128,128]{1,0:T(8,128)(2,1)S(1)}, bf16[128,128]{1,0:T(8,128)(2,1)}, u32[]{:S(2)}) copy-start(bf16[128,128]{1,0:T(8,128)(2,1)} %get-tuple-element.23) | copy-start | bytes 98308
  205.5 23.5 %all-to-all-start.3 = ((bf16[32,64,128]{2,1,0:T(8,128)(2,1)}), bf16[32,64,128]{2,1,0:T(8,128)(2,1)S(1)}, u32[]{:S(2)}, u32[]{:S(2)}) async-start(bf16[32,64,128]{2,1,0:T(8,128)(2,1)} %get-tuple-element.24), calls=%async_computation.3 | async-start | bytes 1048576 | tf_op jit(solution)/shard_map/all_to_all | solution.py:327
  229.0 19.1 %copy-start.2 = (bf16[32,64,128]{2,1,0:T(8,128)(2,1)}, bf16[32,64,128]{2,1,0:T(8,128)(2,1)S(1)}, u32[]{:S(2)}) copy-start(bf16[32,64,128]{2,1,0:T(8,128)(2,1)S(1)} %all-to-all-done.3.packed_ref) | copy-start | bytes 1572868
  229.0 25.0 %all-to-all-start.6 = ((bf16[4,128,128]{2,1,0:T(8,128)(2,1)}), bf16[4,128,128]{2,1,0:T(8,128)(2,1)S(1)}, u32[]{:S(2)}, u32[]{:S(2)}) async-start(bf16[4,128,128]{2,1,0:T(8,128)(2,1)} %shard_map.109), calls=%async_computation.6 | async-start | bytes 262144 | tf_op jit(solution)/shard_map/all_to_all | solution.py:327
  232.4 17.9 %collective-permute-start = (bf16[128,128]{1,0:T(8,128)(2,1)S(1)}, bf16[128,128]{1,0:T(8,128)(2,1)S(1)}, u32[]{:S(2)}, u32[]{:S(2)}) collective-permute-start(bf16[128,128]{1,0:T(8,128)(2,1)S(1)} %copy-done.9), channel_id=1, source_target_pairs={{0,128},{128,256},{256,384},{384,0},{1,129},{129,257},{257,385},{3... | collective-permute-start | bytes 98312 | tf_op jit(solution)/shard_map/ppermute | solution.py:335
  237.2 13.1 %collective-permute-start.1 = (bf16[128,128]{1,0:T(8,128)(2,1)S(1)}, bf16[128,128]{1,0:T(8,128)(2,1)S(1)}, u32[]{:S(2)}, u32[]{:S(2)}) collective-permute-start(bf16[128,128]{1,0:T(8,128)(2,1)S(1)} %copy-done.8), channel_id=1, source_target_pairs={{0,256},{128,384},{256,0},{384,128},{1,257},{129,385},{257,1},{385... | collective-permute-start | bytes 98312 | tf_op jit(solution)/shard_map/ppermute | solution.py:335
  242.7 7.6 %collective-permute-start.2 = (bf16[128,128]{1,0:T(8,128)(2,1)S(1)}, bf16[128,128]{1,0:T(8,128)(2,1)S(1)}, u32[]{:S(2)}, u32[]{:S(2)}) collective-permute-start(bf16[128,128]{1,0:T(8,128)(2,1)S(1)} %copy-done.7), channel_id=1, source_target_pairs={{0,384},{128,0},{256,128},{384,256},{1,385},{129,1},{257,129},{385... | collective-permute-start | bytes 98312 | tf_op jit(solution)/shard_map/ppermute | solution.py:335
  250.2 0.6 copy-start.4
  250.2 0.6 copy-start.5
  250.3 0.6 copy-start.6
  254.1 0.7 copy-start.3
Sparse Core Ops, SparseCore 0:
  10.9 70.3 all-gather.4
Sparse Core Ops, SparseCore 1:
  151.0 45.2 all-gather.2

commit v7 on v5

--- a/solution.py
+++ b/solution.py
@@ -87,11 +87,6 @@
     projected = dot(rows_ref[...], weight_ref[...], 1, 0).astype(bf16)
     for g in range(out_ref.shape[0]):
         out_ref[g] = projected[:, g * LANES : (g + 1) * LANES]
-
-
-def copies_kernel(x_ref, out_ref):
-    for k in range(out_ref.shape[0]):
-        out_ref[k] = x_ref[...]
 
 
 def attend_kernel(
@@ -269,10 +264,10 @@
     )
 
 
-def group_sum_kernel(me_ref, terms_ref, rows_ref, *refs):
+def group_sum_kernel(me_ref, terms_ref, left_ref, right_ref, *refs):
     owners = terms_ref.shape[1]
     sums_refs, part_ref = refs[:owners], refs[owners]
-    part = None
+    parts = None
     for k in range(owners):
         owner = lax.rem(me_ref[0] + k, owners)
         total = terms_ref[0, owner].astype(f32)
@@ -280,10 +275,12 @@
             total = total + terms_ref[member, owner].astype(f32)
         low = total.astype(bf16)
         sums_refs[k][...] = low
-        product = dot(low, rows_ref[owner], 1, 0)
-        part = product if part is None else part + product
+        products = [dot(low, rows_ref[owner], 1, 0) for rows_ref in (left_ref, right_ref)]
+        parts = products if parts is None else [p + q for p, q in zip(parts, products)]
+    half = part_ref.shape[0] // 2
     for chunk in range(part_ref.shape[0]):
-        part_ref[chunk] = part[:, chunk * LANES : (chunk + 1) * LANES].astype(bf16)
+        at = slice(chunk % half * LANES, (chunk % half + 1) * LANES)
+        part_ref[chunk] = parts[chunk // half][:, at].astype(bf16)
 
 
 def unpack_queries_kernel(packed_ref, out_ref):
@@ -358,10 +355,10 @@
     head_rows = exchange(packed, SP).reshape(heads * positions, LANES)
     projected = call(project_kernel, shape((kv_heads, positions, LANES)), rows, weight)
     group_kv = exchange(projected, "zg")
-    copies = call(copies_kernel, shape((members, *group_kv.shape)), group_kv)
+    copies = jnp.broadcast_to(group_kv[None], (members, *group_kv.shape))
     head_kv = exchange(copies, GROUP)
-    head_kv, late_rows = lax.optimization_barrier((head_kv, rows))
-    near_rows = gather(late_rows, "zg", False)
+    half = features // 2
+    near_rows = [gather(rows[:, k * half : (k + 1) * half], "zg", False) for k in range(2)]
 
     dq, dkv, grad_cum = attend(head_rows, head_kv, cum_gate[0])
     terms = exchange(dkv, GROUP)
@@ -369,7 +366,7 @@
     *sums, part = call(
         group_sum_kernel,
         (*[shape((LANES, positions))] * zg, shape((dp, LANES, LANES))),
-        me, terms, near_rows,
+        me, terms, *near_rows,
     )
     own_sums = [sums[0]] + [shift(sums[k], "zg", zg, k) for k in range(1, zg)]
     grad_input = call(grad_input_kernel, shape((positions, features)), me, weight, *own_sums)
@@ -379,8 +376,8 @@
     along = exchange(along, GROUP)
     along = call(sum_parts_kernel, shape((zg, LANES, LANES)), along)
     along = exchange(along, "zg")
-    half = shape((LANES, kv_width), f32)
-    grad_key, grad_value = call(finish_kernel, (half, half), along)
+    gradient = shape((LANES, kv_width), f32)
+    grad_key, grad_value = call(finish_kernel, (gradient, gradient), along)
     return grad_input[None], grad_queries[None], grad_cum[None], grad_key, grad_value
 
 

time: 284 us -> 274 us (0.965)
  waiting for transfers between devices: 118 us -> 95.5 us
  starting transfers between devices: 41 us -> 49.3 us
    all_to_all x5, waiting for transfers between devices: 69.3 us -> 26.4 us  [exchange(): return lax.all_to_all(x, axes, split_axis=0, concat_axis=0, tiled=True)]
    all_gather x2 -> x3, waiting for transfers between devices: 48.2 us -> 68.6 us  [gather(): return lax.all_gather(x, axes, axis=0, tiled=tiled)]
    all_to_all x5, starting transfers between devices: 25.2 us -> 33.5 us  [exchange(): return lax.all_to_all(x, axes, split_axis=0, concat_axis=0, tiled=True)]
    pallas_call x11 -> x10, Pallas kernels: 57.9 us -> 55.8 us  [call(): pl.pallas_call(kernel, out_shape=out_shapes, in_specs=[pl.BlockSpec(memor...]
  transfers between devices with their start and end apart: 10 -> 11, of which waited for: 5 -> 4; matrix products, arithmetic and copies ran while one was open for 0% -> 0% of each run, Pallas kernels for 16% -> 17%
where the time goes in v7:
time: 274 us; the launch traced here: 272 us
  waiting for transfers between devices  95.5 us (35%)
  Pallas kernels  55.8 us (20%)
  blocking collectives  50.7 us (19%)
  starting transfers between devices  49.3 us (18%)
  between operations  15.6 us (6%)
  local copies, waits for them, and re-layouts  5.38 us (2%)
    all_gather x3, waiting for transfers between devices, gather(): return lax.all_gather(x, axes, axis=0, tiled=tiled)  68.6 us
    pallas_call x10, Pallas kernels, call(): pl.pallas_call(kernel, out_shape=out_shapes, in_specs=[pl.BlockSpec(memor...  55.8 us
    all_to_all x3, blocking collectives, exchange(): return lax.all_to_all(x, axes, split_axis=0, concat_axis=0, tiled=True)  50.7 us
    all_to_all x5, starting transfers between devices, exchange(): return lax.all_to_all(x, axes, split_axis=0, concat_axis=0, tiled=True)  33.5 us
    all_to_all x5, waiting for transfers between devices, exchange(): return lax.all_to_all(x, axes, split_axis=0, concat_axis=0, tiled=True)  26.4 us
    ppermute x3, starting transfers between devices, shift(): return lax.ppermute(x, axis, [(k, (k + by) % size) for k in range(size)])  15.7 us
  transfers between devices with their start and end apart: 11, of which 4 were waited for; matrix products, arithmetic and copies ran while one was open for 0% of the time, Pallas kernels for 17%

profile of v7, /device:TPU:2, one launch (start us, length us, event | category | flops | bytes accessed | tf_op | source)
XLA Modules:
  0.0 272.4 jit_solution(15788817000676538565)
XLA Ops:
  8.0 0.0 all-gather.6.cloned.1.call-start
  8.0 1.6 shard_map.101
  9.7 0.0 all-gather.6.cloned.1.call-update
  9.7 2.6 shard_map.102
  12.3 13.5 %all-to-all-start = ((bf16[32,128,128]{2,1,0:T(8,128)(2,1)}), bf16[32,128,128]{2,1,0:T(8,128)(2,1)S(1)}, u32[]{:S(2)}, u32[]{:S(2)}) async-start(bf16[32,128,128]{2,1,0:T(8,128)(2,1)} %shard_map.102), calls=%async_computation | async-start | bytes 2097152 | tf_op jit(solution)/shard_map/all_to_all | solution.py:326
  25.8 32.1 %all-gather.6.cloned.1.call-done.weight_ref = bf16[2048,512]{1,0:T(8,128)(2,1)} async-done(((bf16[128,512]{1,0:T(8,128)(2,1)}), bf16[2048,512]{1,0:T(8,128)(2,1)}) %all-gather.6.cloned.1.call-update) | async-done | bytes 2097168 | tf_op jit(solution)/shard_map/all_gather | solution.py:330
  57.9 2.9 %shard_map.103 = bf16[4,128,128]{2,1,0:T(8,128)(2,1)} custom-call(bf16[128,2048]{1,0:T(8,128)(2,1)} %bitcast.12, bf16[2048,512]{1,0:T(8,128)(2,1)} %all-gather.6.cloned.1.call-done.weight_ref), custom_call_target="tpu_custom_call" | custom-call | tf_op jit(solution)/shard_map/pallas_call | solution.py:52
  60.8 0.0 all-to-all-done
  60.8 16.7 %all_to_all.40 = bf16[4,128,128]{2,1,0:T(8,128)(2,1)S(1)} all-to-all(bf16[4,128,128]{2,1,0:T(8,128)(2,1)} %shard_map.103), channel_id=1, replica_groups=mesh['zg'=4,'zp'=2,'x'=4,'dp'=16] {'zg'}, dimensions={0} | all-to-all | bytes 262144 | tf_op jit(solution)/shard_map/all_to_all | solution.py:326
  77.5 1.3 broadcast_in_dim.15
  78.8 5.1 %all-to-all-start.2 = ((bf16[8,4,128,128]{3,2,1,0:T(8,128)(2,1)}), bf16[8,4,128,128]{3,2,1,0:T(8,128)(2,1)S(1)}, u32[]{:S(2)}, u32[]{:S(2)}) async-start(bf16[8,4,128,128]{3,2,1,0:T(8,128)(2,1)} %broadcast_in_dim.15), calls=%async_computation.2 | async-start | bytes 2097152 | tf_op jit(solution)/shard_map/all_to_all | solution.py:326
  83.9 0.0 all-gather.8.cloned.1.call-start
  83.9 0.8 fusion
  84.7 0.0 all-gather.8.cloned.1.call-update
  84.8 10.9 %all-to-all-done.2.parts_ref = bf16[8,4,128,128]{3,2,1,0:T(8,128)(2,1)S(1)} async-done(((bf16[8,4,128,128]{3,2,1,0:T(8,128)(2,1)}), bf16[8,4,128,128]{3,2,1,0:T(8,128)(2,1)S(1)}, u32[]{:S(2)}, u32[]{:S(2)}) %all-to-all-start.2) | async-done | bytes 1048608 | tf_op jit(solution)/shard_map/all_to_all | solution.py:326
  95.7 1.0 copy-done.2
  96.7 34.8 %shard_map.104 = (bf16[32,64,128]{2,1,0:T(8,128)(2,1)}, bf16[8,4,128,128]{3,2,1,0:T(8,128)(2,1)}, f32[1,4096]{1,0:T(1,128)}) custom-call(bf16[4096,128]{1,0:T(8,128)(2,1)} %bitcast.11, bf16[8,4,128,128]{3,2,1,0:T(8,128)(2,1)} %copy-done.2, f32[1,4096]{1,0:T(1,128)} %bitcast.20), custom_call_target="tpu_custom_call" | custom-call | tf_op jit(solution)/shard_map/pallas_call | solution.py:52
  131.5 4.9 %all-to-all-start.3 = ((bf16[8,4,128,128]{3,2,1,0:T(8,128)(2,1)}), bf16[8,4,128,128]{3,2,1,0:T(8,128)(2,1)S(1)}, u32[]{:S(2)}, u32[]{:S(2)}) async-start(bf16[8,4,128,128]{3,2,1,0:T(8,128)(2,1)} %get-tuple-element.15), calls=%async_computation.3 | async-start | bytes 2097152 | tf_op jit(solution)/shard_map/all_to_all | solution.py:326
  136.4 0.6 all-gather.10.cloned.1.call-update
  136.9 0.0 all-gather.8.cloned.1.call-done
  137.0 36.4 %all-gather.10.cloned.1.call-done = bf16[512,1024]{1,0:T(8,128)(2,1)} async-done(((bf16[128,1024]{1,0:T(8,128)(2,1)}), bf16[512,1024]{1,0:T(8,128)(2,1)}) %all-gather.10.cloned.1.call-update) | async-done | bytes 1048592 | tf_op jit(solution)/shard_map/all_gather | solution.py:330
  173.4 0.0 all-to-all-done.3.terms_ref
  173.4 1.0 copy-done.1
  174.4 3.4 %shard_map.105 = (bf16[128,128]{1,0:T(8,128)(2,1)}, bf16[128,128]{1,0:T(8,128)(2,1)}, bf16[128,128]{1,0:T(8,128)(2,1)}, bf16[128,128]{1,0:T(8,128)(2,1)}, bf16[16,128,128]{2,1,0:T(8,128)(2,1)}) custom-call(s32[1]{0:T(128)} %bitcast.me_ref, bf16[8,4,128,128]{3,2,1,0:T(8,128)(2,1)} %copy-done.1, bf16[4,128,1024]{2,1,0:T(8,128)(2,1)} %bitcast.14, ...), custom_call_target="tpu_custom_call" | custom-call | tf_op jit(solution)/shard_map/pallas_call | solution.py:52
  177.8 23.0 %all_to_all.41.parts_ref = bf16[16,128,128]{2,1,0:T(8,128)(2,1)} all-to-all(bf16[16,128,128]{2,1,0:T(8,128)(2,1)} %get-tuple-element.22), channel_id=1, replica_groups=mesh['zg'=4,'zp'=2,'x'=4,'dp'=16] {'dp'}, dimensions={0} | all-to-all | bytes 1048576 | tf_op jit(solution)/shard_map/all_to_all | solution.py:326
  200.8 1.8 shard_map.108
  202.6 11.0 %all_to_all.42.parts_ref = bf16[8,128,128]{2,1,0:T(8,128)(2,1)} all-to-all(bf16[8,128,128]{2,1,0:T(8,128)(2,1)} %shard_map.108), channel_id=1, replica_groups=mesh['zg'=4,'zp'=2,'x'=4,'dp'=16] {'zp','x'}, dimensions={0} | all-to-all | bytes 524288 | tf_op jit(solution)/shard_map/all_to_all | solution.py:326
  213.6 6.7 %all-to-all-start.4 = ((bf16[32,64,128]{2,1,0:T(8,128)(2,1)}), bf16[32,64,128]{2,1,0:T(8,128)(2,1)S(1)}, u32[]{:S(2)}, u32[]{:S(2)}) async-start(bf16[32,64,128]{2,1,0:T(8,128)(2,1)} %get-tuple-element.20), calls=%async_computation.4 | async-start | bytes 1048576 | tf_op jit(solution)/shard_map/all_to_all | solution.py:326
  220.4 1.6 shard_map.109
  222.0 15.5 %all-to-all-done.4.packed_ref = bf16[32,64,128]{2,1,0:T(8,128)(2,1)S(1)} async-done(((bf16[32,64,128]{2,1,0:T(8,128)(2,1)}), bf16[32,64,128]{2,1,0:T(8,128)(2,1)S(1)}, u32[]{:S(2)}, u32[]{:S(2)}) %all-to-all-start.4) | async-done | bytes 524320 | tf_op jit(solution)/shard_map/all_to_all | solution.py:326
  237.5 3.3 %all-to-all-start.7 = ((bf16[4,128,128]{2,1,0:T(8,128)(2,1)}), bf16[4,128,128]{2,1,0:T(8,128)(2,1)S(1)}, u32[]{:S(2)}, u32[]{:S(2)}) async-start(bf16[4,128,128]{2,1,0:T(8,128)(2,1)} %shard_map.109), calls=%async_computation.7 | async-start | bytes 262144 | tf_op jit(solution)/shard_map/all_to_all | solution.py:326
  240.8 0.0 copy-done.11
  240.8 4.8 %collective-permute-start = (bf16[128,128]{1,0:T(8,128)(2,1)S(1)}, bf16[128,128]{1,0:T(8,128)(2,1)S(1)}, u32[]{:S(2)}, u32[]{:S(2)}) collective-permute-start(bf16[128,128]{1,0:T(8,128)(2,1)S(1)} %copy-done.11), channel_id=1, source_target_pairs={{0,128},{128,256},{256,384},{384,0},{1,129},{129,257},{257,385},{3... | collective-permute-start | bytes 98312 | tf_op jit(solution)/shard_map/ppermute | solution.py:334
  245.6 0.0 copy-done.10
  245.6 5.5 %collective-permute-start.1 = (bf16[128,128]{1,0:T(8,128)(2,1)S(1)}, bf16[128,128]{1,0:T(8,128)(2,1)S(1)}, u32[]{:S(2)}, u32[]{:S(2)}) collective-permute-start(bf16[128,128]{1,0:T(8,128)(2,1)S(1)} %copy-done.10), channel_id=1, source_target_pairs={{0,256},{128,384},{256,0},{384,128},{1,257},{129,385},{257,1},{385... | collective-permute-start | bytes 98312 | tf_op jit(solution)/shard_map/ppermute | solution.py:334
  251.1 5.5 %collective-permute-start.2 = (bf16[128,128]{1,0:T(8,128)(2,1)S(1)}, bf16[128,128]{1,0:T(8,128)(2,1)S(1)}, u32[]{:S(2)}, u32[]{:S(2)}) collective-permute-start(bf16[128,128]{1,0:T(8,128)(2,1)S(1)} %copy-done.9), channel_id=1, source_target_pairs={{0,384},{128,0},{256,128},{384,256},{1,385},{129,1},{257,129},{385... | collective-permute-start | bytes 98312 | tf_op jit(solution)/shard_map/ppermute | solution.py:334
  256.6 2.1 shard_map.107
  258.7 0.0 collective-permute-done.refs_1_
  258.7 0.0 collective-permute-done.1.refs_2_
  258.7 0.0 copy-start.7
  258.7 0.0 collective-permute-done.2.refs_3_
  258.7 0.6 copy-done.6
  259.3 0.0 copy-done.7
  259.3 0.0 copy-done.8
  259.3 3.2 %shard_map.106 = bf16[128,2048]{1,0:T(8,128)(2,1)} custom-call(s32[1]{0:T(128)} %bitcast.me_ref, bf16[2048,512]{1,0:T(8,128)(2,1)} %all-gather.6.cloned.1.call-done.weight_ref, bf16[128,128]{1,0:T(8,128)(2,1)} %get-tuple-element.16.refs_0_, bf16[128,128]{1,0:T(8,128)(2,1)} %copy-done.6, bf16[128,128]{1,0:T(8,128)(2,1)} %copy-done.7, bf16[128,128]{1,0:T(8,128)(2,1)} %copy-done.8), custom_call_target="tpu_custom_call" | custom-call | tf_op jit(solution)/shard_map/pallas_call | solution.py:52
  262.5 0.0 all-to-all-done.7.parts_ref
  262.5 0.6 copy-done.5
  263.1 1.8 shard_map.110
  (16 shorter events, 0.0 us)
Async XLA Ops:
  8.0 49.9 %all-gather.6.cloned.1.call-start = ((), (), s32[]{:S(2)}) async-start(), calls=%async_computation.8 | async-start | bytes 2228224 | tf_op jit(solution)/shard_map/all_gather | solution.py:330
  12.3 48.5 %all-to-all-start = ((bf16[32,128,128]{2,1,0:T(8,128)(2,1)}), bf16[32,128,128]{2,1,0:T(8,128)(2,1)S(1)}, u32[]{:S(2)}, u32[]{:S(2)}) async-start(bf16[32,128,128]{2,1,0:T(8,128)(2,1)} %shard_map.102), calls=%async_computation | async-start | bytes 2097152 | tf_op jit(solution)/shard_map/all_to_all | solution.py:326
  60.8 23.1 %copy-start.4 = (bf16[1,128,2048]{2,1,0:T(8,128)(2,1)S(1)}, bf16[1,128,2048]{2,1,0:T(8,128)(2,1)}, u32[]{:S(2)}) copy-start(bf16[1,128,2048]{2,1,0:T(8,128)(2,1)} %param.6) | copy-start | bytes 1572868
  60.8 23.9 %copy-start = (bf16[32,128,128]{2,1,0:T(8,128)(2,1)}, bf16[32,128,128]{2,1,0:T(8,128)(2,1)S(1)}, u32[]{:S(2)}) copy-start(bf16[32,128,128]{2,1,0:T(8,128)(2,1)S(1)} %all-to-all-done) | copy-start | bytes 3145732
  78.8 16.9 %all-to-all-start.2 = ((bf16[8,4,128,128]{3,2,1,0:T(8,128)(2,1)}), bf16[8,4,128,128]{3,2,1,0:T(8,128)(2,1)S(1)}, u32[]{:S(2)}, u32[]{:S(2)}) async-start(bf16[8,4,128,128]{3,2,1,0:T(8,128)(2,1)} %broadcast_in_dim.15), calls=%async_computation.2 | async-start | bytes 2097152 | tf_op jit(solution)/shard_map/all_to_all | solution.py:326
  83.9 53.1 %all-gather.8.cloned.1.call-start = ((), (), s32[]{:S(2)}) async-start(), calls=%async_computation.9 | async-start | bytes 1310720 | tf_op jit(solution)/shard_map/all_gather | solution.py:330
  95.7 1.0 copy-start.2
  131.5 41.9 %all-to-all-start.3 = ((bf16[8,4,128,128]{3,2,1,0:T(8,128)(2,1)}), bf16[8,4,128,128]{3,2,1,0:T(8,128)(2,1)S(1)}, u32[]{:S(2)}, u32[]{:S(2)}) async-start(bf16[8,4,128,128]{3,2,1,0:T(8,128)(2,1)} %get-tuple-element.15), calls=%async_computation.3 | async-start | bytes 2097152 | tf_op jit(solution)/shard_map/all_to_all | solution.py:326
  136.4 37.0 %all-gather.10.cloned.1.call-start = ((), (), s32[]{:S(2)}) async-start(), calls=%async_computation.10 | async-start | bytes 1310720 | tf_op jit(solution)/shard_map/all_gather | solution.py:330
  173.4 1.0 copy-start.1
  177.8 63.0 %copy-start.11 = (bf16[128,128]{1,0:T(8,128)(2,1)S(1)}, bf16[128,128]{1,0:T(8,128)(2,1)}, u32[]{:S(2)}) copy-start(bf16[128,128]{1,0:T(8,128)(2,1)} %get-tuple-element.17) | copy-start | bytes 98308
  177.8 67.8 %copy-start.10 = (bf16[128,128]{1,0:T(8,128)(2,1)S(1)}, bf16[128,128]{1,0:T(8,128)(2,1)}, u32[]{:S(2)}) copy-start(bf16[128,128]{1,0:T(8,128)(2,1)} %get-tuple-element.18) | copy-start | bytes 98308
  177.8 73.3 %copy-start.9 = (bf16[128,128]{1,0:T(8,128)(2,1)S(1)}, bf16[128,128]{1,0:T(8,128)(2,1)}, u32[]{:S(2)}) copy-start(bf16[128,128]{1,0:T(8,128)(2,1)} %get-tuple-element.19) | copy-start | bytes 98308
  213.6 23.9 %all-to-all-start.4 = ((bf16[32,64,128]{2,1,0:T(8,128)(2,1)}), bf16[32,64,128]{2,1,0:T(8,128)(2,1)S(1)}, u32[]{:S(2)}, u32[]{:S(2)}) async-start(bf16[32,64,128]{2,1,0:T(8,128)(2,1)} %get-tuple-element.20), calls=%async_computation.4 | async-start | bytes 1048576 | tf_op jit(solution)/shard_map/all_to_all | solution.py:326
  237.5 19.1 %copy-start.3 = (bf16[32,64,128]{2,1,0:T(8,128)(2,1)}, bf16[32,64,128]{2,1,0:T(8,128)(2,1)S(1)}, u32[]{:S(2)}) copy-start(bf16[32,64,128]{2,1,0:T(8,128)(2,1)S(1)} %all-to-all-done.4.packed_ref) | copy-start | bytes 1572868
  237.5 25.0 %all-to-all-start.7 = ((bf16[4,128,128]{2,1,0:T(8,128)(2,1)}), bf16[4,128,128]{2,1,0:T(8,128)(2,1)S(1)}, u32[]{:S(2)}, u32[]{:S(2)}) async-start(bf16[4,128,128]{2,1,0:T(8,128)(2,1)} %shard_map.109), calls=%async_computation.7 | async-start | bytes 262144 | tf_op jit(solution)/shard_map/all_to_all | solution.py:326
  240.8 17.9 %collective-permute-start = (bf16[128,128]{1,0:T(8,128)(2,1)S(1)}, bf16[128,128]{1,0:T(8,128)(2,1)S(1)}, u32[]{:S(2)}, u32[]{:S(2)}) collective-permute-start(bf16[128,128]{1,0:T(8,128)(2,1)S(1)} %copy-done.11), channel_id=1, source_target_pairs={{0,128},{128,256},{256,384},{384,0},{1,129},{129,257},{257,385},{3... | collective-permute-start | bytes 98312 | tf_op jit(solution)/shard_map/ppermute | solution.py:334
  245.6 13.1 %collective-permute-start.1 = (bf16[128,128]{1,0:T(8,128)(2,1)S(1)}, bf16[128,128]{1,0:T(8,128)(2,1)S(1)}, u32[]{:S(2)}, u32[]{:S(2)}) collective-permute-start(bf16[128,128]{1,0:T(8,128)(2,1)S(1)} %copy-done.10), channel_id=1, source_target_pairs={{0,256},{128,384},{256,0},{384,128},{1,257},{129,385},{257,1},{385... | collective-permute-start | bytes 98312 | tf_op jit(solution)/shard_map/ppermute | solution.py:334
  251.1 7.6 %collective-permute-start.2 = (bf16[128,128]{1,0:T(8,128)(2,1)S(1)}, bf16[128,128]{1,0:T(8,128)(2,1)S(1)}, u32[]{:S(2)}, u32[]{:S(2)}) collective-permute-start(bf16[128,128]{1,0:T(8,128)(2,1)S(1)} %copy-done.9), channel_id=1, source_target_pairs={{0,384},{128,0},{256,128},{384,256},{1,385},{129,1},{257,129},{385... | collective-permute-start | bytes 98312 | tf_op jit(solution)/shard_map/ppermute | solution.py:334
  258.7 0.6 copy-start.6
  258.7 0.6 copy-start.7
  258.7 0.6 copy-start.8
  262.5 0.6 copy-start.5
Sparse Core Ops, SparseCore 0:
  11.5 46.3 all-gather.5
Sparse Core Ops, SparseCore 1:
  86.5 32.6 all-gather.7
  139.5 33.8 all-gather.9
